TPU v7x, 256 devices: a whole 4x4x8 slice. The times are simulated.
256 devices in a mesh: ep: 64 (over z, y, core), tp: 4 (over x).
Axes of the slice: x: 4, y: 4, z: 8, core: 2. Of those that a mesh axis runs over, the one named last changes fastest.
Arguments:
- mixer_in: bfloat16 [32768, 2048], P('ep'), may hold values from -6 to 6
- mixer_gain: float32 [2048], replicated, may hold values from 0.1 to 1.9
- query_weight: bfloat16 [2048, 1024], P(None, 'tp'), may hold values from -0.125 to 0.125
- key_weight: bfloat16 [2048, 1024], P(None, 'tp'), may hold values from -0.125 to 0.125
- value_weight: bfloat16 [2048, 1024], P(None, 'tp'), may hold values from -0.125 to 0.125
- input_gate: float32 [8, 32768], P('tp', 'ep'), may hold values from -4 to 240
- forget_gate: float32 [8, 32768], P('tp', 'ep'), may hold values from 0 to 25
- head_gain: float32 [1024], replicated, may hold values from 0.1 to 1.9
- mixer_out_weight: bfloat16 [1024, 2048], P('tp'), may hold values from -0.1875 to 0.1875
- expert_in: bfloat16 [16384, 2048], P('ep'), may hold values from -6 to 6
- expert_gain: float32 [2048], replicated, may hold values from 0.1 to 1.9
- group_router: bfloat16 [2048, 16], replicated, may hold values from -0.125 to 0.125
- expert_router: bfloat16 [2048, 64], replicated, may hold values from -0.125 to 0.125
- routes: int32 [16384, 2], P('ep'), may hold values from 0 to 63, all different within a row; in each aligned block of 256 rows (0 to 255, 256 to 511, ...) at most 16 rows name the same one
- gate_experts: bfloat16 [64, 2048, 1024], P('ep', None, 'tp'), may hold values from -0.125 to 0.125
- up_experts: bfloat16 [64, 2048, 1024], P('ep', None, 'tp'), may hold values from -0.125 to 0.125
- down_experts: bfloat16 [64, 1024, 2048], P('ep', 'tp'), may hold values from -0.1875 to 0.1875
Outputs:
- mixer_out: bfloat16 [32768, 2048], P(('ep', 'tp'))
- expert_out: bfloat16 [16384, 2048], P('ep', 'tp')
Inputs may be any that keep to these rules, and one draw needn't show every extreme that they name: `routes`: each row names 2 different experts. In each aligned block of 256 rows (the rows of one index of ep) no expert is named by more than 16 rows, a bound that some block reaches.
All inputs are finite; a program needn't handle non-finite values.
Results may differ from a plain program's by a relative error of at most 0.014.
The roundings to bfloat16 on the way count: a program that leaves them out, or rounds other values in their place, can miss the bound.
Values may be sent and summed in bfloat16 or wider, within the bound.
No kernel may reach another device: no remote copies, remote signals or barrier semaphores. Data moves between devices by JAX's collectives and lax.ppermute only.
A program may use at most 128 MiB of HBM per device.

v0:
```python
import jax
import jax.numpy as jnp
from jax import lax
from jax.sharding import Mesh
from jax.sharding import PartitionSpec as P

BLOCK = 128
EP = ("ep_0", "ep_1", "ep_2")
EP_TP = ("ep_0", "ep_1", "ep_2", "tp")


epsilon = 1e-06
highest = lax.Precision.HIGHEST
floor_log = -1e30


def filled_with(x, identity):
    return jax.tree.map(
        lambda a, e: jnp.broadcast_to(jnp.asarray(e, a.dtype), a.shape), x, identity
    )


def collected_together(x, axis):
    leaves = jax.tree.leaves(x)
    order = sorted(range(len(leaves)), key=lambda k: -leaves[k].size)
    width = (1, *leaves[order[0]].shape)[-1]
    lines = [
        jnp.pad(leaves[k].reshape(-1), (0, -leaves[k].size % width)).reshape(-1, width)
        for k in order
    ]
    both, at, found = (lax.all_gather(jnp.concatenate(lines), axis), 0, {})
    for k, line in zip(order, lines):
        slab = both[:, at : at + len(line)].reshape(len(both), -1)
        found[k] = slab[:, : leaves[k].size].reshape(-1, *leaves[k].shape)
        at += len(line)
    numbers = iter(range(len(leaves)))
    return jax.tree.map(lambda _: found[next(numbers)], x)


def prefix_by_axis(x, axes, combine, identity):
    before = start = filled_with(x, identity)
    so_far = x
    for axis in reversed(axes):
        length, place = (lax.axis_size(axis), lax.axis_index(axis))
        pieces = collected_together(so_far, axis)
        inside, so_far = (start, start)
        for k in range(length):
            passed = k < place
            so_far = combine(so_far, jax.tree.map(lambda part: part[k], pieces))
            inside = jax.tree.map(lambda new, old: jnp.where(passed, new, old), so_far, inside)
        before = combine(inside, before)
    return before


def split_up(x, dim, length):
    shape = x.shape
    parts = x.reshape(*shape[:dim], length, shape[dim] // length, *shape[dim + 1 :])
    return jnp.moveaxis(parts, dim, 0)


def sum_at_owner(x, axis, dim):
    length = lax.axis_size(axis)
    parts = lax.all_to_all(split_up(x, dim, length), axis, 0, 0, tiled=True)
    return jnp.sum(parts.astype(jnp.float32), axis=0)


def rms_rows(matrix, gain):
    widened = matrix.astype(jnp.float32)
    scaled = widened * lax.rsqrt(jnp.mean(widened * widened, axis=-1, keepdims=True) + epsilon)
    return scaled * gain


def block_state(keys, value_rows, input_block, forget_block, scale):
    cumulative = jnp.cumsum(forget_block, axis=-1)
    total_log = cumulative[..., -1]
    log_weight = total_log[..., None] - cumulative + input_block
    peak_log = jnp.max(log_weight, axis=-1)
    weights = jnp.exp(log_weight - peak_log[..., None])
    key_float = keys.astype(jnp.float32) * scale
    value_weighted = value_rows.astype(jnp.float32) * weights[..., None]
    memory = jnp.einsum("...sv,...sk->...vk", value_weighted, key_float, precision=highest)
    return (memory, peak_log, total_log)


def merge_state(earlier, later):
    peak_log = jnp.maximum(later[2] + earlier[1], later[1])
    fade_earlier = jnp.exp(later[2] + earlier[1] - peak_log)
    fade_later = jnp.exp(later[1] - peak_log)
    memory = fade_earlier[..., None, None] * earlier[0] + fade_later[..., None, None] * later[0]
    return (memory, peak_log, earlier[2] + later[2])


def block_out(queries, keys, value_rows, input_block, forget_block, state, scale):
    cumulative = jnp.cumsum(forget_block, axis=-1)
    length = cumulative.shape[-1]
    causal = jnp.tril(jnp.ones((length, length), dtype=bool))
    within = jnp.where(
        causal,
        cumulative[..., :, None] - cumulative[..., None, :] + input_block[..., None, :],
        -jnp.inf,
    )
    carried = cumulative + state[1][..., None]
    highest_log = jnp.maximum(jnp.max(within, axis=-1), carried)
    weight_within = jnp.exp(within - highest_log[..., None])
    weight_carried = jnp.exp(carried - highest_log)
    raw_scores = (
        jnp.einsum("...td,...sd->...ts", queries, keys, preferred_element_type=jnp.float32) * scale
    )
    block_scores = raw_scores * weight_within
    numerator = jnp.einsum(
        "...ts,...sd->...td",
        block_scores.astype(jnp.bfloat16),
        value_rows,
        preferred_element_type=jnp.float32,
    )
    query_float = queries.astype(jnp.float32)
    return numerator + weight_carried[..., None] * jnp.einsum(
        "...vk,...tk->...tv", state[0], query_float, precision=highest
    )


def take_block(states, block_index):
    return tuple((member[block_index] for member in states))


def route_weights(group_logits, expert_logits, routes):
    members = expert_logits.shape[1] // group_logits.shape[1]
    chosen = jnp.take_along_axis(expert_logits, routes, axis=1)
    group_pick = jnp.take_along_axis(group_logits, routes // members, axis=1)
    return jax.nn.sigmoid(group_pick) * jax.nn.sigmoid(chosen - chosen[:, ::-1])


def shards(
    mixer_in,
    mixer_gain,
    query_weight,
    key_weight,
    value_weight,
    input_gate,
    forget_gate,
    head_gain,
    mixer_out_weight,
    expert_in,
    expert_gain,
    group_router,
    expert_router,
    routes,
    gate_experts,
    up_experts,
    down_experts,
):
    normed_a = rms_rows(mixer_in, mixer_gain).astype(jnp.bfloat16)
    queries = jnp.dot(normed_a, query_weight, preferred_element_type=jnp.float32).astype(
        jnp.bfloat16
    )
    keys = jnp.dot(normed_a, key_weight, preferred_element_type=jnp.float32).astype(jnp.bfloat16)
    value_rows = jnp.dot(normed_a, value_weight, preferred_element_type=jnp.float32).astype(
        jnp.bfloat16
    )
    row_count = normed_a.shape[0]
    head_local = input_gate.shape[0]
    width_local = queries.shape[1]
    head_size = width_local // head_local
    block_count = row_count // BLOCK
    scale = head_size ** (-0.5)

    def split_heads(matrix):
        return matrix.reshape(block_count, BLOCK, head_local, head_size).transpose(0, 2, 1, 3)

    def split_gates(gates):
        return gates.reshape(head_local, block_count, BLOCK).transpose(1, 0, 2)

    query_blocks = split_heads(queries)
    key_blocks = split_heads(keys)
    value_blocks = split_heads(value_rows)
    input_blocks = split_gates(input_gate)
    forget_blocks = split_gates(jax.nn.log_sigmoid(forget_gate))
    summaries = block_state(key_blocks, value_blocks, input_blocks, forget_blocks, scale)
    summary = take_block(summaries, 0)
    for block_index in range(1, block_count):
        summary = merge_state(summary, take_block(summaries, block_index))
    identity = (
        jnp.zeros_like(summary[0]),
        jnp.full_like(summary[1], floor_log),
        jnp.zeros_like(summary[2]),
    )
    current = prefix_by_axis(summary, EP, merge_state, identity)
    start_list = [current]
    for block_index in range(block_count - 1):
        current = merge_state(current, take_block(summaries, block_index))
        start_list.append(current)
    starts = tuple((jnp.stack([entry[member] for entry in start_list]) for member in range(3)))
    cells = block_out(
        query_blocks, key_blocks, value_blocks, input_blocks, forget_blocks, starts, scale
    )
    cells = cells.transpose(0, 2, 1, 3).reshape(row_count, head_local, head_size)
    gain_local = lax.dynamic_slice_in_dim(
        head_gain, lax.axis_index("tp") * width_local, width_local
    ).reshape(head_local, head_size)
    cell_rows = rms_rows(cells, gain_local).reshape(row_count, width_local).astype(jnp.bfloat16)
    mixer_out = sum_at_owner(
        jnp.dot(cell_rows, mixer_out_weight, preferred_element_type=jnp.float32).astype(
            jnp.bfloat16
        ),
        "tp",
        0,
    ).astype(jnp.bfloat16)
    normed_b = rms_rows(expert_in, expert_gain).astype(jnp.bfloat16)
    group_logits = jnp.dot(normed_b, group_router, preferred_element_type=jnp.float32)
    expert_logits = jnp.dot(normed_b, expert_router, preferred_element_type=jnp.float32)
    combine = route_weights(group_logits, expert_logits, routes)
    token_count = normed_b.shape[0]
    expert_total = expert_logits.shape[1]
    capacity = 4 * token_count // expert_total
    flat_routes = routes.reshape(-1)
    pair_total = flat_routes.shape[0]
    matches = (flat_routes[:, None] == jnp.arange(expert_total, dtype=jnp.int32)[None, :]).astype(
        jnp.int32
    )
    sequence_place = jnp.sum(jnp.cumsum(matches, axis=0) * matches, axis=1) - 1
    slot_index = flat_routes * capacity + sequence_place
    owner = (
        jnp.full((expert_total * capacity,), pair_total, jnp.int32)
        .at[slot_index]
        .set(jnp.arange(pair_total, dtype=jnp.int32))
    )
    padded = jnp.concatenate([normed_b, jnp.zeros((1, normed_b.shape[1]), jnp.bfloat16)], axis=0)
    outgoing = padded[owner // 2].reshape(expert_total, capacity, normed_b.shape[1])
    gate_weight = gate_experts[0]
    up_weight = up_experts[0]
    down_weight = down_experts[0]
    arrived = lax.all_to_all(outgoing, EP, split_axis=0, concat_axis=0, tiled=True)
    gate_act = jnp.einsum("scd,df->scf", arrived, gate_weight, preferred_element_type=jnp.float32)
    up_act = jnp.einsum("scd,df->scf", arrived, up_weight, preferred_element_type=jnp.float32)
    hidden = (jax.nn.silu(gate_act) * up_act).astype(jnp.bfloat16)
    partial_rows = jnp.einsum(
        "scf,fo->sco", hidden, down_weight, preferred_element_type=jnp.float32
    )
    summed = lax.psum_scatter(
        partial_rows.astype(jnp.bfloat16), "tp", scatter_dimension=2, tiled=True
    )
    returned = lax.all_to_all(summed, EP, split_axis=0, concat_axis=0, tiled=True)
    picked = jnp.take(returned.reshape(-1, returned.shape[2]), slot_index, axis=0).astype(
        jnp.float32
    )
    weighted = picked * combine.reshape(-1)[:, None]
    expert_out = jnp.sum(weighted.reshape(token_count, 2, weighted.shape[1]), axis=1).astype(
        jnp.bfloat16
    )
    return (mixer_out, expert_out)


def solution(mesh):
    split = Mesh(mesh.devices.reshape(8, 4, 2, mesh.shape["tp"]), ("ep_0", "ep_1", "ep_2", "tp"))
    placed = (
        P(EP, None),
        P(),
        P(None, "tp"),
        P(None, "tp"),
        P(None, "tp"),
        P("tp", EP),
        P("tp", EP),
        P(),
        P("tp", None),
        P(EP, None),
        P(),
        P(),
        P(),
        P(EP, None),
        P(EP, None, "tp"),
        P(EP, None, "tp"),
        P(EP, "tp", None),
    )
    return jax.shard_map(
        shards,
        mesh=split,
        in_specs=placed,
        out_specs=(P(EP_TP, None), P(EP, "tp")),
        check_vma=False,
    )
```

profile of v0, /device:TPU:1, one launch (start us, length us, event | category | flops | bytes accessed | tf_op | source)
XLA Modules:
  0.0 275.8 jit_solution(7234844089155936487)
XLA Ops:
  9.9 1.5 fusion.3
  13.4 2.4 scatter_custom_fusion
  15.9 1.5 fusion.5
  17.5 6.0 %gather_fusion = bf16[1024,2048]{1,0:T(8,128)(2,1)} fusion(bf16[257,2048]{1,0:T(8,128)(2,1)S(1)} %concatenate.15, s32[1024]{0:T(1024)S(1)} %fusion.84), kind=kCustom, calls=%fused_computation | custom fusion | bytes 8392704 | tf_op jit(solution)/shard_map/gather | solution.py:228
  23.5 13.5 %all-to-all-start.1 = ((bf16[64,16,2048]{2,1,0:T(8,128)(2,1)}), bf16[64,16,2048]{2,1,0:T(8,128)(2,1)}, u32[]{:S(2)}, u32[]{:S(2)}) async-start(bf16[64,16,2048]{2,1,0:T(8,128)(2,1)} %bitcast.570), calls=%async_computation.1 | async-start | bytes 8388608 | tf_op jit(solution)/shard_map/all_to_all | solution.py:232
  37.0 1.2 reduce_window_sum.27
  38.6 2.1 fusion
  40.9 2.5 convolution_convert_fusion.3
  46.1 2.2 all-gather.3
  49.9 15.3 %all-gather.4 = f32[4,258,128]{2,1,0:T(8,128)S(1)} all-gather(f32[1,258,128]{2,1,0:T(8,128)S(1)} %maximum_bitcast_fusion.1), channel_id=3, replica_groups=mesh['ep_0'=8,'ep_1'=4,'ep_2'=2,'tp'=4] {'ep_1'}, dimensions={0}, use_global_device_ids=true | all-gather | bytes 660480 | tf_op jit(solution)/shard_map/all_gather | solution.py:31
  67.3 74.5 %all-to-all-done.1 = bf16[64,16,2048]{2,1,0:T(8,128)(2,1)} async-done(((bf16[64,16,2048]{2,1,0:T(8,128)(2,1)}), bf16[64,16,2048]{2,1,0:T(8,128)(2,1)}, u32[]{:S(2)}, u32[]{:S(2)}) %all-to-all-start.1) | async-done | bytes 4194336 | tf_op jit(solution)/shard_map/all_to_all | solution.py:232
  141.8 4.7 %fusion.14 = f32[64,16,256]{2,1,0:T(8,128)} fusion(bf16[64,16,2048]{2,1,0:T(8,128)(2,1)} %all-to-all-done.1, bf16[1,2048,256]{2,1,0:T(8,128)(2,1)} %param.31), kind=kOutput, calls=%fused_computation.31 | convolution fusion | flops 1073741824 | bytes 6291456 | tf_op jit(solution)/shard_map/scd,df->scf/dot_general | solution.py:233
  146.5 9.1 %convolution_convert_fusion = bf16[64,16,2048]{2,1,0:T(8,128)(2,1)} fusion(bf16[64,16,2048]{2,1,0:T(8,128)(2,1)} %all-to-all-done.1, bf16[1,256,2048]{2,1,0:T(8,128)(2,1)S(1)} %copy-done, bf16[1,2048,256]{2,1,0:T(8,128)(2,1)} %param.32, f32[64,16,256]{2,1,0:T(8,128)} %fusion.14), kind=kOutput, calls=%fused_computation.10 | convolution fusion | flops 2151153664 | bytes 11534336 | tf_op jit(solution)/shard_map/scf,fo->sco/dot_general | solution.py:236
  155.7 3.3 %convolution_convert_fusion.4 = bf16[512,256]{1,0:T(8,128)(2,1)} fusion(bf16[2048,256]{1,0:T(8,128)(2,1)} %param.19, bf16[512,2048]{1,0:T(8,128)(2,1)} %param.17, f32[2048]{0:T(1024)S(1)} %copy-done.49, f32[512]{0:T(512)S(1)} %add_rsqrt_fusion), kind=kOutput, calls=%fused_computation.28 | convolution fusion | flops 541196288 | bytes 3418112 | tf_op jit(solution)/shard_map/dot_general | solution.py:153
  159.0 1.7 reshape.2597
  160.7 1.4 dynamic_slice.3
  169.0 1.3 add_maximum_fusion
  170.4 1.4 fusion.147
  171.7 1.8 multiply_add_fusion
  173.6 1.5 fusion.9
  175.0 2.5 multiply_reduce_fusion.1
  177.7 1.3 copy.118
  179.7 2.0 convolution_convert_fusion.1
  181.7 41.8 %all_to_all.15 = bf16[4,128,2048]{2,1,0:T(8,128)(2,1)} all-to-all(bf16[4,128,2048]{2,1,0:T(8,128)(2,1)S(1)} %bitcast.571), channel_id=1, replica_groups=mesh['ep_0'=8,'ep_1'=4,'ep_2'=2,'tp'=4] {'tp'}, dimensions={0} | all-to-all | bytes 4194304 | tf_op jit(solution)/shard_map/all_to_all | solution.py:63
  223.5 11.6 %all-to-all-start.2 = ((bf16[64,16,512]{2,1,0:T(8,128)(2,1)}), bf16[64,16,512]{2,1,0:T(8,128)(2,1)S(1)}, u32[]{:S(2)}, u32[]{:S(2)}) async-start(bf16[64,16,512]{2,1,0:T(8,128)(2,1)} %reduce-scatter.2.cloned.1.call-done), calls=%async_computation.3 | async-start | bytes 2097152 | tf_op jit(solution)/shard_map/all_to_all | solution.py:242
  236.1 1.4 fusion.159
  237.5 4.5 %gather_fusion.3 = f32[512]{0:T(512)S(1)} fusion(f32[256,64]{0,1:T(8,128)S(1)} %fusion.159, s32[512]{0:T(512)S(1)} %reshape.2644), kind=kCustom, calls=%fused_computation.3 | custom fusion | bytes 8192 | tf_op jit(solution)/shard_map/jit(take_along_axis)/gather | solution.py:128
  242.8 4.6 %gather_fusion.2 = f32[512]{0:T(512)S(1)} fusion(f32[256,16]{0,1:T(8,128)S(1)} %fusion.158, s32[512]{0:T(512)S(1)} %reshape.2638), kind=kCustom, calls=%fused_computation.2 | custom fusion | bytes 8192 | tf_op jit(solution)/shard_map/jit(take_along_axis)/gather | solution.py:129
  247.8 2.9 %reduce_sum.59 = bf16[128,2048]{1,0:T(8,128)(2,1)} reduce(bf16[4,128,2048]{2,1,0:T(8,128)(2,1)} %all_to_all.15, bf16[]{:T(256)} %constant.143.clone.1), dimensions={0}, to_apply=%region_5.6 | reduce | flops 786432 | bytes 2621442 | tf_op jit(solution)/shard_map/reduce_sum | solution.py:64
  250.7 12.5 %all-to-all-done.2 = bf16[64,16,512]{2,1,0:T(8,128)(2,1)S(1)} async-done(((bf16[64,16,512]{2,1,0:T(8,128)(2,1)}), bf16[64,16,512]{2,1,0:T(8,128)(2,1)S(1)}, u32[]{:S(2)}, u32[]{:S(2)}) %all-to-all-start.2) | async-done | bytes 1048608 | tf_op jit(solution)/shard_map/all_to_all | solution.py:242
  263.2 2.0 gather_fusion.1
  265.4 2.9 %multiply_reduce_fusion = bf16[256,512]{1,0:T(8,128)(2,1)} fusion(bf16[256,2,512]{2,1,0:T(2,128)(2,1)S(1)} %gather.19, pred[256,2]{1,0:T(8,128)(4,1)S(1)} %copy.124, f32[256,2]{1,0:T(8,128)S(1)} %copy.130), kind=kLoop, calls=%fused_computation.33 | loop fusion | flops 917504 | bytes 788992 | tf_op jit(solution)/shard_map/reduce_sum | solution.py:247
  (209 shorter events, 20.3 us)
Async XLA Ops:
  8.0 138.6 %copy-start = (bf16[1,256,2048]{2,1,0:T(8,128)(2,1)S(1)}, bf16[1,256,2048]{2,1,0:T(8,128)(2,1)}, u32[]{:S(2)}) copy-start(bf16[1,256,2048]{2,1,0:T(8,128)(2,1)} %param.33) | copy-start | bytes 3145732
  13.3 2.5 copy-start.16
  13.4 2.5 copy-start.24
  23.5 13.5 %copy-start.33 = (f32[2,512]{1,0:T(2,128)S(1)}, f32[2,512]{1,0:T(2,128)}, u32[]{:S(2)}) copy-start(f32[2,512]{1,0:T(2,128)} %param.23) | copy-start | bytes 12292
  23.5 17.4 %copy-start.47 = (bf16[2048,256]{1,0:T(8,128)(2,1)S(1)}, bf16[2048,256]{1,0:T(8,128)(2,1)}, u32[]{:S(2)}) copy-start(bf16[2048,256]{1,0:T(8,128)(2,1)} %param.20) | copy-start | bytes 3145732
  23.5 17.4 %copy-start.49 = (f32[2048]{0:T(1024)S(1)}, f32[2048]{0:T(1024)}, u32[]{:S(2)}) copy-start(f32[2048]{0:T(1024)} %param.18) | copy-start | bytes 24580
  23.5 118.3 %all-to-all-start.1 = ((bf16[64,16,2048]{2,1,0:T(8,128)(2,1)}), bf16[64,16,2048]{2,1,0:T(8,128)(2,1)}, u32[]{:S(2)}, u32[]{:S(2)}) async-start(bf16[64,16,2048]{2,1,0:T(8,128)(2,1)} %bitcast.570), calls=%async_computation.1 | async-start | bytes 8388608 | tf_op jit(solution)/shard_map/all_to_all | solution.py:232
  37.0 127.7 %all-gather.8.cloned.1.call-start = ((), (), s32[]{:S(2)}) async-start(), calls=%async_computation.5 | async-start | bytes 1216512 | tf_op jit(solution)/shard_map/all_gather | solution.py:31
  38.3 123.8 %copy-start.6 = (f32[4,2,128]{2,1,0:T(2,128)}, f32[4,2,128]{2,1,0:T(2,128)S(1)}, u32[]{:S(2)}) copy-start(f32[4,2,128]{2,1,0:T(2,128)S(1)} %reduce_window_sum.27) | copy-start | bytes 12292
  38.5 5.9 %copy-start.20 = (f32[2]{0:T(128)}, f32[2]{0:T(128)S(1)}, u32[]{:S(2)}) copy-start(f32[2]{0:T(128)S(1)} %get-tuple-element.4) | copy-start | bytes 28
  38.5 5.9 %copy-start.22 = (f32[2]{0:T(128)}, f32[2]{0:T(128)S(1)}, u32[]{:S(2)}) copy-start(f32[2]{0:T(128)S(1)} %get-tuple-element.2) | copy-start | bytes 28
  38.5 5.9 %copy-start.23 = (f32[2]{0:T(128)}, f32[2]{0:T(128)S(1)}, u32[]{:S(2)}) copy-start(f32[2]{0:T(128)S(1)} %get-tuple-element.3) | copy-start | bytes 28
  40.9 2.5 copy-start.1
  40.9 2.5 copy-start.48
  44.4 1.7 copy-start.9
  44.6 5.2 %copy-start.2 = (bf16[4,128,2,128]{3,2,1,0:T(2,128)(2,1)}, bf16[4,128,2,128]{3,2,1,0:T(2,128)(2,1)S(1)}, u32[]{:S(2)}) copy-start(bf16[4,128,2,128]{3,2,1,0:T(2,128)(2,1)S(1)} %reshape.2598) | copy-start | bytes 786436
  48.3 1.5 copy-start.18
  48.3 1.5 copy-start.19
  48.3 1.5 copy-start.21
  67.1 156.4 %reduce-scatter.2.cloned.1.call-start = ((), (), s32[]{:S(2)}) async-start(), calls=%async_computation.4 | async-start | bytes 5242880 | tf_op jit(solution)/shard_map/reduce_scatter | solution.py:239
  162.1 1.7 copy-start.11
  163.8 11.2 %copy-start.3 = (bf16[4,128,2,128]{3,2,1,0:T(2,128)(2,1)S(1)}, bf16[4,128,2,128]{3,2,1,0:T(2,128)(2,1)}, u32[]{:S(2)}) copy-start(bf16[4,128,2,128]{3,2,1,0:T(2,128)(2,1)} %copy-done.2) | copy-start | bytes 786436
  164.6 10.4 %copy-start.5 = (bf16[4,128,2,128]{1,3,2,0:T(8,128)(2,1)S(1)}, bf16[4,128,2,128]{1,3,2,0:T(8,128)(2,1)}, u32[]{:S(2)}) copy-start(bf16[4,128,2,128]{1,3,2,0:T(8,128)(2,1)} %copy-done.4) | copy-start | bytes 786436
  164.6 10.4 %copy-start.7 = (f32[4,2,128]{2,1,0:T(2,128)S(1)}, f32[4,2,128]{2,1,0:T(2,128)}, u32[]{:S(2)}) copy-start(f32[4,2,128]{2,1,0:T(2,128)} %copy-done.6) | copy-start | bytes 12292
  164.6 8.9 %copy-start.8 = (bf16[4,128,2,128]{3,2,1,0:T(2,128)(2,1)S(1)}, bf16[4,128,2,128]{3,2,1,0:T(2,128)(2,1)}, u32[]{:S(2)}) copy-start(bf16[4,128,2,128]{3,2,1,0:T(2,128)(2,1)} %reshape.2597) | copy-start | bytes 786436
  170.3 4.7 %copy-start.32 = (f32[4,2,128]{2,1,0:T(2,128)S(1)}, f32[4,2,128]{2,1,0:T(2,128)}, u32[]{:S(2)}) copy-start(f32[4,2,128]{2,1,0:T(2,128)} %add_maximum_fusion) | copy-start | bytes 12292
  173.5 6.1 %copy-start.31 = (f32[256]{0:T(256)S(1)}, f32[256]{0:T(256)}, u32[]{:S(2)}) copy-start(f32[256]{0:T(256)} %dynamic_slice.3) | copy-start | bytes 3076
  181.6 53.4 %copy-start.17 = (s32[512]{0:T(512)S(1)}, s32[512]{0:T(512)}, u32[]{:S(2)}) copy-start(s32[512]{0:T(512)} %copy-done.16) | copy-start | bytes 6148
  181.7 53.6 %copy-start.12 = (s32[256,2]{0,1:T(2,128)S(1)}, s32[256,2]{0,1:T(2,128)}, u32[]{:S(2)}) copy-start(s32[256,2]{0,1:T(2,128)} %param.30) | copy-start | bytes 6148
  223.5 39.8 %all-to-all-start.2 = ((bf16[64,16,512]{2,1,0:T(8,128)(2,1)}), bf16[64,16,512]{2,1,0:T(8,128)(2,1)S(1)}, u32[]{:S(2)}, u32[]{:S(2)}) async-start(bf16[64,16,512]{2,1,0:T(8,128)(2,1)} %reduce-scatter.2.cloned.1.call-done), calls=%async_computation.3 | async-start | bytes 2097152 | tf_op jit(solution)/shard_map/all_to_all | solution.py:242
  237.5 4.9 %copy-start.10 = (bf16[2048,16]{0,1:T(8,128)(2,1)S(1)}, bf16[2048,16]{0,1:T(8,128)(2,1)}, u32[]{:S(2)}) copy-start(bf16[2048,16]{0,1:T(8,128)(2,1)} %param.28) | copy-start | bytes 196612
  242.8 5.0 %copy-start.25 = (s32[512,1]{0,1:T(1,128)S(1)}, s32[512,1]{0,1:T(1,128)}, u32[]{:S(2)}) copy-start(s32[512,1]{0,1:T(1,128)} %copy-done.24) | copy-start | bytes 6148
  (22 other events, 15.8 us)
Sparse Core Ops, SparseCore 0:
  67.2 55.2 all-gather.7
Sparse Core Ops, SparseCore 1:
  155.8 66.6 reduce-scatter.1
where the time goes:
time: 277 us; the launch traced here: 276 us
  waiting for transfers between devices  87.1 us (31%)
  blocking collectives  59.3 us (21%)
  local copies, waits for them, and re-layouts  34.3 us (12%)
  matrix products  28.8 us (10%)
  starting transfers between devices  25.3 us (9%)
  other arithmetic  24.5 us (9%)
  between operations  16.5 us (6%)
    all_to_all x1, waiting for transfers between devices, shards(): lax.all_to_all(outgoing, EP, split_axis=0, concat_axis=0, tiled=True)  74.5 us
    all_to_all x1, blocking collectives, sum_at_owner(): parts = lax.all_to_all(split_up(x, dim, length), axis, 0, 0, tiled=True)  41.8 us
    all_gather x2, blocking collectives, collected_together(): both, at, found = (lax.all_gather(jnp.concatenate(lines), axis), 0, {})  17.5 us
    all_to_all x1, starting transfers between devices, shards(): lax.all_to_all(outgoing, EP, split_axis=0, concat_axis=0, tiled=True)  13.5 us
    all_to_all x1, waiting for transfers between devices, shards(): lax.all_to_all(summed, EP, split_axis=0, concat_axis=0, tiled=True)  12.5 us
    all_to_all x1, starting transfers between devices, shards(): lax.all_to_all(summed, EP, split_axis=0, concat_axis=0, tiled=True)  11.6 us
    dot_general x1, matrix products, shards(): jnp.einsum('scf,fo->sco', hidden, down_weight, preferred_element_type=jnp...  9.1 us
    gather x1, local copies, waits for them, and re-layouts, shards(): padded[owner // 2].reshape(expert_total, capacity, normed_b.shape[1])  5.98 us
  transfers between devices with their start and end apart: 4, of which 2 were waited for; matrix products, arithmetic and copies ran while one was open for 24% of the time, Pallas kernels for 0%

commit v1 on v0

v1 whole, which is shorter than its diff:
```python
import jax
import jax.numpy as jnp
from jax import lax
from jax.experimental import pallas as pl
from jax.experimental.pallas import tpu as pltpu
from jax.sharding import Mesh
from jax.sharding import PartitionSpec as P

EP = ("z", "y", "c")
EP_TP = ("z", "y", "c", "tp")
ZY = ("z", "y")
YC = ("y", "c")
NEAR = [(i, i ^ 1) for i in range(4)]
FAR = [(i, 3 - i) for i in range(4)]
ACROSS = [(i, i ^ 2) for i in range(4)]
SWAP = [(0, 1), (1, 0)]
CROSS = [(c * 4 + t, (c if t < 2 else 1 - c) * 4 + t) for c in range(2) for t in range(4)]
LINES = 136
f32 = jnp.float32
bf16 = jnp.bfloat16

epsilon = 1e-06
highest = lax.Precision.HIGHEST
floor_log = -1e30


def normalized(matrix):
    return matrix * lax.rsqrt(jnp.mean(matrix * matrix, axis=-1, keepdims=True) + epsilon)


def thirds(x):
    high = x.astype(bf16)
    rest = x - high.astype(f32)
    middle = rest.astype(bf16)
    return high, middle, (rest - middle.astype(f32)).astype(bf16)


def merged(earlier, later):
    moved = later[2] + earlier[1]
    peak = jnp.maximum(moved, later[1])
    memory = jnp.exp(moved - peak) * earlier[0] + jnp.exp(later[1] - peak) * later[0]
    return (memory, peak, earlier[2] + later[2])


def summary_at(ref, base):
    return (ref[base : base + 128, :], ref[base + 128 : base + 129, :], ref[base + 129 : base + 130, :])


def put_summary(ref, base, summary):
    row = lax.broadcasted_iota(jnp.int32, (8, 128), 0)
    ref[base : base + 128, :] = summary[0]
    ref[base + 128 : base + 136, :] = jnp.where(
        row == 0, summary[1], jnp.where(row == 1, summary[2], 0.0)
    )


def no_summary():
    return (jnp.zeros((128, 128), f32), jnp.full((1, 128), floor_log, f32), jnp.zeros((1, 128), f32))


def chosen_summary(flag, a, b):
    return tuple(jnp.where(flag, p, q) for p, q in zip(a, b))


def gate_sums(log_forget, input_gate):
    s = lax.broadcasted_iota(jnp.int32, (128, 128), 0)
    t = lax.broadcasted_iota(jnp.int32, (128, 128), 1)
    upto = (s <= t).astype(f32)
    sums = jnp.dot(log_forget[...], upto, preferred_element_type=f32, precision=highest)
    total = jnp.sum(log_forget[...], axis=1, keepdims=True)
    log_weight = total - sums + input_gate[...]
    peak = jnp.max(log_weight, axis=1, keepdims=True)
    return sums, total, log_weight, peak


def as_columns(rows):
    return jnp.concatenate([rows, jnp.zeros((120, 128), f32)], axis=0).T


def mixer_head_kernel(rows, gain, wq, wk, wv, log_forget, input_gate, q, k, v, memories, spread, normed):
    normed[...] = (normalized(rows[...].astype(f32)) * gain[...]).astype(bf16)
    for weight, target in ((wq, q), (wk, k), (wv, v)):
        target[...] = jnp.dot(normed[...], weight[...], preferred_element_type=f32).astype(bf16)
    _, total, log_weight, peak = gate_sums(log_forget, input_gate)
    columns = as_columns(jnp.exp(log_weight - peak))
    for h in range(2):
        whole_summary = None
        for b in range(4):
            n = h * 4 + b
            at = (slice(b * 128, b * 128 + 128), slice(h * 128, h * 128 + 128))
            keys = k[at].astype(f32).T.astype(bf16)
            weighted = v[at].astype(f32) * columns[:, n : n + 1]
            parts = [jnp.dot(keys, p, preferred_element_type=f32) for p in thirds(weighted)]
            memory = (parts[2] + parts[1] + parts[0]) * 128**-0.5
            memories[n * 128 : n * 128 + 128, :] = memory
            ones = jnp.ones((1, 128), f32)
            summary = (memory, peak[n : n + 1, :] * ones, total[n : n + 1, :] * ones)
            whole_summary = summary if b == 0 else merged(whole_summary, summary)
        for y in range(4):
            put_summary(spread, (2 * y + h) * LINES, whole_summary)


def fold_slab_kernel(place, members, spread, before):
    running = no_summary()
    captured = [no_summary(), no_summary()]
    for n in range(8):
        captured[n % 2] = chosen_summary(place[3] == n // 2, running, captured[n % 2])
        running = merged(running, summary_at(members, n * LINES))
    for n in range(8):
        put_summary(spread, n * LINES, running)
    for n in range(2):
        put_summary(before, n * LINES, captured[n])


def fold_all_kernel(place, slabs, before, mine, theirs):
    running = no_summary()
    start = no_summary()
    for n in range(8):
        start = chosen_summary(place[2] == n, running, start)
        if n < 7:
            running = merged(running, summary_at(slabs, n * LINES))
    pair = [merged(start, summary_at(before, n * LINES)) for n in range(2)]
    put_summary(mine, 0, chosen_summary(place[1] == 0, pair[0], pair[1]))
    put_summary(theirs, 0, chosen_summary(place[1] == 0, pair[1], pair[0]))


def mixer_tail_kernel(
    place, q, k, v, log_forget, input_gate, memories, mine, theirs, gain, weight,
    own, near, far, across_near, across_far, cells
):
    sums, total, _, peak = gate_sums(log_forget, input_gate)
    columns = as_columns(sums)
    later = lax.broadcasted_iota(jnp.int32, (128, 128), 1) > lax.broadcasted_iota(
        jnp.int32, (128, 128), 0
    )
    ones = jnp.ones((1, 128), f32)
    for h in range(2):
        state = chosen_summary(place[1] == h, summary_at(mine, 0), summary_at(theirs, 0))
        head_gain = gain[:, pl.ds(pl.multiple_of(place[0] * 256 + h * 128, 128), 128)]
        for b in range(4):
            n = h * 4 + b
            at = (slice(b * 128, b * 128 + 128), slice(h * 128, h * 128 + 128))
            column = columns[:, n : n + 1]
            within = column - sums[n : n + 1, :] + input_gate[n : n + 1, :]
            within = jnp.where(later, floor_log, within)
            carried = column + state[1][:, 0:1]
            top = jnp.maximum(jnp.max(within, axis=1, keepdims=True), carried)
            raw = lax.dot_general(
                q[at], k[at], (((1,), (1,)), ((), ())), preferred_element_type=f32
            )
            scores = raw * 128**-0.5 * jnp.exp(within - top)
            scores = jnp.where(later, 0.0, scores).astype(bf16)
            inside = jnp.dot(scores, v[at], preferred_element_type=f32)
            parts = [jnp.dot(q[at], p, preferred_element_type=f32) for p in thirds(state[0])]
            outside = parts[2] + parts[1] + parts[0]
            cell = inside + jnp.exp(carried - top) * outside
            cells[at] = (normalized(cell) * head_gain).astype(bf16)
            if b < 3:
                block = (memories[n * 128 : n * 128 + 128, :], peak[n : n + 1, :] * ones, total[n : n + 1, :] * ones)
                state = merged(state, block)
    count = own.shape[0]
    rank = place[0]
    for target, device, start in (
        (own, rank, 0),
        (near, rank ^ 1, 0),
        (far, 3 - rank, 0),
        (across_near, rank ^ 2, 0),
        (across_far, rank ^ 2, count // 2),
    ):
        at = pl.ds(pl.multiple_of(device * count + start, count // 2), target.shape[0])
        target[...] = jnp.dot(cells[at, :], weight[...], preferred_element_type=f32).astype(bf16)


def relay_kernel(near, far, from_near, from_far, to_near, to_far):
    half = from_near.shape[0]
    to_far[:half, :] = (far[:half, :].astype(f32) + from_near[...].astype(f32)).astype(bf16)
    to_far[half:, :] = far[half:, :]
    to_near[:half, :] = near[:half, :]
    to_near[half:, :] = (near[half:, :].astype(f32) + from_far[...].astype(f32)).astype(bf16)


def sum_kernel(own, near, far, out):
    total = own[...].astype(f32) + near[...].astype(f32) + far[...].astype(f32)
    out[...] = total.astype(bf16)


def cut_kernel(place, weights, own, near, far, across):
    rank = place[0]
    share = weights.shape[1] // 4
    for target, device in ((own, rank), (near, rank ^ 1), (far, 3 - rank), (across, rank ^ 2)):
        for j, quarter in enumerate((device, 3 - device)):
            target[:, j * share : (j + 1) * share] = weights[
                :, pl.ds(pl.multiple_of(quarter * share, share), share)
            ]


def dispatch_kernel(place, rows, gain, group_router, expert_router, routes, send, notes, normed):
    rank, core = place[0], place[1]
    normed[...] = (normalized(rows[...].astype(f32)) * gain[...]).astype(bf16)
    group_logits = jnp.dot(normed[...], group_router[...], preferred_element_type=f32)
    expert_logits = jnp.dot(normed[...], expert_router[...], preferred_element_type=f32)
    tokens, experts = expert_logits.shape
    groups = group_logits.shape[1]
    expert_ids = lax.broadcasted_iota(jnp.int32, (tokens, experts), 1)
    group_ids = lax.broadcasted_iota(jnp.int32, (tokens, groups), 1)
    table = routes[...]
    named = [table[:, k : k + 1] for k in range(2)]
    hot = [(expert_ids == e).astype(f32) for e in named]
    below = (
        lax.broadcasted_iota(jnp.int32, (tokens, tokens), 1)
        < lax.broadcasted_iota(jnp.int32, (tokens, tokens), 0)
    ).astype(bf16)
    counts = [jnp.dot(below, h.astype(bf16), preferred_element_type=f32) for h in hot]
    counts[1] = counts[1] + jnp.sum(hot[0], axis=0, keepdims=True)
    slots = []
    for k in range(2):
        at = jnp.sum(hot[k] * counts[k], axis=1, keepdims=True).astype(jnp.int32)
        here = ((named[k] & 1) ^ core) == rank // 2
        slots.append(jnp.where(here, (named[k] >> 1) * 16 + at, -1))
    chosen = [jnp.sum(h * expert_logits, axis=1, keepdims=True) for h in hot]
    grouped = [
        jnp.sum(jnp.where(group_ids == e // (experts // groups), group_logits, 0.0), axis=1, keepdims=True)
        for e in named
    ]
    combine = [
        jax.nn.sigmoid(grouped[k]) * jax.nn.sigmoid(chosen[k] - chosen[1 - k]) for k in range(2)
    ]
    lane = lax.broadcasted_iota(jnp.int32, (tokens, 128), 1)
    wide = jnp.where(lane == 0, slots[0].astype(f32), slots[1].astype(f32))
    notes[...] = jnp.where(lane < 2, wide, jnp.where(lane == 2, combine[0], combine[1]))
    across = wide.T
    first, second = (across[k : k + 1].astype(jnp.int32) for k in range(2))
    share = rows.shape[1] // 4
    slot_ids = lax.broadcasted_iota(jnp.int32, (send.shape[0], tokens), 0)
    pick = ((slot_ids == first) | (slot_ids == second)).astype(bf16)
    for j, quarter in enumerate((rank, 3 - rank)):
        features = normed[:, pl.ds(pl.multiple_of(quarter * share, share), share)]
        send[:, j * share : (j + 1) * share] = jnp.dot(
            pick, features, preferred_element_type=f32
        ).astype(bf16)


def hidden_kernel(place, own, other, gate, up, far_gate, far_up, out):
    rank = place[0]
    share = own.shape[1] // 2
    units = gate.shape[1]
    blocks = [
        (own, 0, rank),
        (own, 1, 3 - rank),
        (other, 0, rank ^ 1),
        (other, 1, 3 - (rank ^ 1)),
    ]
    for part, (g, u) in enumerate(((gate, up), (far_gate, far_up))):
        gate_act = up_act = None
        for rows, half, quarter in blocks:
            features = rows[:, half * share : (half + 1) * share]
            at = pl.ds(pl.multiple_of(quarter * share, share), share)
            a = jnp.dot(features, g[at, :], preferred_element_type=f32)
            b = jnp.dot(features, u[at, :], preferred_element_type=f32)
            gate_act = a if gate_act is None else gate_act + a
            up_act = b if up_act is None else up_act + b
        out[:, part * units : (part + 1) * units] = (jax.nn.silu(gate_act) * up_act).astype(bf16)


def down_kernel(own, other, w_own, w_far, w_near, w_across, out):
    units = own.shape[1] // 2
    total = jnp.dot(own[:, :units], w_own[...], preferred_element_type=f32)
    total = total + jnp.dot(own[:, units:], w_far[...], preferred_element_type=f32)
    total = total + jnp.dot(other[:, :units], w_near[...], preferred_element_type=f32)
    total = total + jnp.dot(other[:, units:], w_across[...], preferred_element_type=f32)
    out[...] = total.astype(bf16)


def combine_kernel(notes, rows, keep, send):
    tokens, share = keep.shape
    slots = [notes[:, k : k + 1].astype(jnp.int32) for k in range(2)]
    lanes = lax.broadcasted_iota(jnp.int32, (tokens, rows.shape[0]), 1)
    weight = jnp.where(lanes == slots[0], notes[:, 2:3], 0.0) + jnp.where(
        lanes == slots[1], notes[:, 3:4], 0.0
    )
    high = weight.astype(bf16)
    low = (weight - high.astype(f32)).astype(bf16)
    total = jnp.dot(high, rows[...], preferred_element_type=f32)
    total = total + jnp.dot(low, rows[...], preferred_element_type=f32)
    keep[...] = total[:, :share]
    send[...] = total[:, share:].astype(bf16)


def last_kernel(keep, received, out):
    out[...] = (keep[...] + received[...].astype(f32)).astype(bf16)


def run(kernel, shapes, args, place=None, scratch=()):
    specs = [pl.BlockSpec(memory_space=pltpu.VMEM)] * len(args)
    if place is not None:
        specs = [pl.BlockSpec(memory_space=pltpu.SMEM)] + specs
        args = (place, *args)
    outs = tuple(jax.ShapeDtypeStruct(s, d) for s, d in shapes)
    result = pl.pallas_call(
        kernel,
        out_shape=outs,
        in_specs=specs,
        out_specs=tuple([pl.BlockSpec(memory_space=pltpu.VMEM)] * len(outs)),
        scratch_shapes=[pltpu.VMEM(s, d) for s, d in scratch],
        compiler_params=pltpu.CompilerParams(vmem_limit_bytes=48 * 1024 * 1024),
    )(*args)
    return result if len(outs) > 1 else result[0]


def traded(x, axis):
    return lax.all_to_all(x, axis, 0, 0, tiled=True)


def shards(
    mixer_in,
    mixer_gain,
    query_weight,
    key_weight,
    value_weight,
    input_gate,
    forget_gate,
    head_gain,
    mixer_out_weight,
    expert_in,
    expert_gain,
    group_router,
    expert_router,
    routes,
    gate_experts,
    up_experts,
    down_experts,
):
    place = jnp.stack([lax.axis_index(a) for a in ("tp", "c", "z", "y")]).astype(jnp.int32)
    tokens, width = expert_in.shape
    share = width // 4
    slots = 32 * 16
    gate, up, down = gate_experts[0], up_experts[0], down_experts[0]
    units = gate.shape[1]
    send, notes = run(
        dispatch_kernel,
        (((slots, 2 * share), bf16), ((tokens, 128), f32)),
        (expert_in, expert_gain.reshape(1, -1), group_router, expert_router, routes),
        place,
        [((tokens, width), bf16)],
    )
    send = lax.ppermute(send, ("c", "tp"), CROSS)
    arrived = traded(send, ZY)

    far_gate = lax.ppermute(gate, "tp", FAR)
    far_up = lax.ppermute(up, "tp", FAR)
    w_own, w_near, w_far, w_across = run(
        cut_kernel, (((units, 2 * share), bf16),) * 4, (down,), place
    )
    w_near = lax.ppermute(w_near, "tp", NEAR)
    w_far = lax.ppermute(w_far, "tp", FAR)
    w_across = lax.ppermute(w_across, "tp", ACROSS)

    row_count = mixer_in.shape[0]
    local = query_weight.shape[1]
    log_forget = jax.nn.log_sigmoid(forget_gate).reshape(8, 128)
    inputs = input_gate.reshape(8, 128)
    q, k, v, memories, spread = run(
        mixer_head_kernel,
        (((row_count, local), bf16),) * 3 + (((8 * 128, 128), f32), ((8 * LINES, 128), f32)),
        (mixer_in, mixer_gain.reshape(1, -1), query_weight, key_weight, value_weight, log_forget, inputs),
        None,
        [((row_count, width), bf16)],
    )
    members = traded(spread, YC)
    spread, before = run(
        fold_slab_kernel, (((8 * LINES, 128), f32), ((2 * LINES, 128), f32)), (members,), place
    )
    slabs = traded(spread, "z")
    mine, theirs = run(fold_all_kernel, (((LINES, 128), f32),) * 2, (slabs, before), place)
    theirs = lax.ppermute(theirs, "c", SWAP)
    count = row_count // 4
    own, near, far, across_near, across_far = run(
        mixer_tail_kernel,
        (((count, width), bf16),) * 3 + (((count // 2, width), bf16),) * 2,
        (q, k, v, log_forget, inputs, memories, mine, theirs, head_gain.reshape(1, -1), mixer_out_weight),
        place,
        [((row_count, local), bf16)],
    )
    from_near = lax.ppermute(across_near, "tp", NEAR)
    from_far = lax.ppermute(across_far, "tp", FAR)
    to_near, to_far = run(
        relay_kernel, (((count, width), bf16),) * 2, (near, far, from_near, from_far)
    )
    near = lax.ppermute(to_near, "tp", NEAR)
    far = lax.ppermute(to_far, "tp", FAR)
    mixer_out = run(sum_kernel, (((count, width), bf16),), (own, near, far))

    other_rows = lax.ppermute(arrived, "tp", NEAR)
    hidden = run(
        hidden_kernel,
        (((slots, 2 * units), bf16),),
        (arrived, other_rows, gate, up, far_gate, far_up),
        place,
    )
    other_hidden = lax.ppermute(hidden, "tp", NEAR)
    result = run(
        down_kernel,
        (((slots, 2 * share), bf16),),
        (hidden, other_hidden, w_own, w_far, w_near, w_across),
    )
    back = traded(result, ZY)
    back = lax.ppermute(back, ("c", "tp"), CROSS)
    keep, give = run(
        combine_kernel, (((tokens, share), f32), ((tokens, share), bf16)), (notes, back)
    )
    received = lax.ppermute(give, "tp", FAR)
    expert_out = run(last_kernel, (((tokens, share), bf16),), (keep, received))
    return (mixer_out, expert_out)


def solution(mesh):
    split = Mesh(mesh.devices.reshape(8, 4, 2, mesh.shape["tp"]), EP_TP)
    placed = (
        P(EP, None),
        P(),
        P(None, "tp"),
        P(None, "tp"),
        P(None, "tp"),
        P("tp", EP),
        P("tp", EP),
        P(),
        P("tp", None),
        P(EP, None),
        P(),
        P(),
        P(),
        P(EP, None),
        P(EP, None, "tp"),
        P(EP, None, "tp"),
        P(EP, "tp", None),
    )

    return jax.shard_map(
        shards,
        mesh=split,
        in_specs=placed,
        out_specs=(P(EP_TP, None), P(EP, "tp")),
        check_vma=False,
    )
```

time: 277 us -> 210 us (0.76)
  blocking collectives: 59.3 us -> 0 us
  starting transfers between devices: 25.3 us -> 67.7 us
  matrix products: 28.8 us -> 0 us
  Pallas kernels: 0 us -> 25.2 us
  other arithmetic: 24.5 us -> 0.1 us
  local copies, waits for them, and re-layouts: 34.3 us -> 18.1 us
  between operations: 16.5 us -> 0.9 us
  waiting for transfers between devices: 87.1 us -> 96.2 us
    all_to_all x1 -> x0, blocking collectives: 41.8 us -> none  [sum_at_owner(): parts = lax.all_to_all(split_up(x, dim, length), axis, 0, 0, tiled=True)]
    ppermute x0 -> x15, waiting for transfers between devices: none -> 41 us  [the longest x1 14.8 us: shards(): far_up = lax.ppermute(up, 'tp', FAR)]
    ppermute x0 -> x15, starting transfers between devices: none -> 33.7 us  [the longest x1 6.98 us: shards(): from_far = lax.ppermute(across_far, 'tp', FAR)]
    all_to_all x2 -> x4, waiting for transfers between devices: 87 us -> 55.2 us  [traded(): return lax.all_to_all(x, axis, 0, 0, tiled=True)]
    dot_general x11 -> x0, matrix products: 28.8 us -> none  [the longest x1 9.1 us: shards(): jnp.einsum('scf,fo->sco', hidden, down_weight, preferred_element_type=jnp...]
    pallas_call x0 -> x12, Pallas kernels: none -> 25.2 us  [run(): pl.pallas_call(kernel, out_shape=outs, in_specs=specs, out_specs=tuple([p...]
    gather x13 -> x0, local copies, waits for them, and re-layouts: 18.2 us -> none  [the longest x1 5.98 us: shards(): padded[owner // 2].reshape(expert_total, capacity, normed_b.shape[1])]
    all_gather x2 -> x0, blocking collectives: 17.5 us -> none  [collected_together(): both, at, found = (lax.all_gather(jnp.concatenate(lines), axis), 0, {})]
  transfers between devices with their start and end apart: 4 -> 19, of which waited for: 2 -> 11; matrix products, arithmetic and copies ran while one was open for 24% -> 0% of each run, Pallas kernels for 0% -> 11%
where the time goes in v1:
time: 210 us; the launch traced here: 208 us
  waiting for transfers between devices  96.2 us (46%)
  starting transfers between devices  67.7 us (32%)
  Pallas kernels  25.2 us (12%)
  local copies, waits for them, and re-layouts  18.1 us (9%)
    all_to_all x4, waiting for transfers between devices, traded(): return lax.all_to_all(x, axis, 0, 0, tiled=True)  55.2 us
    all_to_all x4, starting transfers between devices, traded(): return lax.all_to_all(x, axis, 0, 0, tiled=True)  34 us
    pallas_call x12, Pallas kernels, run(): pl.pallas_call(kernel, out_shape=outs, in_specs=specs, out_specs=tuple([p...  25.2 us
    unnamed x59, local copies, waits for them, and re-layouts  18 us
    ppermute x1, waiting for transfers between devices, shards(): far_up = lax.ppermute(up, 'tp', FAR)  14.8 us
    ppermute x1, waiting for transfers between devices, shards(): near = lax.ppermute(to_near, 'tp', NEAR)  8.27 us
    ppermute x1, starting transfers between devices, shards(): from_far = lax.ppermute(across_far, 'tp', FAR)  6.98 us
    ppermute x1, starting transfers between devices, shards(): far_gate = lax.ppermute(gate, 'tp', FAR)  6.67 us
  transfers between devices with their start and end apart: 19, of which 11 were waited for; matrix products, arithmetic and copies ran while one was open for 0% of the time, Pallas kernels for 11%

profile of v1, /device:TPU:1, one launch (start us, length us, event | category | flops | bytes accessed | tf_op | source)
XLA Modules:
  0.0 208.1 jit_solution(11109266879862021854)
XLA Ops:
  1.9 1.2 copy.20.expert_router
  4.7 2.3 %shard_map.182 = (bf16[512,1024]{1,0:T(8,128)(2,1)S(1)}, f32[256,128]{1,0:T(8,128)S(1)}) custom-call(s32[4]{0:T(128)S(1)} %pad_add_fusion.place, bf16[256,2048]{1,0:T(8,128)(2,1)S(1)} %copy-done.3, f32[1,2048]{1,0:T(1,128)S(1)} %bitcast.28, bf16[2048,16]{1,0:T(8,128)(2,1)S(1)} %copy.19.group_router, bf16[2048,64]{1,0:T(8,128)(2,1)S(1)} %copy.20.expert_router, ...), custom_call_target="tpu_custom_call" | custom-call | tf_op jit(solution)/shard_map/pallas_call | solution.py:299
  9.6 12.0 %all-to-all-start.2 = ((bf16[32,16,1024]{2,1,0:T(8,128)(2,1)}), bf16[32,16,1024]{2,1,0:T(8,128)(2,1)S(1)}, u32[]{:S(2)}, u32[]{:S(2)}) async-start(bf16[32,16,1024]{2,1,0:T(8,128)(2,1)} %bitcast.31), calls=%async_computation.2 | async-start | bytes 2097152 | tf_op jit(solution)/shard_map/all_to_all | solution.py:311
  21.6 6.7 %collective-permute-start.7 = (bf16[2048,256]{1,0:T(8,128)(2,1)S(1)}, bf16[2048,256]{1,0:T(8,128)(2,1)}, u32[]{:S(2)}, u32[]{:S(2)}) collective-permute-start(bf16[2048,256]{1,0:T(8,128)(2,1)S(1)} %bitcast.23), channel_id=1, source_target_pairs={{0,3},{1,2},{2,1},{3,0},{4,7},{5,6},{6,5},{7,4},{8,11},{9,10},{10,... | collective-permute-start | bytes 3145736 | tf_op jit(solution)/shard_map/ppermute | solution.py:349
  28.4 19.4 %all-to-all-done.2 = bf16[32,16,1024]{2,1,0:T(8,128)(2,1)S(1)} async-done(((bf16[32,16,1024]{2,1,0:T(8,128)(2,1)}), bf16[32,16,1024]{2,1,0:T(8,128)(2,1)S(1)}, u32[]{:S(2)}, u32[]{:S(2)}) %all-to-all-start.2) | async-done | bytes 1048608 | tf_op jit(solution)/shard_map/all_to_all | solution.py:311
  49.0 1.8 shard_map.184
  51.6 6.1 %collective-permute-start.10 = (bf16[256,1024]{1,0:T(8,128)(2,1)}, bf16[256,1024]{1,0:T(8,128)(2,1)}, u32[]{:S(2)}, u32[]{:S(2)}) collective-permute-start(bf16[256,1024]{1,0:T(8,128)(2,1)} %get-tuple-element.45), channel_id=1, source_target_pairs={{0,3},{1,2},{2,1},{3,0},{4,7},{5,6},{6,5},{7,4},{8,11},{9,10},{10,... | collective-permute-start | bytes 1572872 | tf_op jit(solution)/shard_map/ppermute | solution.py:355
  58.9 14.8 %collective-permute-done.8.far_up = bf16[2048,256]{1,0:T(8,128)(2,1)} collective-permute-done((bf16[2048,256]{1,0:T(8,128)(2,1)}, bf16[2048,256]{1,0:T(8,128)(2,1)}, u32[]{:S(2)}, u32[]{:S(2)}) %collective-permute-start.8) | collective-permute-done | bytes 1048608 | tf_op jit(solution)/shard_map/ppermute | solution.py:350
  73.8 1.2 copy-done.7
  75.0 1.2 copy-done.8
  76.2 3.9 %shard_map.183.own = bf16[512,512]{1,0:T(8,128)(2,1)S(1)} custom-call(s32[4]{0:T(128)S(1)} %pad_add_fusion.place, bf16[512,1024]{1,0:T(8,128)(2,1)S(1)} %bitcast.19, bf16[512,1024]{1,0:T(8,128)(2,1)S(1)} %collective-permute-done.6.other, bf16[2048,256]{1,0:T(8,128)(2,1)S(1)} %bitcast.24, bf16[2048,256]{1,0:T(8,128)(2,1)S(1)} %bitcast.26, ...), custom_call_target="tpu_custom_call" | custom-call | tf_op jit(solution)/shard_map/pallas_call | solution.py:299
  80.3 1.2 copy-done.1
  81.6 1.2 copy-done.2
  82.8 4.6 %shard_map.176 = (bf16[512,256]{1,0:T(8,128)(2,1)S(1)}, bf16[512,256]{1,0:T(8,128)(2,1)S(1)}, bf16[512,256]{1,0:T(8,128)(2,1)S(1)}, f32[1024,128]{1,0:T(8,128)S(1)}, f32[1088,128]{1,0:T(8,128)S(1)}) custom-call(bf16[512,2048]{1,0:T(8,128)(2,1)} %rows.2, f32[1,2048]{1,0:T(1,128)S(1)} %bitcast.29, bf16[2048,256]{1,0:T(8,128)(2,1)S(1)} %copy-done, ...), custom_call_target="tpu_custom_call" | custom-call | tf_op jit(solution)/shard_map/pallas_call | solution.py:299
  89.6 8.9 %all-to-all-start = ((f32[8,136,128]{2,1,0:T(8,128)}), f32[8,136,128]{2,1,0:T(8,128)S(1)}, u32[]{:S(2)}, u32[]{:S(2)}) async-start(f32[8,136,128]{2,1,0:T(8,128)} %bitcast.27), calls=%async_computation | async-start | bytes 1114112 | tf_op jit(solution)/shard_map/all_to_all | solution.py:311
  98.9 4.6 %collective-permute-done.9.other = bf16[512,512]{1,0:T(8,128)(2,1)} collective-permute-done((bf16[512,512]{1,0:T(8,128)(2,1)S(1)}, bf16[512,512]{1,0:T(8,128)(2,1)}, u32[]{:S(2)}, u32[]{:S(2)}) %collective-permute-start.9) | collective-permute-done | bytes 524320 | tf_op jit(solution)/shard_map/ppermute | solution.py:400
  104.6 3.7 %shard_map.185 = bf16[512,1024]{1,0:T(8,128)(2,1)} custom-call(bf16[512,512]{1,0:T(8,128)(2,1)S(1)} %shard_map.183.own, bf16[512,512]{1,0:T(8,128)(2,1)} %collective-permute-done.9.other, bf16[256,1024]{1,0:T(8,128)(2,1)S(1)} %copy-done.13, bf16[256,1024]{1,0:T(8,128)(2,1)} %collective-permute-done.10.w_far, ...), custom_call_target="tpu_custom_call" | custom-call | tf_op jit(solution)/shard_map/pallas_call | solution.py:299
  108.4 8.4 %all-to-all-start.3 = ((bf16[32,16,1024]{2,1,0:T(8,128)(2,1)}), bf16[32,16,1024]{2,1,0:T(8,128)(2,1)}, u32[]{:S(2)}, u32[]{:S(2)}) async-start(bf16[32,16,1024]{2,1,0:T(8,128)(2,1)} %bitcast.16), calls=%async_computation.3 | async-start | bytes 2097152 | tf_op jit(solution)/shard_map/all_to_all | solution.py:311
  116.8 1.4 shard_map.177
  118.8 22.6 %all-to-all-done.3 = bf16[32,16,1024]{2,1,0:T(8,128)(2,1)} async-done(((bf16[32,16,1024]{2,1,0:T(8,128)(2,1)}), bf16[32,16,1024]{2,1,0:T(8,128)(2,1)}, u32[]{:S(2)}, u32[]{:S(2)}) %all-to-all-start.3) | async-done | bytes 1048608 | tf_op jit(solution)/shard_map/all_to_all | solution.py:311
  141.5 4.7 %all-to-all-start.1 = ((f32[8,136,128]{2,1,0:T(8,128)}), f32[8,136,128]{2,1,0:T(8,128)S(1)}, u32[]{:S(2)}, u32[]{:S(2)}) async-start(f32[8,136,128]{2,1,0:T(8,128)} %bitcast.7), calls=%async_computation.1 | async-start | bytes 1114112 | tf_op jit(solution)/shard_map/all_to_all | solution.py:311
  146.1 1.9 collective-permute-start.13
  148.0 13.2 %all-to-all-done.1 = f32[8,136,128]{2,1,0:T(8,128)S(1)} async-done(((f32[8,136,128]{2,1,0:T(8,128)}), f32[8,136,128]{2,1,0:T(8,128)S(1)}, u32[]{:S(2)}, u32[]{:S(2)}) %all-to-all-start.1) | async-done | bytes 557088 | tf_op jit(solution)/shard_map/all_to_all | solution.py:311
  162.7 4.2 %collective-permute-start = (f32[136,128]{1,0:T(8,128)S(1)}, f32[136,128]{1,0:T(8,128)S(1)}, u32[]{:S(2)}, u32[]{:S(2)}) collective-permute-start(f32[136,128]{1,0:T(8,128)S(1)} %get-tuple-element.34), channel_id=1, source_target_pairs={{0,4},{4,0},{1,5},{5,1},{2,6},{6,2},{3,7},{7,3},{8,12},{12,8},{9,1... | collective-permute-start | bytes 208904 | tf_op jit(solution)/shard_map/ppermute | solution.py:375
  169.7 4.0 %shard_map.179 = (bf16[128,2048]{1,0:T(8,128)(2,1)S(1)}, bf16[128,2048]{1,0:T(8,128)(2,1)S(1)}, bf16[128,2048]{1,0:T(8,128)(2,1)S(1)}, bf16[64,2048]{1,0:T(8,128)(2,1)S(1)}, bf16[64,2048]{1,0:T(8,128)(2,1)S(1)}) custom-call(s32[4]{0:T(128)S(1)} %pad_add_fusion.place, bf16[512,256]{1,0:T(8,128)(2,1)S(1)} %get-tuple-element.26.q, ...), custom_call_target="tpu_custom_call" | custom-call | tf_op jit(solution)/shard_map/pallas_call | solution.py:299
  173.7 1.3 collective-permute-start.1
  175.0 7.0 %collective-permute-start.2 = (bf16[64,2048]{1,0:T(8,128)(2,1)S(1)}, bf16[64,2048]{1,0:T(8,128)(2,1)S(1)}, u32[]{:S(2)}, u32[]{:S(2)}) collective-permute-start(bf16[64,2048]{1,0:T(8,128)(2,1)S(1)} %get-tuple-element.39), channel_id=1, source_target_pairs={{0,3},{1,2},{2,1},{3,0},{4,7},{5,6},{6,5},{7,4},{8,11},{9,10},{10,... | collective-permute-start | bytes 786440 | tf_op jit(solution)/shard_map/ppermute | solution.py:385
  182.0 6.0 %collective-permute-done.2.from_far = bf16[64,2048]{1,0:T(8,128)(2,1)S(1)} collective-permute-done((bf16[64,2048]{1,0:T(8,128)(2,1)S(1)}, bf16[64,2048]{1,0:T(8,128)(2,1)S(1)}, u32[]{:S(2)}, u32[]{:S(2)}) %collective-permute-start.2) | collective-permute-done | bytes 262176 | tf_op jit(solution)/shard_map/ppermute | solution.py:385
  188.6 2.2 %collective-permute-start.4 = (bf16[128,2048]{1,0:T(8,128)(2,1)S(1)}, bf16[128,2048]{1,0:T(8,128)(2,1)S(1)}, u32[]{:S(2)}, u32[]{:S(2)}) collective-permute-start(bf16[128,2048]{1,0:T(8,128)(2,1)S(1)} %get-tuple-element.41), channel_id=1, source_target_pairs={{0,3},{1,2},{2,1},{3,0},{4,7},{5,6},{6,5},{7,4},{8,11},{9,10},{10,... | collective-permute-start | bytes 1572872 | tf_op jit(solution)/shard_map/ppermute | solution.py:390
  192.2 8.3 %collective-permute-done.3.near = bf16[128,2048]{1,0:T(8,128)(2,1)S(1)} collective-permute-done((bf16[128,2048]{1,0:T(8,128)(2,1)S(1)}, bf16[128,2048]{1,0:T(8,128)(2,1)S(1)}, u32[]{:S(2)}, u32[]{:S(2)}) %collective-permute-start.3) | collective-permute-done | bytes 524320 | tf_op jit(solution)/shard_map/ppermute | solution.py:389
  200.5 1.2 collective-permute-done.4.far
  202.8 4.6 %collective-permute-done.14.received = bf16[256,512]{1,0:T(8,128)(2,1)S(1)} collective-permute-done((bf16[256,512]{1,0:T(8,128)(2,1)S(1)}, bf16[256,512]{1,0:T(8,128)(2,1)S(1)}, u32[]{:S(2)}, u32[]{:S(2)}) %collective-permute-start.14) | collective-permute-done | bytes 262176 | tf_op jit(solution)/shard_map/ppermute | solution.py:411
  (81 shorter events, 21.2 us)
Async XLA Ops:
  0.6 3.4 %copy-start.3 = (bf16[256,2048]{1,0:T(8,128)(2,1)S(1)}, bf16[256,2048]{1,0:T(8,128)(2,1)}, u32[]{:S(2)}) copy-start(bf16[256,2048]{1,0:T(8,128)(2,1)} %rows.3) | copy-start | bytes 3145732
  4.7 44.3 %copy-start.4 = (bf16[1,256,2048]{2,1,0:T(8,128)(2,1)S(1)}, bf16[1,256,2048]{2,1,0:T(8,128)(2,1)}, u32[]{:S(2)}) copy-start(bf16[1,256,2048]{2,1,0:T(8,128)(2,1)} %param.33) | copy-start | bytes 3145732
  7.7 13.9 %copy-start.6 = (bf16[1,2048,256]{2,1,0:T(8,128)(2,1)S(1)}, bf16[1,2048,256]{2,1,0:T(8,128)(2,1)}, u32[]{:S(2)}) copy-start(bf16[1,2048,256]{2,1,0:T(8,128)(2,1)} %param.31) | copy-start | bytes 3145732
  7.7 0.9 collective-permute-start.5
  9.6 38.2 %all-to-all-start.2 = ((bf16[32,16,1024]{2,1,0:T(8,128)(2,1)}), bf16[32,16,1024]{2,1,0:T(8,128)(2,1)S(1)}, u32[]{:S(2)}, u32[]{:S(2)}) async-start(bf16[32,16,1024]{2,1,0:T(8,128)(2,1)} %bitcast.31), calls=%async_computation.2 | async-start | bytes 2097152 | tf_op jit(solution)/shard_map/all_to_all | solution.py:311
  21.6 36.4 %collective-permute-start.7 = (bf16[2048,256]{1,0:T(8,128)(2,1)S(1)}, bf16[2048,256]{1,0:T(8,128)(2,1)}, u32[]{:S(2)}, u32[]{:S(2)}) collective-permute-start(bf16[2048,256]{1,0:T(8,128)(2,1)S(1)} %bitcast.23), channel_id=1, source_target_pairs={{0,3},{1,2},{2,1},{3,0},{4,7},{5,6},{6,5},{7,4},{8,11},{9,10},{10,... | collective-permute-start | bytes 3145736 | tf_op jit(solution)/shard_map/ppermute | solution.py:349
  28.3 45.5 %collective-permute-start.8 = (bf16[2048,256]{1,0:T(8,128)(2,1)}, bf16[2048,256]{1,0:T(8,128)(2,1)}, u32[]{:S(2)}, u32[]{:S(2)}) collective-permute-start(bf16[2048,256]{1,0:T(8,128)(2,1)} %bitcast.25), channel_id=1, source_target_pairs={{0,3},{1,2},{2,1},{3,0},{4,7},{5,6},{6,5},{7,4},{8,11},{9,10},{10,... | collective-permute-start | bytes 3145736 | tf_op jit(solution)/shard_map/ppermute | solution.py:350
  47.8 26.0 %collective-permute-start.6 = (bf16[512,1024]{1,0:T(8,128)(2,1)S(1)}, bf16[512,1024]{1,0:T(8,128)(2,1)S(1)}, u32[]{:S(2)}, u32[]{:S(2)}) collective-permute-start(bf16[512,1024]{1,0:T(8,128)(2,1)S(1)} %bitcast.18), channel_id=1, source_target_pairs={{0,1},{1,0},{2,3},{3,2},{4,5},{5,4},{6,7},{7,6},{8,9},{9,8},{10,11... | collective-permute-start | bytes 3145736 | tf_op jit(solution)/shard_map/ppermute | solution.py:393
  51.6 46.9 %collective-permute-start.10 = (bf16[256,1024]{1,0:T(8,128)(2,1)}, bf16[256,1024]{1,0:T(8,128)(2,1)}, u32[]{:S(2)}, u32[]{:S(2)}) collective-permute-start(bf16[256,1024]{1,0:T(8,128)(2,1)} %get-tuple-element.45), channel_id=1, source_target_pairs={{0,3},{1,2},{2,1},{3,0},{4,7},{5,6},{6,5},{7,4},{8,11},{9,10},{10,... | collective-permute-start | bytes 1572872 | tf_op jit(solution)/shard_map/ppermute | solution.py:355
  57.7 40.8 %collective-permute-start.11 = (bf16[256,1024]{1,0:T(8,128)(2,1)}, bf16[256,1024]{1,0:T(8,128)(2,1)}, u32[]{:S(2)}, u32[]{:S(2)}) collective-permute-start(bf16[256,1024]{1,0:T(8,128)(2,1)} %get-tuple-element.46), channel_id=1, source_target_pairs={{0,1},{1,0},{2,3},{3,2},{4,5},{5,4},{6,7},{7,6},{8,9},{9,8},{10,11... | collective-permute-start | bytes 1572872 | tf_op jit(solution)/shard_map/ppermute | solution.py:354
  58.1 22.3 %copy-start = (bf16[2048,256]{1,0:T(8,128)(2,1)S(1)}, bf16[2048,256]{1,0:T(8,128)(2,1)}, u32[]{:S(2)}) copy-start(bf16[2048,256]{1,0:T(8,128)(2,1)} %wq.1) | copy-start | bytes 3145732
  58.1 40.9 %collective-permute-start.12 = (bf16[256,1024]{1,0:T(8,128)(2,1)}, bf16[256,1024]{1,0:T(8,128)(2,1)}, u32[]{:S(2)}, u32[]{:S(2)}) collective-permute-start(bf16[256,1024]{1,0:T(8,128)(2,1)} %get-tuple-element.47), channel_id=1, source_target_pairs={{0,2},{1,3},{2,0},{3,1},{4,6},{5,7},{6,4},{7,5},{8,10},{9,11},{10,... | collective-permute-start | bytes 1572872 | tf_op jit(solution)/shard_map/ppermute | solution.py:356
  76.2 4.0 %copy-start.26 = (f32[2,512]{1,0:T(2,128)S(1)}, f32[2,512]{1,0:T(2,128)}, u32[]{:S(2)}) copy-start(f32[2,512]{1,0:T(2,128)} %param.23) | copy-start | bytes 12292
  76.2 4.1 %copy-start.27 = (f32[2,512]{1,0:T(2,128)S(1)}, f32[2,512]{1,0:T(2,128)}, u32[]{:S(2)}) copy-start(f32[2,512]{1,0:T(2,128)} %param.22) | copy-start | bytes 12292
  76.2 4.1 %copy-start.23 = (f32[2048]{0:T(1024)S(1)}, f32[2048]{0:T(1024)}, u32[]{:S(2)}) copy-start(f32[2048]{0:T(1024)} %param.18) | copy-start | bytes 24580
  80.1 23.4 %collective-permute-start.9 = (bf16[512,512]{1,0:T(8,128)(2,1)S(1)}, bf16[512,512]{1,0:T(8,128)(2,1)}, u32[]{:S(2)}, u32[]{:S(2)}) collective-permute-start(bf16[512,512]{1,0:T(8,128)(2,1)S(1)} %shard_map.183.own), channel_id=1, source_target_pairs={{0,1},{1,0},{2,3},{3,2},{4,5},{5,4},{6,7},{7,6},{8,9},{9,8},{10,11... | collective-permute-start | bytes 1572872 | tf_op jit(solution)/shard_map/ppermute | solution.py:400
  80.3 1.2 copy-start.1
  89.6 14.0 %copy-start.10 = (f32[1024,128]{1,0:T(8,128)}, f32[1024,128]{1,0:T(8,128)S(1)}, u32[]{:S(2)}) copy-start(f32[1024,128]{1,0:T(8,128)S(1)} %get-tuple-element.29.memories) | copy-start | bytes 1572868
  89.6 18.8 %all-to-all-start = ((f32[8,136,128]{2,1,0:T(8,128)}), f32[8,136,128]{2,1,0:T(8,128)S(1)}, u32[]{:S(2)}, u32[]{:S(2)}) async-start(f32[8,136,128]{2,1,0:T(8,128)} %bitcast.27), calls=%async_computation | async-start | bytes 1114112 | tf_op jit(solution)/shard_map/all_to_all | solution.py:311
  108.3 59.5 %copy-start.5 = (bf16[256,2048]{1,0:T(8,128)(2,1)S(1)}, bf16[256,2048]{1,0:T(8,128)(2,1)}, u32[]{:S(2)}) copy-start(bf16[256,2048]{1,0:T(8,128)(2,1)} %weight.1) | copy-start | bytes 3145732
  108.4 59.5 %copy-start.11 = (f32[1024,128]{1,0:T(8,128)S(1)}, f32[1024,128]{1,0:T(8,128)}, u32[]{:S(2)}) copy-start(f32[1024,128]{1,0:T(8,128)} %copy-done.10) | copy-start | bytes 1572868
  108.4 59.5 %copy-start.24 = (f32[1024]{0:T(1024)S(1)}, f32[1024]{0:T(1024)}, u32[]{:S(2)}) copy-start(f32[1024]{0:T(1024)} %param.24) | copy-start | bytes 12292
  108.4 33.1 %all-to-all-start.3 = ((bf16[32,16,1024]{2,1,0:T(8,128)(2,1)}), bf16[32,16,1024]{2,1,0:T(8,128)(2,1)}, u32[]{:S(2)}, u32[]{:S(2)}) async-start(bf16[32,16,1024]{2,1,0:T(8,128)(2,1)} %bitcast.16), calls=%async_computation.3 | async-start | bytes 2097152 | tf_op jit(solution)/shard_map/all_to_all | solution.py:311
  141.5 19.7 %all-to-all-start.1 = ((f32[8,136,128]{2,1,0:T(8,128)}), f32[8,136,128]{2,1,0:T(8,128)S(1)}, u32[]{:S(2)}, u32[]{:S(2)}) async-start(f32[8,136,128]{2,1,0:T(8,128)} %bitcast.7), calls=%async_computation.1 | async-start | bytes 1114112 | tf_op jit(solution)/shard_map/all_to_all | solution.py:311
  146.1 44.6 %collective-permute-start.13 = (bf16[512,1024]{1,0:T(8,128)(2,1)}, bf16[512,1024]{1,0:T(8,128)(2,1)S(1)}, u32[]{:S(2)}, u32[]{:S(2)}) collective-permute-start(bf16[512,1024]{1,0:T(8,128)(2,1)} %bitcast.17), channel_id=1, source_target_pairs={{0,0},{1,1},{2,6},{3,7},{4,4},{5,5},{6,2},{7,3},{8,8},{9,9},{10,14... | collective-permute-start | bytes 3145736 | tf_op jit(solution)/shard_map/ppermute | solution.py:407
  162.0 28.7 %copy-start.21 = (f32[256,128]{1,0:T(8,128)S(1)}, f32[256,128]{1,0:T(8,128)}, u32[]{:S(2)}) copy-start(f32[256,128]{1,0:T(8,128)} %copy-done.20) | copy-start | bytes 393220
  162.7 5.1 %collective-permute-start = (f32[136,128]{1,0:T(8,128)S(1)}, f32[136,128]{1,0:T(8,128)S(1)}, u32[]{:S(2)}, u32[]{:S(2)}) collective-permute-start(f32[136,128]{1,0:T(8,128)S(1)} %get-tuple-element.34), channel_id=1, source_target_pairs={{0,4},{4,0},{1,5},{5,1},{2,6},{6,2},{3,7},{7,3},{8,12},{12,8},{9,1... | collective-permute-start | bytes 208904 | tf_op jit(solution)/shard_map/ppermute | solution.py:375
  173.7 8.3 %collective-permute-start.1 = (bf16[64,2048]{1,0:T(8,128)(2,1)S(1)}, bf16[64,2048]{1,0:T(8,128)(2,1)S(1)}, u32[]{:S(2)}, u32[]{:S(2)}) collective-permute-start(bf16[64,2048]{1,0:T(8,128)(2,1)S(1)} %get-tuple-element.38), channel_id=1, source_target_pairs={{0,1},{1,0},{2,3},{3,2},{4,5},{5,4},{6,7},{7,6},{8,9},{9,8},{10,11... | collective-permute-start | bytes 786440 | tf_op jit(solution)/shard_map/ppermute | solution.py:384
  175.0 13.0 %collective-permute-start.2 = (bf16[64,2048]{1,0:T(8,128)(2,1)S(1)}, bf16[64,2048]{1,0:T(8,128)(2,1)S(1)}, u32[]{:S(2)}, u32[]{:S(2)}) collective-permute-start(bf16[64,2048]{1,0:T(8,128)(2,1)S(1)} %get-tuple-element.39), channel_id=1, source_target_pairs={{0,3},{1,2},{2,1},{3,0},{4,7},{5,6},{6,5},{7,4},{8,11},{9,10},{10,... | collective-permute-start | bytes 786440 | tf_op jit(solution)/shard_map/ppermute | solution.py:385
  188.2 12.4 %collective-permute-start.3 = (bf16[128,2048]{1,0:T(8,128)(2,1)S(1)}, bf16[128,2048]{1,0:T(8,128)(2,1)S(1)}, u32[]{:S(2)}, u32[]{:S(2)}) collective-permute-start(bf16[128,2048]{1,0:T(8,128)(2,1)S(1)} %get-tuple-element.40), channel_id=1, source_target_pairs={{0,1},{1,0},{2,3},{3,2},{4,5},{5,4},{6,7},{7,6},{8,9},{9,8},{10,11... | collective-permute-start | bytes 1572872 | tf_op jit(solution)/shard_map/ppermute | solution.py:389
  188.6 13.2 %collective-permute-start.4 = (bf16[128,2048]{1,0:T(8,128)(2,1)S(1)}, bf16[128,2048]{1,0:T(8,128)(2,1)S(1)}, u32[]{:S(2)}, u32[]{:S(2)}) collective-permute-start(bf16[128,2048]{1,0:T(8,128)(2,1)S(1)} %get-tuple-element.41), channel_id=1, source_target_pairs={{0,3},{1,2},{2,1},{3,0},{4,7},{5,6},{6,5},{7,4},{8,11},{9,10},{10,... | collective-permute-start | bytes 1572872 | tf_op jit(solution)/shard_map/ppermute | solution.py:390
  191.7 15.7 %collective-permute-start.14 = (bf16[256,512]{1,0:T(8,128)(2,1)S(1)}, bf16[256,512]{1,0:T(8,128)(2,1)S(1)}, u32[]{:S(2)}, u32[]{:S(2)}) collective-permute-start(bf16[256,512]{1,0:T(8,128)(2,1)S(1)} %get-tuple-element.49), channel_id=1, source_target_pairs={{0,3},{1,2},{2,1},{3,0},{4,7},{5,6},{6,5},{7,4},{8,11},{9,10},{10,... | collective-permute-start | bytes 786440 | tf_op jit(solution)/shard_map/ppermute | solution.py:411
  (15 other events, 13.6 us)

commit v2 on v1

--- a/solution.py
+++ b/solution.py
@@ -16,6 +16,7 @@
 SWAP = [(0, 1), (1, 0)]
 CROSS = [(c * 4 + t, (c if t < 2 else 1 - c) * 4 + t) for c in range(2) for t in range(4)]
 LINES = 136
+CHUNKS = 2
 f32 = jnp.float32
 bf16 = jnp.bfloat16
 
@@ -194,81 +195,116 @@
             ]
 
 
-def dispatch_kernel(place, rows, gain, group_router, expert_router, routes, send, notes, normed):
+def dispatch_kernel(place, rows, gain, group_router, expert_router, routes, *rest):
+    sends, (notes, normed) = rest[:CHUNKS], rest[CHUNKS:]
     rank, core = place[0], place[1]
     normed[...] = (normalized(rows[...].astype(f32)) * gain[...]).astype(bf16)
-    group_logits = jnp.dot(normed[...], group_router[...], preferred_element_type=f32)
-    expert_logits = jnp.dot(normed[...], expert_router[...], preferred_element_type=f32)
-    tokens, experts = expert_logits.shape
-    groups = group_logits.shape[1]
-    expert_ids = lax.broadcasted_iota(jnp.int32, (tokens, experts), 1)
-    group_ids = lax.broadcasted_iota(jnp.int32, (tokens, groups), 1)
-    table = routes[...]
-    named = [table[:, k : k + 1] for k in range(2)]
+
+    def logits(weights):
+        return lax.dot_general(
+            weights[...], normed[...], (((1,), (1,)), ((), ())), preferred_element_type=f32
+        )
+
+    group_logits, expert_logits = logits(group_router), logits(expert_router)
+    experts, tokens = expert_logits.shape
+    groups = group_logits.shape[0]
+    expert_ids = lax.broadcasted_iota(jnp.int32, (experts, tokens), 0)
+    group_ids = lax.broadcasted_iota(jnp.int32, (groups, tokens), 0)
+    named = [routes[k : k + 1, :] for k in range(2)]
     hot = [(expert_ids == e).astype(f32) for e in named]
-    below = (
-        lax.broadcasted_iota(jnp.int32, (tokens, tokens), 1)
-        < lax.broadcasted_iota(jnp.int32, (tokens, tokens), 0)
+    above = (
+        lax.broadcasted_iota(jnp.int32, (tokens, tokens), 0)
+        < lax.broadcasted_iota(jnp.int32, (tokens, tokens), 1)
     ).astype(bf16)
-    counts = [jnp.dot(below, h.astype(bf16), preferred_element_type=f32) for h in hot]
-    counts[1] = counts[1] + jnp.sum(hot[0], axis=0, keepdims=True)
+    counts = [jnp.dot(h.astype(bf16), above, preferred_element_type=f32) for h in hot]
+    counts[1] = counts[1] + jnp.sum(hot[0], axis=1, keepdims=True)
     slots = []
     for k in range(2):
-        at = jnp.sum(hot[k] * counts[k], axis=1, keepdims=True).astype(jnp.int32)
+        at = jnp.sum(hot[k] * counts[k], axis=0, keepdims=True).astype(jnp.int32)
         here = ((named[k] & 1) ^ core) == rank // 2
         slots.append(jnp.where(here, (named[k] >> 1) * 16 + at, -1))
-    chosen = [jnp.sum(h * expert_logits, axis=1, keepdims=True) for h in hot]
+    chosen = [jnp.sum(h * expert_logits, axis=0, keepdims=True) for h in hot]
     grouped = [
-        jnp.sum(jnp.where(group_ids == e // (experts // groups), group_logits, 0.0), axis=1, keepdims=True)
+        jnp.sum(jnp.where(group_ids == e // (experts // groups), group_logits, 0.0), axis=0, keepdims=True)
         for e in named
     ]
     combine = [
         jax.nn.sigmoid(grouped[k]) * jax.nn.sigmoid(chosen[k] - chosen[1 - k]) for k in range(2)
     ]
-    lane = lax.broadcasted_iota(jnp.int32, (tokens, 128), 1)
-    wide = jnp.where(lane == 0, slots[0].astype(f32), slots[1].astype(f32))
-    notes[...] = jnp.where(lane < 2, wide, jnp.where(lane == 2, combine[0], combine[1]))
-    across = wide.T
-    first, second = (across[k : k + 1].astype(jnp.int32) for k in range(2))
     share = rows.shape[1] // 4
-    slot_ids = lax.broadcasted_iota(jnp.int32, (send.shape[0], tokens), 0)
-    pick = ((slot_ids == first) | (slot_ids == second)).astype(bf16)
-    for j, quarter in enumerate((rank, 3 - rank)):
-        features = normed[:, pl.ds(pl.multiple_of(quarter * share, share), share)]
-        send[:, j * share : (j + 1) * share] = jnp.dot(
-            pick, features, preferred_element_type=f32
-        ).astype(bf16)
-
-
-def hidden_kernel(place, own, other, gate, up, far_gate, far_up, out):
-    rank = place[0]
+    count = sends[0].shape[0]
+    each = 16 // CHUNKS
+    slot_ids = lax.broadcasted_iota(jnp.int32, (count, tokens), 0)
+    for n, send in enumerate(sends):
+        ids = (slot_ids // each) * 16 + slot_ids % each + n * each
+        pick = ((ids == slots[0]) | (ids == slots[1])).astype(bf16)
+        for j, quarter in enumerate((rank, 3 - rank)):
+            features = normed[:, pl.ds(pl.multiple_of(quarter * share, share), share)]
+            send[:, j * share : (j + 1) * share] = jnp.dot(
+                pick, features, preferred_element_type=f32
+            ).astype(bf16)
+    row = lax.broadcasted_iota(jnp.int32, (128, tokens), 0)
+    wide = jnp.where(row == 0, slots[0].astype(f32), slots[1].astype(f32))
+    notes[...] = jnp.where(row < 2, wide, jnp.where(row == 2, combine[0], combine[1])).T
+
+
+def hidden_kernel(place, own, other, gate, up, far_gate, far_up, out, sums):
     share = own.shape[1] // 2
     units = gate.shape[1]
-    blocks = [
-        (own, 0, rank),
-        (own, 1, 3 - rank),
-        (other, 0, rank ^ 1),
-        (other, 1, 3 - (rank ^ 1)),
-    ]
-    for part, (g, u) in enumerate(((gate, up), (far_gate, far_up))):
-        gate_act = up_act = None
-        for rows, half, quarter in blocks:
-            features = rows[:, half * share : (half + 1) * share]
-            at = pl.ds(pl.multiple_of(quarter * share, share), share)
-            a = jnp.dot(features, g[at, :], preferred_element_type=f32)
-            b = jnp.dot(features, u[at, :], preferred_element_type=f32)
-            gate_act = a if gate_act is None else gate_act + a
-            up_act = b if up_act is None else up_act + b
-        out[:, part * units : (part + 1) * units] = (jax.nn.silu(gate_act) * up_act).astype(bf16)
-
-
-def down_kernel(own, other, w_own, w_far, w_near, w_across, out):
-    units = own.shape[1] // 2
-    total = jnp.dot(own[:, :units], w_own[...], preferred_element_type=f32)
-    total = total + jnp.dot(own[:, units:], w_far[...], preferred_element_type=f32)
-    total = total + jnp.dot(other[:, :units], w_near[...], preferred_element_type=f32)
-    total = total + jnp.dot(other[:, units:], w_across[...], preferred_element_type=f32)
-    out[...] = total.astype(bf16)
+    step = pl.program_id(0)
+    for n, rows in enumerate((own, own, other, other)):
+
+        @pl.when(step == n)
+        def _():
+            features = rows[:, (n % 2) * share : (n % 2 + 1) * share]
+            for j, weight in enumerate((gate, far_gate, up, far_up)):
+                at = slice(j * units, (j + 1) * units)
+                term = jnp.dot(features, weight[...], preferred_element_type=f32)
+                sums[:, at] = term if n == 0 else sums[:, at] + term
+
+    @pl.when(step == 3)
+    def _():
+        out[...] = (jax.nn.silu(sums[:, : 2 * units]) * sums[:, 2 * units :]).astype(bf16)
+
+
+def hidden_of(place, own, other, weights):
+    share = own.shape[1] // 2
+    units = weights[0].shape[1]
+    rows = pl.BlockSpec(own.shape, lambda n, place: (0, 0))
+
+    def block(n, place):
+        device = place[0] ^ (n // 2)
+        return (jnp.where(n % 2 == 0, device, 3 - device), 0)
+
+    return pl.pallas_call(
+        hidden_kernel,
+        out_shape=jax.ShapeDtypeStruct((own.shape[0], 2 * units), bf16),
+        grid_spec=pltpu.PrefetchScalarGridSpec(
+            num_scalar_prefetch=1,
+            grid=(4,),
+            in_specs=[rows, rows] + [pl.BlockSpec((share, units), block)] * 4,
+            out_specs=pl.BlockSpec((own.shape[0], 2 * units), lambda n, place: (0, 0)),
+            scratch_shapes=[pltpu.VMEM((own.shape[0], 4 * units), f32)],
+        ),
+        compiler_params=pltpu.CompilerParams(
+            vmem_limit_bytes=32 * 1024 * 1024, dimension_semantics=("arbitrary",)
+        ),
+    )(place, own, other, *weights)
+
+
+def down_kernel(*refs):
+    pairs, (w_own, w_far, w_near, w_across, out) = refs[: 2 * CHUNKS], refs[2 * CHUNKS :]
+    each = 16 // CHUNKS
+    for n in range(CHUNKS):
+        own, other = pairs[2 * n : 2 * n + 2]
+        units = own.shape[1] // 2
+        total = jnp.dot(own[:, :units], w_own[...], preferred_element_type=f32)
+        total = total + jnp.dot(own[:, units:], w_far[...], preferred_element_type=f32)
+        total = total + jnp.dot(other[:, :units], w_near[...], preferred_element_type=f32)
+        total = total + jnp.dot(other[:, units:], w_across[...], preferred_element_type=f32)
+        out[:, n * each : (n + 1) * each, :] = total.astype(bf16).reshape(
+            out.shape[0], each, out.shape[2]
+        )
 
 
 def combine_kernel(notes, rows, keep, send):
@@ -336,18 +372,20 @@
     slots = 32 * 16
     gate, up, down = gate_experts[0], up_experts[0], down_experts[0]
     units = gate.shape[1]
-    send, notes = run(
+    far_gate = lax.ppermute(gate, "tp", FAR)
+    far_up = lax.ppermute(up, "tp", FAR)
+    *sends, notes = run(
         dispatch_kernel,
-        (((slots, 2 * share), bf16), ((tokens, 128), f32)),
-        (expert_in, expert_gain.reshape(1, -1), group_router, expert_router, routes),
+        (((slots // CHUNKS, 2 * share), bf16),) * CHUNKS + (((tokens, 128), f32),),
+        (expert_in, expert_gain.reshape(1, -1), group_router.T, expert_router.T, routes.T),
         place,
         [((tokens, width), bf16)],
     )
-    send = lax.ppermute(send, ("c", "tp"), CROSS)
-    arrived = traded(send, ZY)
-
-    far_gate = lax.ppermute(gate, "tp", FAR)
-    far_up = lax.ppermute(up, "tp", FAR)
+    arrived = []
+    for send in sends:
+        send = lax.ppermute(send, ("c", "tp"), CROSS)
+        arrived.append(traded(send, ZY))
+
     w_own, w_near, w_far, w_across = run(
         cut_kernel, (((units, 2 * share), bf16),) * 4, (down,), place
     )
@@ -390,20 +428,15 @@
     far = lax.ppermute(to_far, "tp", FAR)
     mixer_out = run(sum_kernel, (((count, width), bf16),), (own, near, far))
 
-    other_rows = lax.ppermute(arrived, "tp", NEAR)
-    hidden = run(
-        hidden_kernel,
-        (((slots, 2 * units), bf16),),
-        (arrived, other_rows, gate, up, far_gate, far_up),
-        place,
-    )
-    other_hidden = lax.ppermute(hidden, "tp", NEAR)
+    pairs = []
+    for rows in arrived:
+        other_rows = lax.ppermute(rows, "tp", NEAR)
+        hidden = hidden_of(place, rows, other_rows, (gate, up, far_gate, far_up))
+        pairs += [hidden, lax.ppermute(hidden, "tp", NEAR)]
     result = run(
-        down_kernel,
-        (((slots, 2 * share), bf16),),
-        (hidden, other_hidden, w_own, w_far, w_near, w_across),
-    )
-    back = traded(result, ZY)
+        down_kernel, (((32, 16, 2 * share), bf16),), (*pairs, w_own, w_far, w_near, w_across)
+    )
+    back = traded(result.reshape(slots, 2 * share), ZY)
     back = lax.ppermute(back, ("c", "tp"), CROSS)
     keep, give = run(
         combine_kernel, (((tokens, share), f32), ((tokens, share), bf16)), (notes, back)

time: 210 us -> 242 us (1.15)
  waiting for transfers between devices: 96.2 us -> 117 us
  starting transfers between devices: 67.7 us -> 74.7 us
  Pallas kernels: 25.2 us -> 29.8 us
    all_to_all x4 -> x5, starting transfers between devices: 34 us -> 46.2 us  [traded(): return lax.all_to_all(x, axis, 0, 0, tiled=True)]
    pallas_call x0 -> x2, Pallas kernels: none -> 8.4 us  [hidden_of(): pl.pallas_call(hidden_kernel, out_shape=jax.ShapeDtypeStruct((own.shape[0...]
    ppermute x1, waiting for transfers between devices: 14.8 us -> 22.5 us  [shards(): far_up = lax.ppermute(up, 'tp', FAR)]
    ppermute x1, starting transfers between devices: 6.98 us -> 0.01 us  [shards(): from_far = lax.ppermute(across_far, 'tp', FAR)]
    ppermute x1, waiting for transfers between devices: 0.01 us -> 6.21 us  [shards(): from_near = lax.ppermute(across_near, 'tp', NEAR)]
    all_to_all x4 -> x5, waiting for transfers between devices: 55.2 us -> 61.1 us  [traded(): return lax.all_to_all(x, axis, 0, 0, tiled=True)]
    ppermute x1, waiting for transfers between devices: 6.04 us -> 2.21 us  [shards(): from_far = lax.ppermute(across_far, 'tp', FAR)]
    pallas_call x12 -> x11, Pallas kernels: 25.2 us -> 21.4 us  [run(): pl.pallas_call(kernel, out_shape=outs, in_specs=specs, out_specs=tuple([p...]
  transfers between devices with their start and end apart: 19 -> 23, of which waited for: 11 -> 14; matrix products, arithmetic and copies ran while one was open for 0% -> 0% of each run, Pallas kernels for 11% -> 11%
where the time goes in v2:
time: 242 us; the launch traced here: 239 us
  waiting for transfers between devices  117 us (48%)
  starting transfers between devices  74.7 us (31%)
  Pallas kernels  29.8 us (12%)
  local copies, waits for them, and re-layouts  17.1 us (7%)
    all_to_all x5, waiting for transfers between devices, traded(): return lax.all_to_all(x, axis, 0, 0, tiled=True)  61.1 us
    all_to_all x5, starting transfers between devices, traded(): return lax.all_to_all(x, axis, 0, 0, tiled=True)  46.2 us
    ppermute x1, waiting for transfers between devices, shards(): far_up = lax.ppermute(up, 'tp', FAR)  22.5 us
    pallas_call x11, Pallas kernels, run(): pl.pallas_call(kernel, out_shape=outs, in_specs=specs, out_specs=tuple([p...  21.4 us
    unnamed x56, local copies, waits for them, and re-layouts  17 us
    pallas_call x2, Pallas kernels, hidden_of(): pl.pallas_call(hidden_kernel, out_shape=jax.ShapeDtypeStruct((own.shape[0...  8.4 us
    ppermute x1, waiting for transfers between devices, shards(): near = lax.ppermute(to_near, 'tp', NEAR)  8.2 us
    ppermute x2, waiting for transfers between devices, shards(): pairs += [hidden, lax.ppermute(hidden, 'tp', NEAR)]  7.53 us
  transfers between devices with their start and end apart: 23, of which 14 were waited for; matrix products, arithmetic and copies ran while one was open for 0% of the time, Pallas kernels for 11%

profile of v2, /device:TPU:1, one launch (start us, length us, event | category | flops | bytes accessed | tf_op | source)
XLA Modules:
  0.0 239.4 jit_solution(3897167824531614208)
XLA Ops:
  5.3 2.0 shard_map.182
  8.8 12.0 %all-to-all-start.3 = ((bf16[32,8,1024]{2,1,0:T(8,128)(2,1)}), bf16[32,8,1024]{2,1,0:T(8,128)(2,1)S(1)}, u32[]{:S(2)}, u32[]{:S(2)}) async-start(bf16[32,8,1024]{2,1,0:T(8,128)(2,1)} %bitcast.39), calls=%async_computation.3 | async-start | bytes 1048576 | tf_op jit(solution)/shard_map/all_to_all | solution.py:347
  22.3 14.8 %all-to-all-done.3 = bf16[32,8,1024]{2,1,0:T(8,128)(2,1)S(1)} async-done(((bf16[32,8,1024]{2,1,0:T(8,128)(2,1)}), bf16[32,8,1024]{2,1,0:T(8,128)(2,1)S(1)}, u32[]{:S(2)}, u32[]{:S(2)}) %all-to-all-start.3) | async-done | bytes 524320 | tf_op jit(solution)/shard_map/all_to_all | solution.py:347
  37.1 5.4 %all-to-all-start.2 = ((bf16[32,8,1024]{2,1,0:T(8,128)(2,1)}), bf16[32,8,1024]{2,1,0:T(8,128)(2,1)}, u32[]{:S(2)}, u32[]{:S(2)}) async-start(bf16[32,8,1024]{2,1,0:T(8,128)(2,1)} %bitcast.14), calls=%async_computation.2 | async-start | bytes 1048576 | tf_op jit(solution)/shard_map/all_to_all | solution.py:347
  42.5 6.0 %collective-permute-start.7 = (bf16[2048,256]{1,0:T(8,128)(2,1)S(1)}, bf16[2048,256]{1,0:T(8,128)(2,1)S(1)}, u32[]{:S(2)}, u32[]{:S(2)}) collective-permute-start(bf16[2048,256]{1,0:T(8,128)(2,1)S(1)} %bitcast.22), channel_id=1, source_target_pairs={{0,3},{1,2},{2,1},{3,0},{4,7},{5,6},{6,5},{7,4},{8,11},{9,10},{10,... | collective-permute-start | bytes 3145736 | tf_op jit(solution)/shard_map/ppermute | solution.py:375
  48.6 9.1 %all-to-all-done.2 = bf16[32,8,1024]{2,1,0:T(8,128)(2,1)} async-done(((bf16[32,8,1024]{2,1,0:T(8,128)(2,1)}), bf16[32,8,1024]{2,1,0:T(8,128)(2,1)}, u32[]{:S(2)}, u32[]{:S(2)}) %all-to-all-start.2) | async-done | bytes 524320 | tf_op jit(solution)/shard_map/all_to_all | solution.py:347
  60.1 1.8 shard_map.185
  62.8 5.2 %collective-permute-start.13 = (bf16[256,1024]{1,0:T(8,128)(2,1)}, bf16[256,1024]{1,0:T(8,128)(2,1)}, u32[]{:S(2)}, u32[]{:S(2)}) collective-permute-start(bf16[256,1024]{1,0:T(8,128)(2,1)} %get-tuple-element.47), channel_id=1, source_target_pairs={{0,3},{1,2},{2,1},{3,0},{4,7},{5,6},{6,5},{7,4},{8,11},{9,10},{10,... | collective-permute-start | bytes 1572872 | tf_op jit(solution)/shard_map/ppermute | solution.py:393
  68.0 2.2 collective-permute-done.7.far_gate
  70.3 22.5 %collective-permute-done.8.far_up = bf16[2048,256]{1,0:T(8,128)(2,1)} collective-permute-done((bf16[2048,256]{1,0:T(8,128)(2,1)S(1)}, bf16[2048,256]{1,0:T(8,128)(2,1)}, u32[]{:S(2)}, u32[]{:S(2)}) %collective-permute-start.8) | collective-permute-done | bytes 1048608 | tf_op jit(solution)/shard_map/ppermute | solution.py:376
  98.7 4.6 %shard_map.176 = (bf16[512,256]{1,0:T(8,128)(2,1)S(1)}, bf16[512,256]{1,0:T(8,128)(2,1)S(1)}, bf16[512,256]{1,0:T(8,128)(2,1)S(1)}, f32[1024,128]{1,0:T(8,128)S(1)}, f32[1088,128]{1,0:T(8,128)S(1)}) custom-call(bf16[512,2048]{1,0:T(8,128)(2,1)} %rows.2, f32[1,2048]{1,0:T(1,128)S(1)} %bitcast.36, bf16[2048,256]{1,0:T(8,128)(2,1)S(1)} %copy-done.4, ...), custom_call_target="tpu_custom_call" | custom-call | tf_op jit(solution)/shard_map/pallas_call | solution.py:335
  106.3 15.3 %all-to-all-start = ((f32[8,136,128]{2,1,0:T(8,128)}), f32[8,136,128]{2,1,0:T(8,128)}, u32[]{:S(2)}, u32[]{:S(2)}) async-start(f32[8,136,128]{2,1,0:T(8,128)} %bitcast.32), calls=%async_computation | async-start | bytes 1114112 | tf_op jit(solution)/shard_map/all_to_all | solution.py:347
  122.6 4.1 %shard_map.184.refs_2_ = bf16[256,512]{1,0:T(8,128)(2,1)S(1)} custom-call(s32[4]{0:T(128)S(1)} %pad_add_fusion.place, bf16[256,1024]{1,0:T(8,128)(2,1)S(1)} %bitcast.30, bf16[256,1024]{1,0:T(8,128)(2,1)} %collective-permute-done.11.other, bf16[2048,256]{1,0:T(8,128)(2,1)S(1)} %bitcast.23, bf16[2048,256]{1,0:T(8,128)(2,1)S(1)} %bitcast.26, ...), custom_call_target="tpu_custom_call" | custom-call | tf_op jit(solution)/shard_map/pallas_call | solution.py:279
  126.8 1.8 collective-permute-start.12
  128.6 4.3 %shard_map.183.refs_0_ = bf16[256,512]{1,0:T(8,128)(2,1)S(1)} custom-call(s32[4]{0:T(128)S(1)} %pad_add_fusion.place, bf16[256,1024]{1,0:T(8,128)(2,1)} %bitcast.15.own, bf16[256,1024]{1,0:T(8,128)(2,1)} %collective-permute-done.6.other, bf16[2048,256]{1,0:T(8,128)(2,1)S(1)} %bitcast.24, bf16[2048,256]{1,0:T(8,128)(2,1)S(1)} %bitcast.27, ...), custom_call_target="tpu_custom_call" | custom-call | tf_op jit(solution)/shard_map/pallas_call | solution.py:279
  133.0 2.0 collective-permute-done.12.refs_3_
  135.0 5.5 %collective-permute-done.9.refs_1_ = bf16[256,512]{1,0:T(8,128)(2,1)S(1)} collective-permute-done((bf16[256,512]{1,0:T(8,128)(2,1)S(1)}, bf16[256,512]{1,0:T(8,128)(2,1)S(1)}, u32[]{:S(2)}, u32[]{:S(2)}) %collective-permute-start.9) | collective-permute-done | bytes 262176 | tf_op jit(solution)/shard_map/ppermute | solution.py:435
  140.5 3.6 %shard_map.186 = bf16[32,16,1024]{2,1,0:T(8,128)(2,1)} custom-call(bf16[256,512]{1,0:T(8,128)(2,1)S(1)} %shard_map.183.refs_0_, bf16[256,512]{1,0:T(8,128)(2,1)S(1)} %collective-permute-done.9.refs_1_, bf16[256,512]{1,0:T(8,128)(2,1)S(1)} %shard_map.184.refs_2_, bf16[256,512]{1,0:T(8,128)(2,1)S(1)} %collective-permute-done.12.refs_3_, ...), custom_call_target="tpu_custom_call" | custom-call | tf_op jit(solution)/shard_map/pallas_call | solution.py:335
  144.2 9.2 %all-to-all-start.4 = ((bf16[32,16,1024]{2,1,0:T(8,128)(2,1)}), bf16[32,16,1024]{2,1,0:T(8,128)(2,1)}, u32[]{:S(2)}, u32[]{:S(2)}) async-start(bf16[32,16,1024]{2,1,0:T(8,128)(2,1)} %shard_map.186), calls=%async_computation.4 | async-start | bytes 2097152 | tf_op jit(solution)/shard_map/all_to_all | solution.py:347
  153.4 2.0 shard_map.177
  155.4 23.7 %all-to-all-done.4 = bf16[32,16,1024]{2,1,0:T(8,128)(2,1)} async-done(((bf16[32,16,1024]{2,1,0:T(8,128)(2,1)}), bf16[32,16,1024]{2,1,0:T(8,128)(2,1)}, u32[]{:S(2)}, u32[]{:S(2)}) %all-to-all-start.4) | async-done | bytes 1048608 | tf_op jit(solution)/shard_map/all_to_all | solution.py:347
  179.1 4.2 %all-to-all-start.1 = ((f32[8,136,128]{2,1,0:T(8,128)}), f32[8,136,128]{2,1,0:T(8,128)S(1)}, u32[]{:S(2)}, u32[]{:S(2)}) async-start(f32[8,136,128]{2,1,0:T(8,128)} %bitcast.7), calls=%async_computation.1 | async-start | bytes 1114112 | tf_op jit(solution)/shard_map/all_to_all | solution.py:347
  183.3 1.9 collective-permute-start.16
  185.2 13.5 %all-to-all-done.1 = f32[8,136,128]{2,1,0:T(8,128)S(1)} async-done(((f32[8,136,128]{2,1,0:T(8,128)}), f32[8,136,128]{2,1,0:T(8,128)S(1)}, u32[]{:S(2)}, u32[]{:S(2)}) %all-to-all-start.1) | async-done | bytes 557088 | tf_op jit(solution)/shard_map/all_to_all | solution.py:347
  199.3 3.9 %collective-permute-start = (f32[136,128]{1,0:T(8,128)S(1)}, f32[136,128]{1,0:T(8,128)S(1)}, u32[]{:S(2)}, u32[]{:S(2)}) collective-permute-start(f32[136,128]{1,0:T(8,128)S(1)} %get-tuple-element.35), channel_id=1, source_target_pairs={{0,4},{4,0},{1,5},{5,1},{2,6},{6,2},{3,7},{7,3},{8,12},{12,8},{9,1... | collective-permute-start | bytes 208904 | tf_op jit(solution)/shard_map/ppermute | solution.py:413
  205.4 4.0 %shard_map.179 = (bf16[128,2048]{1,0:T(8,128)(2,1)S(1)}, bf16[128,2048]{1,0:T(8,128)(2,1)S(1)}, bf16[128,2048]{1,0:T(8,128)(2,1)S(1)}, bf16[64,2048]{1,0:T(8,128)(2,1)S(1)}, bf16[64,2048]{1,0:T(8,128)(2,1)S(1)}) custom-call(s32[4]{0:T(128)S(1)} %pad_add_fusion.place, bf16[512,256]{1,0:T(8,128)(2,1)S(1)} %get-tuple-element.27.q, ...), custom_call_target="tpu_custom_call" | custom-call | tf_op jit(solution)/shard_map/pallas_call | solution.py:335
  209.4 1.7 collective-permute-start.1
  211.1 6.2 %collective-permute-done.1.from_near = bf16[64,2048]{1,0:T(8,128)(2,1)S(1)} collective-permute-done((bf16[64,2048]{1,0:T(8,128)(2,1)S(1)}, bf16[64,2048]{1,0:T(8,128)(2,1)S(1)}, u32[]{:S(2)}, u32[]{:S(2)}) %collective-permute-start.1) | collective-permute-done | bytes 262176 | tf_op jit(solution)/shard_map/ppermute | solution.py:422
  217.3 2.2 collective-permute-done.2.from_far
  221.0 2.5 %collective-permute-start.17 = (bf16[256,512]{1,0:T(8,128)(2,1)S(1)}, bf16[256,512]{1,0:T(8,128)(2,1)S(1)}, u32[]{:S(2)}, u32[]{:S(2)}) collective-permute-start(bf16[256,512]{1,0:T(8,128)(2,1)S(1)} %get-tuple-element.51), channel_id=1, source_target_pairs={{0,3},{1,2},{2,1},{3,0},{4,7},{5,6},{6,5},{7,4},{8,11},{9,10},{10,... | collective-permute-start | bytes 786440 | tf_op jit(solution)/shard_map/ppermute | solution.py:444
  223.5 8.2 %collective-permute-done.3.near = bf16[128,2048]{1,0:T(8,128)(2,1)S(1)} collective-permute-done((bf16[128,2048]{1,0:T(8,128)(2,1)S(1)}, bf16[128,2048]{1,0:T(8,128)(2,1)S(1)}, u32[]{:S(2)}, u32[]{:S(2)}) %collective-permute-start.3) | collective-permute-done | bytes 524320 | tf_op jit(solution)/shard_map/ppermute | solution.py:427
  234.0 4.6 %collective-permute-done.17.received = bf16[256,512]{1,0:T(8,128)(2,1)S(1)} collective-permute-done((bf16[256,512]{1,0:T(8,128)(2,1)S(1)}, bf16[256,512]{1,0:T(8,128)(2,1)S(1)}, u32[]{:S(2)}, u32[]{:S(2)}) %collective-permute-start.17) | collective-permute-done | bytes 262176 | tf_op jit(solution)/shard_map/ppermute | solution.py:444
  (87 shorter events, 28.4 us)
Async XLA Ops:
  0.6 41.9 %copy-start = (bf16[1,2048,256]{2,1,0:T(8,128)(2,1)S(1)}, bf16[1,2048,256]{2,1,0:T(8,128)(2,1)}, u32[]{:S(2)}) copy-start(bf16[1,2048,256]{2,1,0:T(8,128)(2,1)} %param.31) | copy-start | bytes 3145732
  0.6 47.8 %copy-start.1 = (bf16[1,2048,256]{2,1,0:T(8,128)(2,1)S(1)}, bf16[1,2048,256]{2,1,0:T(8,128)(2,1)}, u32[]{:S(2)}) copy-start(bf16[1,2048,256]{2,1,0:T(8,128)(2,1)} %param.32) | copy-start | bytes 3145732
  5.3 89.0 %copy-start.26 = (f32[2,512]{1,0:T(2,128)S(1)}, f32[2,512]{1,0:T(2,128)}, u32[]{:S(2)}) copy-start(f32[2,512]{1,0:T(2,128)} %param.23) | copy-start | bytes 12292
  5.3 89.0 %copy-start.27 = (f32[2,512]{1,0:T(2,128)S(1)}, f32[2,512]{1,0:T(2,128)}, u32[]{:S(2)}) copy-start(f32[2,512]{1,0:T(2,128)} %param.22) | copy-start | bytes 12292
  7.3 0.7 collective-permute-start.10
  8.8 28.3 %all-to-all-start.3 = ((bf16[32,8,1024]{2,1,0:T(8,128)(2,1)}), bf16[32,8,1024]{2,1,0:T(8,128)(2,1)S(1)}, u32[]{:S(2)}, u32[]{:S(2)}) async-start(bf16[32,8,1024]{2,1,0:T(8,128)(2,1)} %bitcast.39), calls=%async_computation.3 | async-start | bytes 1048576 | tf_op jit(solution)/shard_map/all_to_all | solution.py:347
  20.8 1.5 collective-permute-start.5
  37.1 20.6 %all-to-all-start.2 = ((bf16[32,8,1024]{2,1,0:T(8,128)(2,1)}), bf16[32,8,1024]{2,1,0:T(8,128)(2,1)}, u32[]{:S(2)}, u32[]{:S(2)}) async-start(bf16[32,8,1024]{2,1,0:T(8,128)(2,1)} %bitcast.14), calls=%async_computation.2 | async-start | bytes 1048576 | tf_op jit(solution)/shard_map/all_to_all | solution.py:347
  42.5 27.7 %collective-permute-start.7 = (bf16[2048,256]{1,0:T(8,128)(2,1)S(1)}, bf16[2048,256]{1,0:T(8,128)(2,1)S(1)}, u32[]{:S(2)}, u32[]{:S(2)}) collective-permute-start(bf16[2048,256]{1,0:T(8,128)(2,1)S(1)} %bitcast.22), channel_id=1, source_target_pairs={{0,3},{1,2},{2,1},{3,0},{4,7},{5,6},{6,5},{7,4},{8,11},{9,10},{10,... | collective-permute-start | bytes 3145736 | tf_op jit(solution)/shard_map/ppermute | solution.py:375
  48.5 44.3 %collective-permute-start.8 = (bf16[2048,256]{1,0:T(8,128)(2,1)S(1)}, bf16[2048,256]{1,0:T(8,128)(2,1)}, u32[]{:S(2)}, u32[]{:S(2)}) collective-permute-start(bf16[2048,256]{1,0:T(8,128)(2,1)S(1)} %bitcast.25), channel_id=1, source_target_pairs={{0,3},{1,2},{2,1},{3,0},{4,7},{5,6},{6,5},{7,4},{8,11},{9,10},{10,... | collective-permute-start | bytes 3145736 | tf_op jit(solution)/shard_map/ppermute | solution.py:376
  48.6 73.0 %collective-permute-start.11 = (bf16[256,1024]{1,0:T(8,128)(2,1)}, bf16[256,1024]{1,0:T(8,128)(2,1)}, u32[]{:S(2)}, u32[]{:S(2)}) collective-permute-start(bf16[256,1024]{1,0:T(8,128)(2,1)} %bitcast.29), channel_id=1, source_target_pairs={{0,1},{1,0},{2,3},{3,2},{4,5},{5,4},{6,7},{7,6},{8,9},{9,8},{10,11... | collective-permute-start | bytes 1572872 | tf_op jit(solution)/shard_map/ppermute | solution.py:433
  57.7 70.9 %collective-permute-start.6 = (bf16[256,1024]{1,0:T(8,128)(2,1)}, bf16[256,1024]{1,0:T(8,128)(2,1)}, u32[]{:S(2)}, u32[]{:S(2)}) collective-permute-start(bf16[256,1024]{1,0:T(8,128)(2,1)} %bitcast.15.own), channel_id=1, source_target_pairs={{0,1},{1,0},{2,3},{3,2},{4,5},{5,4},{6,7},{7,6},{8,9},{9,8},{10,11... | collective-permute-start | bytes 1572872 | tf_op jit(solution)/shard_map/ppermute | solution.py:433
  62.8 70.2 %collective-permute-start.13 = (bf16[256,1024]{1,0:T(8,128)(2,1)}, bf16[256,1024]{1,0:T(8,128)(2,1)}, u32[]{:S(2)}, u32[]{:S(2)}) collective-permute-start(bf16[256,1024]{1,0:T(8,128)(2,1)} %get-tuple-element.47), channel_id=1, source_target_pairs={{0,3},{1,2},{2,1},{3,0},{4,7},{5,6},{6,5},{7,4},{8,11},{9,10},{10,... | collective-permute-start | bytes 1572872 | tf_op jit(solution)/shard_map/ppermute | solution.py:393
  70.2 62.8 %collective-permute-start.14 = (bf16[256,1024]{1,0:T(8,128)(2,1)}, bf16[256,1024]{1,0:T(8,128)(2,1)}, u32[]{:S(2)}, u32[]{:S(2)}) collective-permute-start(bf16[256,1024]{1,0:T(8,128)(2,1)} %get-tuple-element.48), channel_id=1, source_target_pairs={{0,1},{1,0},{2,3},{3,2},{4,5},{5,4},{6,7},{7,6},{8,9},{9,8},{10,11... | collective-permute-start | bytes 1572872 | tf_op jit(solution)/shard_map/ppermute | solution.py:392
  92.8 40.2 %collective-permute-start.15 = (bf16[256,1024]{1,0:T(8,128)(2,1)}, bf16[256,1024]{1,0:T(8,128)(2,1)}, u32[]{:S(2)}, u32[]{:S(2)}) collective-permute-start(bf16[256,1024]{1,0:T(8,128)(2,1)} %get-tuple-element.49), channel_id=1, source_target_pairs={{0,2},{1,3},{2,0},{3,1},{4,6},{5,7},{6,4},{7,5},{8,10},{9,11},{10,... | collective-permute-start | bytes 1572872 | tf_op jit(solution)/shard_map/ppermute | solution.py:394
  106.3 37.9 %all-to-all-start = ((f32[8,136,128]{2,1,0:T(8,128)}), f32[8,136,128]{2,1,0:T(8,128)}, u32[]{:S(2)}, u32[]{:S(2)}) async-start(f32[8,136,128]{2,1,0:T(8,128)} %bitcast.32), calls=%async_computation | async-start | bytes 1114112 | tf_op jit(solution)/shard_map/all_to_all | solution.py:347
  126.8 13.8 %copy-start.14 = (bf16[256,1024]{1,0:T(8,128)(2,1)S(1)}, bf16[256,1024]{1,0:T(8,128)(2,1)}, u32[]{:S(2)}) copy-start(bf16[256,1024]{1,0:T(8,128)(2,1)} %copy-done.13) | copy-start | bytes 1572868
  126.8 8.3 %collective-permute-start.12 = (bf16[256,512]{1,0:T(8,128)(2,1)S(1)}, bf16[256,512]{1,0:T(8,128)(2,1)S(1)}, u32[]{:S(2)}, u32[]{:S(2)}) collective-permute-start(bf16[256,512]{1,0:T(8,128)(2,1)S(1)} %shard_map.184.refs_2_), channel_id=1, source_target_pairs={{0,1},{1,0},{2,3},{3,2},{4,5},{5,4},{6,7},{7,6},{8,9},{9,8},{10,11... | collective-permute-start | bytes 786440 | tf_op jit(solution)/shard_map/ppermute | solution.py:435
  132.9 7.7 %collective-permute-start.9 = (bf16[256,512]{1,0:T(8,128)(2,1)S(1)}, bf16[256,512]{1,0:T(8,128)(2,1)S(1)}, u32[]{:S(2)}, u32[]{:S(2)}) collective-permute-start(bf16[256,512]{1,0:T(8,128)(2,1)S(1)} %shard_map.183.refs_0_), channel_id=1, source_target_pairs={{0,1},{1,0},{2,3},{3,2},{4,5},{5,4},{6,7},{7,6},{8,9},{9,8},{10,11... | collective-permute-start | bytes 786440 | tf_op jit(solution)/shard_map/ppermute | solution.py:435
  144.1 60.0 %copy-start.12 = (f32[1024,128]{1,0:T(8,128)S(1)}, f32[1024,128]{1,0:T(8,128)}, u32[]{:S(2)}) copy-start(f32[1024,128]{1,0:T(8,128)} %copy-done.11) | copy-start | bytes 1572868
  144.1 60.0 %copy-start.17 = (bf16[512,256]{1,0:T(8,128)(2,1)S(1)}, bf16[512,256]{1,0:T(8,128)(2,1)}, u32[]{:S(2)}) copy-start(bf16[512,256]{1,0:T(8,128)(2,1)} %copy-done.16) | copy-start | bytes 786436
  144.2 60.0 %copy-start.19 = (bf16[512,256]{1,0:T(8,128)(2,1)S(1)}, bf16[512,256]{1,0:T(8,128)(2,1)}, u32[]{:S(2)}) copy-start(bf16[512,256]{1,0:T(8,128)(2,1)} %copy-done.18) | copy-start | bytes 786436
  144.2 60.0 %copy-start.23 = (f32[1024]{0:T(1024)S(1)}, f32[1024]{0:T(1024)}, u32[]{:S(2)}) copy-start(f32[1024]{0:T(1024)} %param.24) | copy-start | bytes 12292
  144.2 34.9 %all-to-all-start.4 = ((bf16[32,16,1024]{2,1,0:T(8,128)(2,1)}), bf16[32,16,1024]{2,1,0:T(8,128)(2,1)}, u32[]{:S(2)}, u32[]{:S(2)}) async-start(bf16[32,16,1024]{2,1,0:T(8,128)(2,1)} %shard_map.186), calls=%async_computation.4 | async-start | bytes 2097152 | tf_op jit(solution)/shard_map/all_to_all | solution.py:347
  179.1 19.6 %all-to-all-start.1 = ((f32[8,136,128]{2,1,0:T(8,128)}), f32[8,136,128]{2,1,0:T(8,128)S(1)}, u32[]{:S(2)}, u32[]{:S(2)}) async-start(f32[8,136,128]{2,1,0:T(8,128)} %bitcast.7), calls=%async_computation.1 | async-start | bytes 1114112 | tf_op jit(solution)/shard_map/all_to_all | solution.py:347
  183.3 36.8 %collective-permute-start.16 = (bf16[512,1024]{1,0:T(8,128)(2,1)}, bf16[512,1024]{1,0:T(8,128)(2,1)S(1)}, u32[]{:S(2)}, u32[]{:S(2)}) collective-permute-start(bf16[512,1024]{1,0:T(8,128)(2,1)} %bitcast.21), channel_id=1, source_target_pairs={{0,0},{1,1},{2,6},{3,7},{4,4},{5,5},{6,2},{7,3},{8,8},{9,9},{10,14... | collective-permute-start | bytes 3145736 | tf_op jit(solution)/shard_map/ppermute | solution.py:440
  199.3 4.8 %collective-permute-start = (f32[136,128]{1,0:T(8,128)S(1)}, f32[136,128]{1,0:T(8,128)S(1)}, u32[]{:S(2)}, u32[]{:S(2)}) collective-permute-start(f32[136,128]{1,0:T(8,128)S(1)} %get-tuple-element.35), channel_id=1, source_target_pairs={{0,4},{4,0},{1,5},{5,1},{2,6},{6,2},{3,7},{7,3},{8,12},{12,8},{9,1... | collective-permute-start | bytes 208904 | tf_op jit(solution)/shard_map/ppermute | solution.py:413
  209.4 7.9 %collective-permute-start.1 = (bf16[64,2048]{1,0:T(8,128)(2,1)S(1)}, bf16[64,2048]{1,0:T(8,128)(2,1)S(1)}, u32[]{:S(2)}, u32[]{:S(2)}) collective-permute-start(bf16[64,2048]{1,0:T(8,128)(2,1)S(1)} %get-tuple-element.39), channel_id=1, source_target_pairs={{0,1},{1,0},{2,3},{3,2},{4,5},{5,4},{6,7},{7,6},{8,9},{9,8},{10,11... | collective-permute-start | bytes 786440 | tf_op jit(solution)/shard_map/ppermute | solution.py:422
  211.1 8.4 %collective-permute-start.2 = (bf16[64,2048]{1,0:T(8,128)(2,1)S(1)}, bf16[64,2048]{1,0:T(8,128)(2,1)S(1)}, u32[]{:S(2)}, u32[]{:S(2)}) collective-permute-start(bf16[64,2048]{1,0:T(8,128)(2,1)S(1)} %get-tuple-element.40), channel_id=1, source_target_pairs={{0,3},{1,2},{2,1},{3,0},{4,7},{5,6},{6,5},{7,4},{8,11},{9,10},{10,... | collective-permute-start | bytes 786440 | tf_op jit(solution)/shard_map/ppermute | solution.py:423
  219.6 12.1 %collective-permute-start.3 = (bf16[128,2048]{1,0:T(8,128)(2,1)S(1)}, bf16[128,2048]{1,0:T(8,128)(2,1)S(1)}, u32[]{:S(2)}, u32[]{:S(2)}) collective-permute-start(bf16[128,2048]{1,0:T(8,128)(2,1)S(1)} %get-tuple-element.41), channel_id=1, source_target_pairs={{0,1},{1,0},{2,3},{3,2},{4,5},{5,4},{6,7},{7,6},{8,9},{9,8},{10,11... | collective-permute-start | bytes 1572872 | tf_op jit(solution)/shard_map/ppermute | solution.py:427
  219.7 13.3 %collective-permute-start.4 = (bf16[128,2048]{1,0:T(8,128)(2,1)S(1)}, bf16[128,2048]{1,0:T(8,128)(2,1)S(1)}, u32[]{:S(2)}, u32[]{:S(2)}) collective-permute-start(bf16[128,2048]{1,0:T(8,128)(2,1)S(1)} %get-tuple-element.42), channel_id=1, source_target_pairs={{0,3},{1,2},{2,1},{3,0},{4,7},{5,6},{6,5},{7,4},{8,11},{9,10},{10,... | collective-permute-start | bytes 1572872 | tf_op jit(solution)/shard_map/ppermute | solution.py:428
  221.0 17.6 %collective-permute-start.17 = (bf16[256,512]{1,0:T(8,128)(2,1)S(1)}, bf16[256,512]{1,0:T(8,128)(2,1)S(1)}, u32[]{:S(2)}, u32[]{:S(2)}) collective-permute-start(bf16[256,512]{1,0:T(8,128)(2,1)S(1)} %get-tuple-element.51), channel_id=1, source_target_pairs={{0,3},{1,2},{2,1},{3,0},{4,7},{5,6},{6,5},{7,4},{8,11},{9,10},{10,... | collective-permute-start | bytes 786440 | tf_op jit(solution)/shard_map/ppermute | solution.py:444
  (19 other events, 22.4 us)

commit v3 on v2

--- a/solution.py
+++ b/solution.py
@@ -12,11 +12,10 @@
 YC = ("y", "c")
 NEAR = [(i, i ^ 1) for i in range(4)]
 FAR = [(i, 3 - i) for i in range(4)]
-ACROSS = [(i, i ^ 2) for i in range(4)]
 SWAP = [(0, 1), (1, 0)]
 CROSS = [(c * 4 + t, (c if t < 2 else 1 - c) * 4 + t) for c in range(2) for t in range(4)]
 LINES = 136
-CHUNKS = 2
+CHUNKS = 1
 f32 = jnp.float32
 bf16 = jnp.bfloat16
 
@@ -185,14 +184,16 @@
     out[...] = total.astype(bf16)
 
 
-def cut_kernel(place, weights, own, near, far, across):
+def cut_kernel(place, weights, far_weights, keep, give):
     rank = place[0]
+    units = weights.shape[0]
     share = weights.shape[1] // 4
-    for target, device in ((own, rank), (near, rank ^ 1), (far, 3 - rank), (across, rank ^ 2)):
+    for target, device in ((keep, rank), (give, rank ^ 1)):
         for j, quarter in enumerate((device, 3 - device)):
-            target[:, j * share : (j + 1) * share] = weights[
-                :, pl.ds(pl.multiple_of(quarter * share, share), share)
-            ]
+            at = pl.ds(pl.multiple_of(quarter * share, share), share)
+            columns = slice(j * share, (j + 1) * share)
+            target[:units, columns] = weights[:, at]
+            target[units:, columns] = far_weights[:, at]
 
 
 def dispatch_kernel(place, rows, gain, group_router, expert_router, routes, *rest):
@@ -287,24 +288,15 @@
             scratch_shapes=[pltpu.VMEM((own.shape[0], 4 * units), f32)],
         ),
         compiler_params=pltpu.CompilerParams(
-            vmem_limit_bytes=32 * 1024 * 1024, dimension_semantics=("arbitrary",)
+            vmem_limit_bytes=16 * 1024 * 1024, dimension_semantics=("arbitrary",)
         ),
     )(place, own, other, *weights)
 
 
-def down_kernel(*refs):
-    pairs, (w_own, w_far, w_near, w_across, out) = refs[: 2 * CHUNKS], refs[2 * CHUNKS :]
-    each = 16 // CHUNKS
-    for n in range(CHUNKS):
-        own, other = pairs[2 * n : 2 * n + 2]
-        units = own.shape[1] // 2
-        total = jnp.dot(own[:, :units], w_own[...], preferred_element_type=f32)
-        total = total + jnp.dot(own[:, units:], w_far[...], preferred_element_type=f32)
-        total = total + jnp.dot(other[:, :units], w_near[...], preferred_element_type=f32)
-        total = total + jnp.dot(other[:, units:], w_across[...], preferred_element_type=f32)
-        out[:, n * each : (n + 1) * each, :] = total.astype(bf16).reshape(
-            out.shape[0], each, out.shape[2]
-        )
+def down_kernel(own, other, mine, theirs, out):
+    total = jnp.dot(own[...], mine[...], preferred_element_type=f32)
+    total = total + jnp.dot(other[...], theirs[...], preferred_element_type=f32)
+    out[...] = total.astype(bf16)
 
 
 def combine_kernel(notes, rows, keep, send):
@@ -326,8 +318,11 @@
     out[...] = (keep[...] + received[...].astype(f32)).astype(bf16)
 
 
-def run(kernel, shapes, args, place=None, scratch=()):
-    specs = [pl.BlockSpec(memory_space=pltpu.VMEM)] * len(args)
+def run(kernel, shapes, args, place=None, scratch=(), room=8):
+    def block(shape):
+        return pl.BlockSpec(tuple(shape), lambda n: (0,) * len(shape))
+
+    specs = [block(a.shape) for a in args]
     if place is not None:
         specs = [pl.BlockSpec(memory_space=pltpu.SMEM)] + specs
         args = (place, *args)
@@ -335,10 +330,11 @@
     result = pl.pallas_call(
         kernel,
         out_shape=outs,
+        grid=(1,),
         in_specs=specs,
-        out_specs=tuple([pl.BlockSpec(memory_space=pltpu.VMEM)] * len(outs)),
+        out_specs=tuple(block(o.shape) for o in outs),
         scratch_shapes=[pltpu.VMEM(s, d) for s, d in scratch],
-        compiler_params=pltpu.CompilerParams(vmem_limit_bytes=48 * 1024 * 1024),
+        compiler_params=pltpu.CompilerParams(vmem_limit_bytes=room * 1024 * 1024),
     )(*args)
     return result if len(outs) > 1 else result[0]
 
@@ -372,6 +368,7 @@
     slots = 32 * 16
     gate, up, down = gate_experts[0], up_experts[0], down_experts[0]
     units = gate.shape[1]
+    far_down = lax.ppermute(down, "tp", FAR)
     far_gate = lax.ppermute(gate, "tp", FAR)
     far_up = lax.ppermute(up, "tp", FAR)
     *sends, notes = run(
@@ -380,18 +377,17 @@
         (expert_in, expert_gain.reshape(1, -1), group_router.T, expert_router.T, routes.T),
         place,
         [((tokens, width), bf16)],
+        room=16,
     )
     arrived = []
     for send in sends:
         send = lax.ppermute(send, ("c", "tp"), CROSS)
         arrived.append(traded(send, ZY))
 
-    w_own, w_near, w_far, w_across = run(
-        cut_kernel, (((units, 2 * share), bf16),) * 4, (down,), place
-    )
-    w_near = lax.ppermute(w_near, "tp", NEAR)
-    w_far = lax.ppermute(w_far, "tp", FAR)
-    w_across = lax.ppermute(w_across, "tp", ACROSS)
+    down_mine, give = run(
+        cut_kernel, (((2 * units, 2 * share), bf16),) * 2, (down, far_down), place, room=16
+    )
+    down_theirs = lax.ppermute(give, "tp", NEAR)
 
     row_count = mixer_in.shape[0]
     local = query_weight.shape[1]
@@ -403,6 +399,7 @@
         (mixer_in, mixer_gain.reshape(1, -1), query_weight, key_weight, value_weight, log_forget, inputs),
         None,
         [((row_count, width), bf16)],
+        room=24,
     )
     members = traded(spread, YC)
     spread, before = run(
@@ -418,6 +415,7 @@
         (q, k, v, log_forget, inputs, memories, mine, theirs, head_gain.reshape(1, -1), mixer_out_weight),
         place,
         [((row_count, local), bf16)],
+        room=16,
     )
     from_near = lax.ppermute(across_near, "tp", NEAR)
     from_far = lax.ppermute(across_far, "tp", FAR)
@@ -434,9 +432,9 @@
         hidden = hidden_of(place, rows, other_rows, (gate, up, far_gate, far_up))
         pairs += [hidden, lax.ppermute(hidden, "tp", NEAR)]
     result = run(
-        down_kernel, (((32, 16, 2 * share), bf16),), (*pairs, w_own, w_far, w_near, w_across)
-    )
-    back = traded(result.reshape(slots, 2 * share), ZY)
+        down_kernel, (((slots, 2 * share), bf16),), (*pairs, down_mine, down_theirs), room=16
+    )
+    back = traded(result, ZY)
     back = lax.ppermute(back, ("c", "tp"), CROSS)
     keep, give = run(
         combine_kernel, (((tokens, share), f32), ((tokens, share), bf16)), (notes, back)

time: 242 us -> 224 us (0.926)
  starting transfers between devices: 74.7 us -> 53.9 us
  waiting for transfers between devices: 117 us -> 124 us
  Pallas kernels: 29.8 us -> 25.1 us
    ppermute x1, waiting for transfers between devices: 2.19 us -> 19.8 us  [shards(): far_gate = lax.ppermute(gate, 'tp', FAR)]
    all_to_all x5 -> x4, starting transfers between devices: 46.2 us -> 29.3 us  [traded(): return lax.all_to_all(x, axis, 0, 0, tiled=True)]
    ppermute x2 -> x1, waiting for transfers between devices: 7.53 us -> 0.01 us  [shards(): pairs += [hidden, lax.ppermute(hidden, 'tp', NEAR)]]
    ppermute x1, starting transfers between devices: 5.96 us -> 0.1 us  [shards(): far_gate = lax.ppermute(gate, 'tp', FAR)]
    ppermute x1, waiting for transfers between devices: 6.21 us -> 3.44 us  [shards(): from_near = lax.ppermute(across_near, 'tp', NEAR)]
    ppermute x1, starting transfers between devices: 0.01 us -> 2.67 us  [shards(): from_far = lax.ppermute(across_far, 'tp', FAR)]
    pallas_call x2 -> x1, Pallas kernels: 8.4 us -> 5.73 us  [hidden_of(): pl.pallas_call(hidden_kernel, out_shape=jax.ShapeDtypeStruct((own.shape[0...]
    ppermute x1, starting transfers between devices: 0.11 us -> 2.58 us  [shards(): far_up = lax.ppermute(up, 'tp', FAR)]
  transfers between devices with their start and end apart: 23 -> 18, of which waited for: 14 -> 13; matrix products, arithmetic and copies ran while one was open for 0% -> 0% of each run, Pallas kernels for 11% -> 10%
where the time goes in v3:
time: 224 us; the launch traced here: 221 us
  waiting for transfers between devices  124 us (55%)
  starting transfers between devices  53.9 us (24%)
  Pallas kernels  25.1 us (11%)
  local copies, waits for them, and re-layouts  17.4 us (8%)
    all_to_all x4, waiting for transfers between devices, traded(): return lax.all_to_all(x, axis, 0, 0, tiled=True)  59.8 us
    all_to_all x4, starting transfers between devices, traded(): return lax.all_to_all(x, axis, 0, 0, tiled=True)  29.3 us
    ppermute x1, waiting for transfers between devices, shards(): far_up = lax.ppermute(up, 'tp', FAR)  22.5 us
    ppermute x1, waiting for transfers between devices, shards(): far_gate = lax.ppermute(gate, 'tp', FAR)  19.8 us
    pallas_call x11, Pallas kernels, run(): pl.pallas_call(kernel, out_shape=outs, grid=(1,), in_specs=specs, out_spe...  19.3 us
    unnamed x62, local copies, waits for them, and re-layouts  17.4 us
    ppermute x1, waiting for transfers between devices, shards(): near = lax.ppermute(to_near, 'tp', NEAR)  8.19 us
    ppermute x1, starting transfers between devices, shards(): far_down = lax.ppermute(down, 'tp', FAR)  5.88 us
  transfers between devices with their start and end apart: 18, of which 13 were waited for; matrix products, arithmetic and copies ran while one was open for 0% of the time, Pallas kernels for 10%

profile of v3, /device:TPU:1, one launch (start us, length us, event | category | flops | bytes accessed | tf_op | source)
XLA Modules:
  0.0 221.5 jit_solution(5982452437926740696)
XLA Ops:
  0.7 1.2 copy-done.4
  5.1 2.0 shard_map.182
  7.8 1.7 collective-permute-start.5
  9.4 12.0 %all-to-all-start.2 = ((bf16[32,16,1024]{2,1,0:T(8,128)(2,1)}), bf16[32,16,1024]{2,1,0:T(8,128)(2,1)S(1)}, u32[]{:S(2)}, u32[]{:S(2)}) async-start(bf16[32,16,1024]{2,1,0:T(8,128)(2,1)} %bitcast.14), calls=%async_computation.2 | async-start | bytes 2097152 | tf_op jit(solution)/shard_map/all_to_all | solution.py:343
  21.5 5.9 %collective-permute-start.10 = (bf16[256,2048]{1,0:T(8,128)(2,1)S(1)}, bf16[256,2048]{1,0:T(8,128)(2,1)S(1)}, u32[]{:S(2)}, u32[]{:S(2)}) collective-permute-start(bf16[256,2048]{1,0:T(8,128)(2,1)S(1)} %bitcast.25), channel_id=1, source_target_pairs={{0,3},{1,2},{2,1},{3,0},{4,7},{5,6},{6,5},{7,4},{8,11},{9,10},{10,... | collective-permute-start | bytes 3145736 | tf_op jit(solution)/shard_map/ppermute | solution.py:371
  27.5 2.6 %collective-permute-start.8 = (bf16[2048,256]{1,0:T(8,128)(2,1)}, bf16[2048,256]{1,0:T(8,128)(2,1)}, u32[]{:S(2)}, u32[]{:S(2)}) collective-permute-start(bf16[2048,256]{1,0:T(8,128)(2,1)} %bitcast.29), channel_id=1, source_target_pairs={{0,3},{1,2},{2,1},{3,0},{4,7},{5,6},{6,5},{7,4},{8,11},{9,10},{10,... | collective-permute-start | bytes 3145736 | tf_op jit(solution)/shard_map/ppermute | solution.py:373
  30.0 17.6 %all-to-all-done.2 = bf16[32,16,1024]{2,1,0:T(8,128)(2,1)S(1)} async-done(((bf16[32,16,1024]{2,1,0:T(8,128)(2,1)}), bf16[32,16,1024]{2,1,0:T(8,128)(2,1)S(1)}, u32[]{:S(2)}, u32[]{:S(2)}) %all-to-all-start.2) | async-done | bytes 1048608 | tf_op jit(solution)/shard_map/all_to_all | solution.py:343
  48.9 1.4 collective-permute-done.10.far_weights
  50.2 1.7 shard_map.184
  53.0 19.8 %collective-permute-done.7.far_gate = bf16[2048,256]{1,0:T(8,128)(2,1)} collective-permute-done((bf16[2048,256]{1,0:T(8,128)(2,1)}, bf16[2048,256]{1,0:T(8,128)(2,1)}, u32[]{:S(2)}, u32[]{:S(2)}) %collective-permute-start.7) | collective-permute-done | bytes 1048608 | tf_op jit(solution)/shard_map/ppermute | solution.py:372
  72.8 22.5 %collective-permute-done.8.far_up = bf16[2048,256]{1,0:T(8,128)(2,1)} collective-permute-done((bf16[2048,256]{1,0:T(8,128)(2,1)}, bf16[2048,256]{1,0:T(8,128)(2,1)}, u32[]{:S(2)}, u32[]{:S(2)}) %collective-permute-start.8) | collective-permute-done | bytes 1048608 | tf_op jit(solution)/shard_map/ppermute | solution.py:373
  95.3 5.7 %shard_map.183.own = bf16[512,512]{1,0:T(8,128)(2,1)} custom-call(s32[4]{0:T(128)S(1)} %pad_add_fusion.place, bf16[512,1024]{1,0:T(8,128)(2,1)S(1)} %bitcast.22, bf16[512,1024]{1,0:T(8,128)(2,1)S(1)} %collective-permute-done.6.other, bf16[2048,256]{1,0:T(8,128)(2,1)S(1)} %bitcast.28, bf16[2048,256]{1,0:T(8,128)(2,1)S(1)} %bitcast.30, ...), custom_call_target="tpu_custom_call" | custom-call | tf_op jit(solution)/shard_map/pallas_call | solution.py:280
  104.8 3.0 %shard_map.176 = (bf16[512,256]{1,0:T(8,128)(2,1)S(1)}, bf16[512,256]{1,0:T(8,128)(2,1)S(1)}, bf16[512,256]{1,0:T(8,128)(2,1)S(1)}, f32[1024,128]{1,0:T(8,128)S(1)}, f32[1088,128]{1,0:T(8,128)S(1)}) custom-call(bf16[512,2048]{1,0:T(8,128)(2,1)S(1)} %copy-done, f32[1,2048]{1,0:T(1,128)S(1)} %bitcast.35, bf16[2048,256]{1,0:T(8,128)(2,1)S(1)} %copy-done.1, ...), custom_call_target="tpu_custom_call" | custom-call | tf_op jit(solution)/shard_map/pallas_call | solution.py:330
  110.9 5.7 %all-to-all-start = ((f32[8,136,128]{2,1,0:T(8,128)}), f32[8,136,128]{2,1,0:T(8,128)S(1)}, u32[]{:S(2)}, u32[]{:S(2)}) async-start(f32[8,136,128]{2,1,0:T(8,128)} %bitcast.31), calls=%async_computation | async-start | bytes 1114112 | tf_op jit(solution)/shard_map/all_to_all | solution.py:343
  117.8 3.8 %shard_map.185 = bf16[512,1024]{1,0:T(8,128)(2,1)} custom-call(bf16[512,512]{1,0:T(8,128)(2,1)} %shard_map.183.own, bf16[512,512]{1,0:T(8,128)(2,1)} %collective-permute-done.9.other, bf16[512,1024]{1,0:T(8,128)(2,1)S(1)} %copy-done.10, bf16[512,1024]{1,0:T(8,128)(2,1)} %collective-permute-done.11.theirs), custom_call_target="tpu_custom_call" | custom-call | tf_op jit(solution)/shard_map/pallas_call | solution.py:330
  121.6 4.7 %all-to-all-done = f32[8,136,128]{2,1,0:T(8,128)S(1)} async-done(((f32[8,136,128]{2,1,0:T(8,128)}), f32[8,136,128]{2,1,0:T(8,128)S(1)}, u32[]{:S(2)}, u32[]{:S(2)}) %all-to-all-start) | async-done | bytes 557088 | tf_op jit(solution)/shard_map/all_to_all | solution.py:343
  126.3 7.5 %all-to-all-start.3 = ((bf16[32,16,1024]{2,1,0:T(8,128)(2,1)}), bf16[32,16,1024]{2,1,0:T(8,128)(2,1)S(1)}, u32[]{:S(2)}, u32[]{:S(2)}) async-start(bf16[32,16,1024]{2,1,0:T(8,128)(2,1)} %bitcast.19), calls=%async_computation.3 | async-start | bytes 2097152 | tf_op jit(solution)/shard_map/all_to_all | solution.py:343
  133.8 1.4 shard_map.177
  135.9 24.0 %all-to-all-done.3 = bf16[32,16,1024]{2,1,0:T(8,128)(2,1)S(1)} async-done(((bf16[32,16,1024]{2,1,0:T(8,128)(2,1)}), bf16[32,16,1024]{2,1,0:T(8,128)(2,1)S(1)}, u32[]{:S(2)}, u32[]{:S(2)}) %all-to-all-start.3) | async-done | bytes 1048608 | tf_op jit(solution)/shard_map/all_to_all | solution.py:343
  159.9 4.0 %all-to-all-start.1 = ((f32[8,136,128]{2,1,0:T(8,128)}), f32[8,136,128]{2,1,0:T(8,128)S(1)}, u32[]{:S(2)}, u32[]{:S(2)}) async-start(f32[8,136,128]{2,1,0:T(8,128)} %bitcast.7), calls=%async_computation.1 | async-start | bytes 1114112 | tf_op jit(solution)/shard_map/all_to_all | solution.py:343
  163.9 1.9 collective-permute-start.12
  165.8 13.5 %all-to-all-done.1 = f32[8,136,128]{2,1,0:T(8,128)S(1)} async-done(((f32[8,136,128]{2,1,0:T(8,128)}), f32[8,136,128]{2,1,0:T(8,128)S(1)}, u32[]{:S(2)}, u32[]{:S(2)}) %all-to-all-start.1) | async-done | bytes 557088 | tf_op jit(solution)/shard_map/all_to_all | solution.py:343
  180.8 3.9 %collective-permute-start = (f32[136,128]{1,0:T(8,128)S(1)}, f32[136,128]{1,0:T(8,128)S(1)}, u32[]{:S(2)}, u32[]{:S(2)}) collective-permute-start(f32[136,128]{1,0:T(8,128)S(1)} %get-tuple-element.32), channel_id=1, source_target_pairs={{0,4},{4,0},{1,5},{5,1},{2,6},{6,2},{3,7},{7,3},{8,12},{12,8},{9,1... | collective-permute-start | bytes 208904 | tf_op jit(solution)/shard_map/ppermute | solution.py:410
  187.5 4.0 %shard_map.179 = (bf16[128,2048]{1,0:T(8,128)(2,1)S(1)}, bf16[128,2048]{1,0:T(8,128)(2,1)S(1)}, bf16[128,2048]{1,0:T(8,128)(2,1)S(1)}, bf16[64,2048]{1,0:T(8,128)(2,1)S(1)}, bf16[64,2048]{1,0:T(8,128)(2,1)S(1)}) custom-call(s32[4]{0:T(128)S(1)} %pad_add_fusion.place, bf16[512,256]{1,0:T(8,128)(2,1)S(1)} %get-tuple-element.24.q, ...), custom_call_target="tpu_custom_call" | custom-call | tf_op jit(solution)/shard_map/pallas_call | solution.py:330
  191.5 1.6 collective-permute-start.1
  193.1 2.7 %collective-permute-start.2 = (bf16[64,2048]{1,0:T(8,128)(2,1)S(1)}, bf16[64,2048]{1,0:T(8,128)(2,1)S(1)}, u32[]{:S(2)}, u32[]{:S(2)}) collective-permute-start(bf16[64,2048]{1,0:T(8,128)(2,1)S(1)} %get-tuple-element.37), channel_id=1, source_target_pairs={{0,3},{1,2},{2,1},{3,0},{4,7},{5,6},{6,5},{7,4},{8,11},{9,10},{10,... | collective-permute-start | bytes 786440 | tf_op jit(solution)/shard_map/ppermute | solution.py:421
  195.8 3.4 %collective-permute-done.1.from_near = bf16[64,2048]{1,0:T(8,128)(2,1)S(1)} collective-permute-done((bf16[64,2048]{1,0:T(8,128)(2,1)S(1)}, bf16[64,2048]{1,0:T(8,128)(2,1)S(1)}, u32[]{:S(2)}, u32[]{:S(2)}) %collective-permute-start.1) | collective-permute-done | bytes 262176 | tf_op jit(solution)/shard_map/ppermute | solution.py:420
  199.2 2.3 %collective-permute-done.2.from_far = bf16[64,2048]{1,0:T(8,128)(2,1)S(1)} collective-permute-done((bf16[64,2048]{1,0:T(8,128)(2,1)S(1)}, bf16[64,2048]{1,0:T(8,128)(2,1)S(1)}, u32[]{:S(2)}, u32[]{:S(2)}) %collective-permute-start.2) | collective-permute-done | bytes 262176 | tf_op jit(solution)/shard_map/ppermute | solution.py:421
  201.8 2.7 %collective-permute-start.4 = (bf16[128,2048]{1,0:T(8,128)(2,1)S(1)}, bf16[128,2048]{1,0:T(8,128)(2,1)S(1)}, u32[]{:S(2)}, u32[]{:S(2)}) collective-permute-start(bf16[128,2048]{1,0:T(8,128)(2,1)S(1)} %get-tuple-element.39), channel_id=1, source_target_pairs={{0,3},{1,2},{2,1},{3,0},{4,7},{5,6},{6,5},{7,4},{8,11},{9,10},{10,... | collective-permute-start | bytes 1572872 | tf_op jit(solution)/shard_map/ppermute | solution.py:426
  205.6 8.2 %collective-permute-done.3.near = bf16[128,2048]{1,0:T(8,128)(2,1)S(1)} collective-permute-done((bf16[128,2048]{1,0:T(8,128)(2,1)S(1)}, bf16[128,2048]{1,0:T(8,128)(2,1)S(1)}, u32[]{:S(2)}, u32[]{:S(2)}) %collective-permute-start.3) | collective-permute-done | bytes 524320 | tf_op jit(solution)/shard_map/ppermute | solution.py:425
  213.8 1.3 collective-permute-done.4.far
  216.1 4.6 %collective-permute-done.13.received = bf16[256,512]{1,0:T(8,128)(2,1)S(1)} collective-permute-done((bf16[256,512]{1,0:T(8,128)(2,1)S(1)}, bf16[256,512]{1,0:T(8,128)(2,1)S(1)}, u32[]{:S(2)}, u32[]{:S(2)}) %collective-permute-start.13) | collective-permute-done | bytes 262176 | tf_op jit(solution)/shard_map/ppermute | solution.py:442
  (82 shorter events, 22.3 us)
Async XLA Ops:
  0.7 1.2 copy-start.4
  5.1 16.4 %copy-start.5 = (bf16[1,256,2048]{2,1,0:T(8,128)(2,1)S(1)}, bf16[1,256,2048]{2,1,0:T(8,128)(2,1)}, u32[]{:S(2)}) copy-start(bf16[1,256,2048]{2,1,0:T(8,128)(2,1)} %param.33) | copy-start | bytes 3145732
  7.8 1.7 collective-permute-start.5
  9.4 38.2 %all-to-all-start.2 = ((bf16[32,16,1024]{2,1,0:T(8,128)(2,1)}), bf16[32,16,1024]{2,1,0:T(8,128)(2,1)S(1)}, u32[]{:S(2)}, u32[]{:S(2)}) async-start(bf16[32,16,1024]{2,1,0:T(8,128)(2,1)} %bitcast.14), calls=%async_computation.2 | async-start | bytes 2097152 | tf_op jit(solution)/shard_map/all_to_all | solution.py:343
  21.5 28.8 %collective-permute-start.10 = (bf16[256,2048]{1,0:T(8,128)(2,1)S(1)}, bf16[256,2048]{1,0:T(8,128)(2,1)S(1)}, u32[]{:S(2)}, u32[]{:S(2)}) collective-permute-start(bf16[256,2048]{1,0:T(8,128)(2,1)S(1)} %bitcast.25), channel_id=1, source_target_pairs={{0,3},{1,2},{2,1},{3,0},{4,7},{5,6},{6,5},{7,4},{8,11},{9,10},{10,... | collective-permute-start | bytes 3145736 | tf_op jit(solution)/shard_map/ppermute | solution.py:371
  27.4 45.5 %collective-permute-start.7 = (bf16[2048,256]{1,0:T(8,128)(2,1)}, bf16[2048,256]{1,0:T(8,128)(2,1)}, u32[]{:S(2)}, u32[]{:S(2)}) collective-permute-start(bf16[2048,256]{1,0:T(8,128)(2,1)} %bitcast.27), channel_id=1, source_target_pairs={{0,3},{1,2},{2,1},{3,0},{4,7},{5,6},{6,5},{7,4},{8,11},{9,10},{10,... | collective-permute-start | bytes 3145736 | tf_op jit(solution)/shard_map/ppermute | solution.py:372
  27.5 67.8 %collective-permute-start.8 = (bf16[2048,256]{1,0:T(8,128)(2,1)}, bf16[2048,256]{1,0:T(8,128)(2,1)}, u32[]{:S(2)}, u32[]{:S(2)}) collective-permute-start(bf16[2048,256]{1,0:T(8,128)(2,1)} %bitcast.29), channel_id=1, source_target_pairs={{0,3},{1,2},{2,1},{3,0},{4,7},{5,6},{6,5},{7,4},{8,11},{9,10},{10,... | collective-permute-start | bytes 3145736 | tf_op jit(solution)/shard_map/ppermute | solution.py:373
  47.7 47.6 %copy-start.7 = (bf16[1,2048,256]{2,1,0:T(8,128)(2,1)S(1)}, bf16[1,2048,256]{2,1,0:T(8,128)(2,1)}, u32[]{:S(2)}) copy-start(bf16[1,2048,256]{2,1,0:T(8,128)(2,1)} %param.31) | copy-start | bytes 3145732
  47.7 47.6 %copy-start.8 = (bf16[1,2048,256]{2,1,0:T(8,128)(2,1)S(1)}, bf16[1,2048,256]{2,1,0:T(8,128)(2,1)}, u32[]{:S(2)}) copy-start(bf16[1,2048,256]{2,1,0:T(8,128)(2,1)} %param.32) | copy-start | bytes 3145732
  47.7 47.6 %collective-permute-start.6 = (bf16[512,1024]{1,0:T(8,128)(2,1)S(1)}, bf16[512,1024]{1,0:T(8,128)(2,1)S(1)}, u32[]{:S(2)}, u32[]{:S(2)}) collective-permute-start(bf16[512,1024]{1,0:T(8,128)(2,1)S(1)} %bitcast.21), channel_id=1, source_target_pairs={{0,1},{1,0},{2,3},{3,2},{4,5},{5,4},{6,7},{7,6},{8,9},{9,8},{10,11... | collective-permute-start | bytes 3145736 | tf_op jit(solution)/shard_map/ppermute | solution.py:431
  52.9 48.1 %copy-start.29 = (f32[2,512]{1,0:T(2,128)S(1)}, f32[2,512]{1,0:T(2,128)}, u32[]{:S(2)}) copy-start(f32[2,512]{1,0:T(2,128)} %param.23) | copy-start | bytes 12292
  52.9 48.2 %copy-start.30 = (f32[2,512]{1,0:T(2,128)S(1)}, f32[2,512]{1,0:T(2,128)}, u32[]{:S(2)}) copy-start(f32[2,512]{1,0:T(2,128)} %param.22) | copy-start | bytes 12292
  52.9 48.2 %copy-start = (bf16[512,2048]{1,0:T(8,128)(2,1)S(1)}, bf16[512,2048]{1,0:T(8,128)(2,1)}, u32[]{:S(2)}) copy-start(bf16[512,2048]{1,0:T(8,128)(2,1)} %rows.2) | copy-start | bytes 6291460
  52.9 48.2 %copy-start.25 = (f32[2048]{0:T(1024)S(1)}, f32[2048]{0:T(1024)}, u32[]{:S(2)}) copy-start(f32[2048]{0:T(1024)} %param.18) | copy-start | bytes 24580
  52.9 63.7 %collective-permute-start.11 = (bf16[512,1024]{1,0:T(8,128)(2,1)}, bf16[512,1024]{1,0:T(8,128)(2,1)}, u32[]{:S(2)}, u32[]{:S(2)}) collective-permute-start(bf16[512,1024]{1,0:T(8,128)(2,1)} %get-tuple-element.43), channel_id=1, source_target_pairs={{0,1},{1,0},{2,3},{3,2},{4,5},{5,4},{6,7},{7,6},{8,9},{9,8},{10,11... | collective-permute-start | bytes 3145736 | tf_op jit(solution)/shard_map/ppermute | solution.py:390
  101.0 15.6 %collective-permute-start.9 = (bf16[512,512]{1,0:T(8,128)(2,1)}, bf16[512,512]{1,0:T(8,128)(2,1)}, u32[]{:S(2)}, u32[]{:S(2)}) collective-permute-start(bf16[512,512]{1,0:T(8,128)(2,1)} %shard_map.183.own), channel_id=1, source_target_pairs={{0,1},{1,0},{2,3},{3,2},{4,5},{5,4},{6,7},{7,6},{8,9},{9,8},{10,11... | collective-permute-start | bytes 1572872 | tf_op jit(solution)/shard_map/ppermute | solution.py:433
  101.1 1.2 copy-start.1
  110.9 15.4 %all-to-all-start = ((f32[8,136,128]{2,1,0:T(8,128)}), f32[8,136,128]{2,1,0:T(8,128)S(1)}, u32[]{:S(2)}, u32[]{:S(2)}) async-start(f32[8,136,128]{2,1,0:T(8,128)} %bitcast.31), calls=%async_computation | async-start | bytes 1114112 | tf_op jit(solution)/shard_map/all_to_all | solution.py:343
  126.3 59.3 %copy-start.6 = (bf16[256,2048]{1,0:T(8,128)(2,1)S(1)}, bf16[256,2048]{1,0:T(8,128)(2,1)}, u32[]{:S(2)}) copy-start(bf16[256,2048]{1,0:T(8,128)(2,1)} %weight.1) | copy-start | bytes 3145732
  126.3 59.3 %copy-start.13 = (f32[1024,128]{1,0:T(8,128)S(1)}, f32[1024,128]{1,0:T(8,128)}, u32[]{:S(2)}) copy-start(f32[1024,128]{1,0:T(8,128)} %copy-done.12) | copy-start | bytes 1572868
  126.3 59.3 %copy-start.26 = (f32[1024]{0:T(1024)S(1)}, f32[1024]{0:T(1024)}, u32[]{:S(2)}) copy-start(f32[1024]{0:T(1024)} %param.24) | copy-start | bytes 12292
  126.3 33.5 %all-to-all-start.3 = ((bf16[32,16,1024]{2,1,0:T(8,128)(2,1)}), bf16[32,16,1024]{2,1,0:T(8,128)(2,1)S(1)}, u32[]{:S(2)}, u32[]{:S(2)}) async-start(bf16[32,16,1024]{2,1,0:T(8,128)(2,1)} %bitcast.19), calls=%async_computation.3 | async-start | bytes 2097152 | tf_op jit(solution)/shard_map/all_to_all | solution.py:343
  159.9 4.1 %copy-start.28 = (bf16[32,16,1024]{2,1,0:T(8,128)(2,1)}, bf16[32,16,1024]{2,1,0:T(8,128)(2,1)S(1)}, u32[]{:S(2)}) copy-start(bf16[32,16,1024]{2,1,0:T(8,128)(2,1)S(1)} %all-to-all-done.3) | copy-start | bytes 3145732
  159.9 19.4 %all-to-all-start.1 = ((f32[8,136,128]{2,1,0:T(8,128)}), f32[8,136,128]{2,1,0:T(8,128)S(1)}, u32[]{:S(2)}, u32[]{:S(2)}) async-start(f32[8,136,128]{2,1,0:T(8,128)} %bitcast.7), calls=%async_computation.1 | async-start | bytes 1114112 | tf_op jit(solution)/shard_map/all_to_all | solution.py:343
  163.9 40.6 %collective-permute-start.12 = (bf16[512,1024]{1,0:T(8,128)(2,1)}, bf16[512,1024]{1,0:T(8,128)(2,1)S(1)}, u32[]{:S(2)}, u32[]{:S(2)}) collective-permute-start(bf16[512,1024]{1,0:T(8,128)(2,1)} %bitcast.38), channel_id=1, source_target_pairs={{0,0},{1,1},{2,6},{3,7},{4,4},{5,5},{6,2},{7,3},{8,8},{9,9},{10,14... | collective-permute-start | bytes 3145736 | tf_op jit(solution)/shard_map/ppermute | solution.py:438
  180.2 24.4 %copy-start.22 = (f32[256,128]{1,0:T(8,128)S(1)}, f32[256,128]{1,0:T(8,128)}, u32[]{:S(2)}) copy-start(f32[256,128]{1,0:T(8,128)} %copy-done.21) | copy-start | bytes 393220
  180.8 4.8 %collective-permute-start = (f32[136,128]{1,0:T(8,128)S(1)}, f32[136,128]{1,0:T(8,128)S(1)}, u32[]{:S(2)}, u32[]{:S(2)}) collective-permute-start(f32[136,128]{1,0:T(8,128)S(1)} %get-tuple-element.32), channel_id=1, source_target_pairs={{0,4},{4,0},{1,5},{5,1},{2,6},{6,2},{3,7},{7,3},{8,12},{12,8},{9,1... | collective-permute-start | bytes 208904 | tf_op jit(solution)/shard_map/ppermute | solution.py:410
  191.5 7.7 %collective-permute-start.1 = (bf16[64,2048]{1,0:T(8,128)(2,1)S(1)}, bf16[64,2048]{1,0:T(8,128)(2,1)S(1)}, u32[]{:S(2)}, u32[]{:S(2)}) collective-permute-start(bf16[64,2048]{1,0:T(8,128)(2,1)S(1)} %get-tuple-element.36), channel_id=1, source_target_pairs={{0,1},{1,0},{2,3},{3,2},{4,5},{5,4},{6,7},{7,6},{8,9},{9,8},{10,11... | collective-permute-start | bytes 786440 | tf_op jit(solution)/shard_map/ppermute | solution.py:420
  193.1 8.4 %collective-permute-start.2 = (bf16[64,2048]{1,0:T(8,128)(2,1)S(1)}, bf16[64,2048]{1,0:T(8,128)(2,1)S(1)}, u32[]{:S(2)}, u32[]{:S(2)}) collective-permute-start(bf16[64,2048]{1,0:T(8,128)(2,1)S(1)} %get-tuple-element.37), channel_id=1, source_target_pairs={{0,3},{1,2},{2,1},{3,0},{4,7},{5,6},{6,5},{7,4},{8,11},{9,10},{10,... | collective-permute-start | bytes 786440 | tf_op jit(solution)/shard_map/ppermute | solution.py:421
  201.7 12.1 %collective-permute-start.3 = (bf16[128,2048]{1,0:T(8,128)(2,1)S(1)}, bf16[128,2048]{1,0:T(8,128)(2,1)S(1)}, u32[]{:S(2)}, u32[]{:S(2)}) collective-permute-start(bf16[128,2048]{1,0:T(8,128)(2,1)S(1)} %get-tuple-element.38), channel_id=1, source_target_pairs={{0,1},{1,0},{2,3},{3,2},{4,5},{5,4},{6,7},{7,6},{8,9},{9,8},{10,11... | collective-permute-start | bytes 1572872 | tf_op jit(solution)/shard_map/ppermute | solution.py:425
  201.8 13.2 %collective-permute-start.4 = (bf16[128,2048]{1,0:T(8,128)(2,1)S(1)}, bf16[128,2048]{1,0:T(8,128)(2,1)S(1)}, u32[]{:S(2)}, u32[]{:S(2)}) collective-permute-start(bf16[128,2048]{1,0:T(8,128)(2,1)S(1)} %get-tuple-element.39), channel_id=1, source_target_pairs={{0,3},{1,2},{2,1},{3,0},{4,7},{5,6},{6,5},{7,4},{8,11},{9,10},{10,... | collective-permute-start | bytes 1572872 | tf_op jit(solution)/shard_map/ppermute | solution.py:426
  205.5 15.2 %collective-permute-start.13 = (bf16[256,512]{1,0:T(8,128)(2,1)S(1)}, bf16[256,512]{1,0:T(8,128)(2,1)S(1)}, u32[]{:S(2)}, u32[]{:S(2)}) collective-permute-start(bf16[256,512]{1,0:T(8,128)(2,1)S(1)} %get-tuple-element.45), channel_id=1, source_target_pairs={{0,3},{1,2},{2,1},{3,0},{4,7},{5,6},{6,5},{7,4},{8,11},{9,10},{10,... | collective-permute-start | bytes 786440 | tf_op jit(solution)/shard_map/ppermute | solution.py:442
  (17 other events, 14.9 us)

commit v4 on v3

--- a/solution.py
+++ b/solution.py
@@ -14,8 +14,8 @@
 FAR = [(i, 3 - i) for i in range(4)]
 SWAP = [(0, 1), (1, 0)]
 CROSS = [(c * 4 + t, (c if t < 2 else 1 - c) * 4 + t) for c in range(2) for t in range(4)]
+LAST = [(c * 4 + t, (c if t < 2 else 1 - c) * 4 + 3 - t) for c in range(2) for t in range(4)]
 LINES = 136
-CHUNKS = 1
 f32 = jnp.float32
 bf16 = jnp.bfloat16
 
@@ -196,9 +196,21 @@
             target[units:, columns] = far_weights[:, at]
 
 
-def dispatch_kernel(place, rows, gain, group_router, expert_router, routes, *rest):
-    sends, (notes, normed) = rest[:CHUNKS], rest[CHUNKS:]
+def started(copies):
+    for copy in copies:
+        copy.start()
+    return copies
+
+
+def dispatch_kernel(
+    place, rows, gain_in, group_in, expert_in, routes, send_out, notes_out,
+    gain, group_router, expert_router, normed, send, notes, sems,
+):
     rank, core = place[0], place[1]
+    sources = ((gain_in, gain), (group_in, group_router), (expert_in, expert_router))
+    copies = started([pltpu.make_async_copy(a, b, sems.at[n]) for n, (a, b) in enumerate(sources)])
+    for copy in copies:
+        copy.wait()
     normed[...] = (normalized(rows[...].astype(f32)) * gain[...]).astype(bf16)
 
     def logits(weights):
@@ -222,8 +234,7 @@
     slots = []
     for k in range(2):
         at = jnp.sum(hot[k] * counts[k], axis=0, keepdims=True).astype(jnp.int32)
-        here = ((named[k] & 1) ^ core) == rank // 2
-        slots.append(jnp.where(here, (named[k] >> 1) * 16 + at, -1))
+        slots.append(jnp.where((named[k] & 1) == core, (named[k] >> 1) * 16 + at, -1))
     chosen = [jnp.sum(h * expert_logits, axis=0, keepdims=True) for h in hot]
     grouped = [
         jnp.sum(jnp.where(group_ids == e // (experts // groups), group_logits, 0.0), axis=0, keepdims=True)
@@ -233,68 +244,61 @@
         jax.nn.sigmoid(grouped[k]) * jax.nn.sigmoid(chosen[k] - chosen[1 - k]) for k in range(2)
     ]
     share = rows.shape[1] // 4
-    count = sends[0].shape[0]
-    each = 16 // CHUNKS
-    slot_ids = lax.broadcasted_iota(jnp.int32, (count, tokens), 0)
-    for n, send in enumerate(sends):
-        ids = (slot_ids // each) * 16 + slot_ids % each + n * each
+    row = lax.broadcasted_iota(jnp.int32, (128, tokens), 0)
+    wide = jnp.where(row == 0, slots[0].astype(f32), slots[1].astype(f32))
+    notes[...] = jnp.where(row < 2, wide, jnp.where(row == 2, combine[0], combine[1])).T
+    copies = started([pltpu.make_async_copy(notes, notes_out, sems.at[0])])
+    half = send.shape[0] // 2
+    slot_ids = lax.broadcasted_iota(jnp.int32, (half, tokens), 0)
+    for n in range(2):
+        at = pl.ds(n * half, half)
+        ids = slot_ids + n * half
         pick = ((ids == slots[0]) | (ids == slots[1])).astype(bf16)
         for j, quarter in enumerate((rank, 3 - rank)):
             features = normed[:, pl.ds(pl.multiple_of(quarter * share, share), share)]
-            send[:, j * share : (j + 1) * share] = jnp.dot(
+            send[at, j * share : (j + 1) * share] = jnp.dot(
                 pick, features, preferred_element_type=f32
             ).astype(bf16)
-    row = lax.broadcasted_iota(jnp.int32, (128, tokens), 0)
-    wide = jnp.where(row == 0, slots[0].astype(f32), slots[1].astype(f32))
-    notes[...] = jnp.where(row < 2, wide, jnp.where(row == 2, combine[0], combine[1])).T
-
-
-def hidden_kernel(place, own, other, gate, up, far_gate, far_up, out, sums):
+        copies += started([pltpu.make_async_copy(send.at[at], send_out.at[at], sems.at[n + 1])])
+    for copy in copies:
+        copy.wait()
+
+
+def hidden_kernel(
+    place, own, other, gate_in, up_in, far_gate_in, far_up_in, out,
+    rows, gate, up, far_gate, far_up, sems,
+):
+    rank = place[0]
     share = own.shape[1] // 2
     units = gate.shape[1]
-    step = pl.program_id(0)
-    for n, rows in enumerate((own, own, other, other)):
-
-        @pl.when(step == n)
-        def _():
-            features = rows[:, (n % 2) * share : (n % 2 + 1) * share]
-            for j, weight in enumerate((gate, far_gate, up, far_up)):
-                at = slice(j * units, (j + 1) * units)
-                term = jnp.dot(features, weight[...], preferred_element_type=f32)
-                sums[:, at] = term if n == 0 else sums[:, at] + term
-
-    @pl.when(step == 3)
-    def _():
-        out[...] = (jax.nn.silu(sums[:, : 2 * units]) * sums[:, 2 * units :]).astype(bf16)
-
-
-def hidden_of(place, own, other, weights):
-    share = own.shape[1] // 2
-    units = weights[0].shape[1]
-    rows = pl.BlockSpec(own.shape, lambda n, place: (0, 0))
-
-    def block(n, place):
-        device = place[0] ^ (n // 2)
-        return (jnp.where(n % 2 == 0, device, 3 - device), 0)
-
-    return pl.pallas_call(
-        hidden_kernel,
-        out_shape=jax.ShapeDtypeStruct((own.shape[0], 2 * units), bf16),
-        grid_spec=pltpu.PrefetchScalarGridSpec(
-            num_scalar_prefetch=1,
-            grid=(4,),
-            in_specs=[rows, rows] + [pl.BlockSpec((share, units), block)] * 4,
-            out_specs=pl.BlockSpec((own.shape[0], 2 * units), lambda n, place: (0, 0)),
-            scratch_shapes=[pltpu.VMEM((own.shape[0], 4 * units), f32)],
-        ),
-        compiler_params=pltpu.CompilerParams(
-            vmem_limit_bytes=16 * 1024 * 1024, dimension_semantics=("arbitrary",)
-        ),
-    )(place, own, other, *weights)
-
-
-def down_kernel(own, other, mine, theirs, out):
+    copies = []
+    for source, device in ((own, rank), (other, rank ^ 1)):
+        for j, quarter in enumerate((device, 3 - device)):
+            at = pl.ds(pl.multiple_of(quarter * share, share), share)
+            copies.append((source.at[:, j * share : (j + 1) * share], rows.at[:, at]))
+    copies += [(gate_in, gate), (up_in, up), (far_gate_in, far_gate), (far_up_in, far_up)]
+    copies = started([pltpu.make_async_copy(a, b, sems.at[n]) for n, (a, b) in enumerate(copies)])
+    for copy in copies[:5]:
+        copy.wait()
+    for part, (g, u) in enumerate(((gate, up), (far_gate, far_up))):
+        if part == 1:
+            copies[6].wait()
+        gate_act = jnp.dot(rows[...], g[...], preferred_element_type=f32)
+        copies[5 + 2 * part].wait()
+        up_act = jnp.dot(rows[...], u[...], preferred_element_type=f32)
+        out[:, part * units : (part + 1) * units] = (jax.nn.silu(gate_act) * up_act).astype(bf16)
+
+
+def down_kernel(own, other, mine_in, theirs_in, out, mine, theirs, sems):
+    copies = started(
+        [
+            pltpu.make_async_copy(mine_in, mine, sems.at[0]),
+            pltpu.make_async_copy(theirs_in, theirs, sems.at[1]),
+        ]
+    )
+    copies[0].wait()
     total = jnp.dot(own[...], mine[...], preferred_element_type=f32)
+    copies[1].wait()
     total = total + jnp.dot(other[...], theirs[...], preferred_element_type=f32)
     out[...] = total.astype(bf16)
 
@@ -314,26 +318,44 @@
     send[...] = total[:, share:].astype(bf16)
 
 
-def last_kernel(keep, received, out):
-    out[...] = (keep[...] + received[...].astype(f32)).astype(bf16)
-
-
-def run(kernel, shapes, args, place=None, scratch=(), room=8):
+def last_kernel(first, second, out):
+    out[...] = (first[...] + second[...].astype(f32)).astype(bf16)
+
+
+def run(
+    kernel, shapes, args, place=None, scratch=(), room=8,
+    hbm_in=(), hbm_out=(), sems=0, free_in=(), free_out=(),
+):
     def block(shape):
         return pl.BlockSpec(tuple(shape), lambda n: (0,) * len(shape))
 
-    specs = [block(a.shape) for a in args]
+    far = pl.BlockSpec(memory_space=pltpu.HBM)
+    near = pl.BlockSpec(memory_space=pltpu.VMEM)
+
+    def spec(n, shape, copied, free):
+        return far if n in copied else near if n in free else block(shape)
+
+    specs = [spec(n, a.shape, hbm_in, free_in) for n, a in enumerate(args)]
+    args = [
+        a if n in free_in else pltpu.with_memory_space_constraint(a, pltpu.HBM)
+        for n, a in enumerate(args)
+    ]
     if place is not None:
         specs = [pl.BlockSpec(memory_space=pltpu.SMEM)] + specs
         args = (place, *args)
-    outs = tuple(jax.ShapeDtypeStruct(s, d) for s, d in shapes)
+    outs = tuple(
+        jax.ShapeDtypeStruct(s, d) if n in free_out else pltpu.HBM(s, d) for n, (s, d) in enumerate(shapes)
+    )
+    scratch = [pltpu.VMEM(s, d) for s, d in scratch]
+    if sems:
+        scratch.append(pltpu.SemaphoreType.DMA((sems,)))
     result = pl.pallas_call(
         kernel,
         out_shape=outs,
         grid=(1,),
         in_specs=specs,
-        out_specs=tuple(block(o.shape) for o in outs),
-        scratch_shapes=[pltpu.VMEM(s, d) for s, d in scratch],
+        out_specs=tuple(spec(n, o.shape, hbm_out, free_out) for n, o in enumerate(outs)),
+        scratch_shapes=scratch,
         compiler_params=pltpu.CompilerParams(vmem_limit_bytes=room * 1024 * 1024),
     )(*args)
     return result if len(outs) > 1 else result[0]
@@ -368,24 +390,35 @@
     slots = 32 * 16
     gate, up, down = gate_experts[0], up_experts[0], down_experts[0]
     units = gate.shape[1]
+    held_rows = lax.ppermute(expert_in, ("c", "tp"), CROSS)
+    held_routes = lax.ppermute(routes.T, ("c", "tp"), CROSS)
     far_down = lax.ppermute(down, "tp", FAR)
     far_gate = lax.ppermute(gate, "tp", FAR)
     far_up = lax.ppermute(up, "tp", FAR)
-    *sends, notes = run(
+    groups, experts = group_router.shape[1], expert_router.shape[1]
+    send, notes = run(
         dispatch_kernel,
-        (((slots // CHUNKS, 2 * share), bf16),) * CHUNKS + (((tokens, 128), f32),),
-        (expert_in, expert_gain.reshape(1, -1), group_router.T, expert_router.T, routes.T),
+        (((slots, 2 * share), bf16), ((tokens, 128), f32)),
+        (held_rows, expert_gain.reshape(1, -1), group_router.T, expert_router.T, held_routes),
         place,
-        [((tokens, width), bf16)],
+        [
+            ((1, width), f32),
+            ((groups, width), bf16),
+            ((experts, width), bf16),
+            ((tokens, width), bf16),
+            ((slots, 2 * share), bf16),
+            ((tokens, 128), f32),
+        ],
         room=16,
-    )
-    arrived = []
-    for send in sends:
-        send = lax.ppermute(send, ("c", "tp"), CROSS)
-        arrived.append(traded(send, ZY))
+        hbm_in=(1, 2, 3),
+        hbm_out=(0, 1),
+        sems=3,
+        free_in=(0, 4),
+    )
+    arrived = traded(send, ZY)
 
     down_mine, give = run(
-        cut_kernel, (((2 * units, 2 * share), bf16),) * 2, (down, far_down), place, room=16
+        cut_kernel, (((2 * units, 2 * share), bf16),) * 2, (down, far_down), place, room=16, free_in=(1,)
     )
     down_theirs = lax.ppermute(give, "tp", NEAR)
 
@@ -403,10 +436,12 @@
     )
     members = traded(spread, YC)
     spread, before = run(
-        fold_slab_kernel, (((8 * LINES, 128), f32), ((2 * LINES, 128), f32)), (members,), place
+        fold_slab_kernel, (((8 * LINES, 128), f32), ((2 * LINES, 128), f32)), (members,), place, free_in=(0,)
     )
     slabs = traded(spread, "z")
-    mine, theirs = run(fold_all_kernel, (((LINES, 128), f32),) * 2, (slabs, before), place)
+    mine, theirs = run(
+        fold_all_kernel, (((LINES, 128), f32),) * 2, (slabs, before), place, free_in=(0,), free_out=(0, 1)
+    )
     theirs = lax.ppermute(theirs, "c", SWAP)
     count = row_count // 4
     own, near, far, across_near, across_far = run(
@@ -416,31 +451,49 @@
         place,
         [((row_count, local), bf16)],
         room=16,
+        free_in=(6, 7),
+        free_out=(3, 4),
     )
     from_near = lax.ppermute(across_near, "tp", NEAR)
     from_far = lax.ppermute(across_far, "tp", FAR)
     to_near, to_far = run(
-        relay_kernel, (((count, width), bf16),) * 2, (near, far, from_near, from_far)
+        relay_kernel, (((count, width), bf16),) * 2, (near, far, from_near, from_far), free_in=(2, 3), free_out=(0, 1)
     )
     near = lax.ppermute(to_near, "tp", NEAR)
     far = lax.ppermute(to_far, "tp", FAR)
-    mixer_out = run(sum_kernel, (((count, width), bf16),), (own, near, far))
-
-    pairs = []
-    for rows in arrived:
-        other_rows = lax.ppermute(rows, "tp", NEAR)
-        hidden = hidden_of(place, rows, other_rows, (gate, up, far_gate, far_up))
-        pairs += [hidden, lax.ppermute(hidden, "tp", NEAR)]
+    mixer_out = run(sum_kernel, (((count, width), bf16),), (own, near, far), free_in=(1, 2))
+
+    other_rows = lax.ppermute(arrived, "tp", NEAR)
+    hidden = run(
+        hidden_kernel,
+        (((slots, 2 * units), bf16),),
+        (arrived, other_rows, gate, up, far_gate, far_up),
+        place,
+        [((slots, width), bf16)] + [((width, units), bf16)] * 4,
+        room=16,
+        hbm_in=range(6),
+        sems=8,
+        free_out=(0,),
+    )
+    other_hidden = lax.ppermute(hidden, "tp", NEAR)
     result = run(
-        down_kernel, (((slots, 2 * share), bf16),), (*pairs, down_mine, down_theirs), room=16
+        down_kernel,
+        (((slots, 2 * share), bf16),),
+        (hidden, other_hidden, down_mine, down_theirs),
+        None,
+        [((2 * units, 2 * share), bf16)] * 2,
+        room=16,
+        hbm_in=(2, 3),
+        sems=2,
+        free_in=(0, 1),
     )
     back = traded(result, ZY)
-    back = lax.ppermute(back, ("c", "tp"), CROSS)
     keep, give = run(
-        combine_kernel, (((tokens, share), f32), ((tokens, share), bf16)), (notes, back)
-    )
-    received = lax.ppermute(give, "tp", FAR)
-    expert_out = run(last_kernel, (((tokens, share), bf16),), (keep, received))
+        combine_kernel, (((tokens, share), f32), ((tokens, share), bf16)), (notes, back), free_in=(1,), free_out=(0, 1)
+    )
+    kept = lax.ppermute(keep, ("c", "tp"), CROSS)
+    received = lax.ppermute(give, ("c", "tp"), LAST)
+    expert_out = run(last_kernel, (((tokens, share), bf16),), (kept, received), free_in=(0, 1))
     return (mixer_out, expert_out)
 
 

time: 224 us -> 169 us (0.75)
  waiting for transfers between devices: 124 us -> 67 us
  local copies, waits for them, and re-layouts: 17.4 us -> 1.21 us
  Pallas kernels: 25.1 us -> 38.4 us
  starting transfers between devices: 53.9 us -> 60.8 us
    all_to_all x4, waiting for transfers between devices: 59.8 us -> 27.1 us  [traded(): return lax.all_to_all(x, axis, 0, 0, tiled=True)]
    ppermute x1, waiting for transfers between devices: 19.8 us -> 0.01 us  [shards(): far_gate = lax.ppermute(gate, 'tp', FAR)]
    pallas_call x11 -> x12, Pallas kernels: 19.3 us -> 38.4 us  [run(): pl.pallas_call(kernel, out_shape=outs, grid=(1,), in_specs=specs, out_spe...]
    unnamed x62 -> x6, local copies, waits for them, and re-layouts: 17.4 us -> 0.01 us
    ppermute x5 -> x6, waiting for transfers between devices: 4.64 us -> 17.1 us  [the longest x1 12.4 us: shards(): other_hidden = lax.ppermute(hidden, 'tp', NEAR)]
    ppermute x5 -> x6, starting transfers between devices: 4.88 us -> 13.2 us  [the longest x1 7.81 us: shards(): received = lax.ppermute(give, ('c', 'tp'), LAST)]
    ppermute x1, waiting for transfers between devices: 8.19 us -> 0.01 us  [shards(): near = lax.ppermute(to_near, 'tp', NEAR)]
    ppermute x1, waiting for transfers between devices: 22.5 us -> 15.9 us  [shards(): far_up = lax.ppermute(up, 'tp', FAR)]
  transfers between devices with their start and end apart: 18 -> 19, of which waited for: 13 -> 9; matrix products, arithmetic and copies ran while one was open for 0% -> 1% of each run, Pallas kernels for 10% -> 20%
where the time goes in v4:
time: 169 us; the launch traced here: 168 us
  waiting for transfers between devices  67 us (40%)
  starting transfers between devices  60.8 us (36%)
  Pallas kernels  38.4 us (23%)
    pallas_call x12, Pallas kernels, run(): pl.pallas_call(kernel, out_shape=outs, grid=(1,), in_specs=specs, out_spe...  38.4 us
    all_to_all x4, starting transfers between devices, traded(): return lax.all_to_all(x, axis, 0, 0, tiled=True)  31.9 us
    all_to_all x4, waiting for transfers between devices, traded(): return lax.all_to_all(x, axis, 0, 0, tiled=True)  27.1 us
    ppermute x1, waiting for transfers between devices, shards(): far_up = lax.ppermute(up, 'tp', FAR)  15.9 us
    ppermute x1, waiting for transfers between devices, shards(): other_hidden = lax.ppermute(hidden, 'tp', NEAR)  12.4 us
    ppermute x1, starting transfers between devices, shards(): received = lax.ppermute(give, ('c', 'tp'), LAST)  7.81 us
    ppermute x1, starting transfers between devices, shards(): far_down = lax.ppermute(down, 'tp', FAR)  5.12 us
    ppermute x1, waiting for transfers between devices, shards(): from_near = lax.ppermute(across_near, 'tp', NEAR)  5.11 us
  transfers between devices with their start and end apart: 19, of which 9 were waited for; matrix products, arithmetic and copies ran while one was open for 1% of the time, Pallas kernels for 20%

profile of v4, /device:TPU:1, one launch (start us, length us, event | category | flops | bytes accessed | tf_op | source)
XLA Modules:
  0.0 168.3 jit_solution(16418696207534904796)
XLA Ops:
  0.7 2.0 %collective-permute-start.5 = (bf16[256,2048]{1,0:T(8,128)(2,1)}, bf16[256,2048]{1,0:T(8,128)(2,1)S(1)}, u32[]{:S(2)}, u32[]{:S(2)}) collective-permute-start(bf16[256,2048]{1,0:T(8,128)(2,1)} %param.26), channel_id=1, source_target_pairs={{0,0},{1,1},{2,6},{3,7},{4,4},{5,5},{6,2},{7,3},{8,8},{9,9},{10,14... | collective-permute-start | bytes 3145736 | tf_op jit(solution)/shard_map/ppermute | solution.py:393
  2.7 1.3 collective-permute-start.6
  4.1 3.9 %shard_map.182 = (bf16[512,1024]{1,0:T(8,128)(2,1)}, f32[256,128]{1,0:T(8,128)}) custom-call(s32[4]{0:T(128)S(1)} %pad_add_fusion.place, bf16[256,2048]{1,0:T(8,128)(2,1)S(1)} %collective-permute-done.5.rows, f32[1,2048]{1,0:T(1,128)} %bitcast.32, bf16[16,2048]{1,0:T(8,128)(2,1)} %bitcast.31, bf16[64,2048]{1,0:T(8,128)(2,1)} %bitcast.30, ...), custom_call_target="tpu_custom_call" | custom-call | tf_op jit(solution)/shard_map/pallas_call | solution.py:352
  8.0 12.0 %all-to-all-start.2 = ((bf16[32,16,1024]{2,1,0:T(8,128)(2,1)}), bf16[32,16,1024]{2,1,0:T(8,128)(2,1)S(1)}, u32[]{:S(2)}, u32[]{:S(2)}) async-start(bf16[32,16,1024]{2,1,0:T(8,128)(2,1)} %bitcast.27), calls=%async_computation.2 | async-start | bytes 2097152 | tf_op jit(solution)/shard_map/all_to_all | solution.py:365
  20.0 5.1 %collective-permute-start.11 = (bf16[256,2048]{1,0:T(8,128)(2,1)}, bf16[256,2048]{1,0:T(8,128)(2,1)S(1)}, u32[]{:S(2)}, u32[]{:S(2)}) collective-permute-start(bf16[256,2048]{1,0:T(8,128)(2,1)} %bitcast.18.weights), channel_id=1, source_target_pairs={{0,3},{1,2},{2,1},{3,0},{4,7},{5,6},{6,5},{7,4},{8,11},{9,10},{10,... | collective-permute-start | bytes 3145736 | tf_op jit(solution)/shard_map/ppermute | solution.py:395
  25.2 2.6 %collective-permute-start.9 = (bf16[2048,256]{1,0:T(8,128)(2,1)}, bf16[2048,256]{1,0:T(8,128)(2,1)}, u32[]{:S(2)}, u32[]{:S(2)}) collective-permute-start(bf16[2048,256]{1,0:T(8,128)(2,1)} %bitcast.17.up_in), channel_id=1, source_target_pairs={{0,3},{1,2},{2,1},{3,0},{4,7},{5,6},{6,5},{7,4},{8,11},{9,10},{10,... | collective-permute-start | bytes 3145736 | tf_op jit(solution)/shard_map/ppermute | solution.py:397
  27.8 18.4 %all-to-all-done.2 = bf16[32,16,1024]{2,1,0:T(8,128)(2,1)S(1)} async-done(((bf16[32,16,1024]{2,1,0:T(8,128)(2,1)}), bf16[32,16,1024]{2,1,0:T(8,128)(2,1)S(1)}, u32[]{:S(2)}, u32[]{:S(2)}) %all-to-all-start.2) | async-done | bytes 1048608 | tf_op jit(solution)/shard_map/all_to_all | solution.py:365
  46.2 1.2 collective-permute-start.7
  48.7 6.5 %shard_map.176 = (bf16[512,256]{1,0:T(8,128)(2,1)}, bf16[512,256]{1,0:T(8,128)(2,1)}, bf16[512,256]{1,0:T(8,128)(2,1)}, f32[1024,128]{1,0:T(8,128)}, f32[1088,128]{1,0:T(8,128)}) custom-call(bf16[512,2048]{1,0:T(8,128)(2,1)} %rows.1, f32[1,2048]{1,0:T(1,128)} %bitcast.33, bf16[2048,256]{1,0:T(8,128)(2,1)} %wq.1, bf16[2048,256]{1,0:T(8,128)(2,1)} %wk.1, ...), custom_call_target="tpu_custom_call" | custom-call | tf_op jit(solution)/shard_map/pallas_call | solution.py:352
  55.2 7.7 %all-to-all-start = ((f32[8,136,128]{2,1,0:T(8,128)}), f32[8,136,128]{2,1,0:T(8,128)S(1)}, u32[]{:S(2)}, u32[]{:S(2)}) async-start(f32[8,136,128]{2,1,0:T(8,128)} %bitcast.29), calls=%async_computation | async-start | bytes 1114112 | tf_op jit(solution)/shard_map/all_to_all | solution.py:365
  62.8 2.7 %shard_map.184 = (bf16[512,1024]{1,0:T(8,128)(2,1)}, bf16[512,1024]{1,0:T(8,128)(2,1)}) custom-call(s32[4]{0:T(128)S(1)} %pad_add_fusion.place, bf16[256,2048]{1,0:T(8,128)(2,1)} %bitcast.18.weights, bf16[256,2048]{1,0:T(8,128)(2,1)S(1)} %collective-permute-done.11.far_weights), custom_call_target="tpu_custom_call" | custom-call | tf_op jit(solution)/shard_map/pallas_call | solution.py:352
  65.8 6.7 %all-to-all-done = f32[8,136,128]{2,1,0:T(8,128)S(1)} async-done(((f32[8,136,128]{2,1,0:T(8,128)}), f32[8,136,128]{2,1,0:T(8,128)S(1)}, u32[]{:S(2)}, u32[]{:S(2)}) %all-to-all-start) | async-done | bytes 557088 | tf_op jit(solution)/shard_map/all_to_all | solution.py:365
  72.5 1.5 shard_map.177
  74.1 3.5 %all-to-all-start.1 = ((f32[8,136,128]{2,1,0:T(8,128)}), f32[8,136,128]{2,1,0:T(8,128)S(1)}, u32[]{:S(2)}, u32[]{:S(2)}) async-start(f32[8,136,128]{2,1,0:T(8,128)} %bitcast.28), calls=%async_computation.1 | async-start | bytes 1114112 | tf_op jit(solution)/shard_map/all_to_all | solution.py:365
  77.6 15.9 %collective-permute-done.9.far_up_in = bf16[2048,256]{1,0:T(8,128)(2,1)} collective-permute-done((bf16[2048,256]{1,0:T(8,128)(2,1)}, bf16[2048,256]{1,0:T(8,128)(2,1)}, u32[]{:S(2)}, u32[]{:S(2)}) %collective-permute-start.9) | collective-permute-done | bytes 1048608 | tf_op jit(solution)/shard_map/ppermute | solution.py:397
  93.5 7.4 %shard_map.183.own = bf16[512,512]{1,0:T(8,128)(2,1)S(1)} custom-call(s32[4]{0:T(128)S(1)} %pad_add_fusion.place, bf16[512,1024]{1,0:T(8,128)(2,1)} %bitcast.26, bf16[512,1024]{1,0:T(8,128)(2,1)} %collective-permute-done.7.other, bf16[2048,256]{1,0:T(8,128)(2,1)} %bitcast.16.gate_in, bf16[2048,256]{1,0:T(8,128)(2,1)} %bitcast.17.up_in, ...), custom_call_target="tpu_custom_call" | custom-call | tf_op jit(solution)/shard_map/pallas_call | solution.py:352
  101.0 12.4 %collective-permute-done.10.other = bf16[512,512]{1,0:T(8,128)(2,1)S(1)} collective-permute-done((bf16[512,512]{1,0:T(8,128)(2,1)S(1)}, bf16[512,512]{1,0:T(8,128)(2,1)S(1)}, u32[]{:S(2)}, u32[]{:S(2)}) %collective-permute-start.10) | collective-permute-done | bytes 524320 | tf_op jit(solution)/shard_map/ppermute | solution.py:478
  113.4 3.8 %shard_map.185 = bf16[512,1024]{1,0:T(8,128)(2,1)} custom-call(bf16[512,512]{1,0:T(8,128)(2,1)S(1)} %shard_map.183.own, bf16[512,512]{1,0:T(8,128)(2,1)S(1)} %collective-permute-done.10.other, bf16[512,1024]{1,0:T(8,128)(2,1)} %get-tuple-element.42.mine_in, bf16[512,1024]{1,0:T(8,128)(2,1)} %collective-permute-done.12.theirs_in), custom_call_target="tpu_custom_call" | custom-call | tf_op jit(solution)/shard_map/pallas_call | solution.py:352
  117.3 8.7 %all-to-all-start.3 = ((bf16[32,16,1024]{2,1,0:T(8,128)(2,1)}), bf16[32,16,1024]{2,1,0:T(8,128)(2,1)S(1)}, u32[]{:S(2)}, u32[]{:S(2)}) async-start(bf16[32,16,1024]{2,1,0:T(8,128)(2,1)} %bitcast.24), calls=%async_computation.3 | async-start | bytes 2097152 | tf_op jit(solution)/shard_map/all_to_all | solution.py:365
  125.9 1.0 shard_map.178
  127.0 2.5 %collective-permute-start = (f32[136,128]{1,0:T(8,128)S(1)}, f32[136,128]{1,0:T(8,128)S(1)}, u32[]{:S(2)}, u32[]{:S(2)}) collective-permute-start(f32[136,128]{1,0:T(8,128)S(1)} %get-tuple-element.32), channel_id=1, source_target_pairs={{0,4},{4,0},{1,5},{5,1},{2,6},{6,2},{3,7},{7,3},{8,12},{12,8},{9,1... | collective-permute-start | bytes 208904 | tf_op jit(solution)/shard_map/ppermute | solution.py:445
  130.4 5.6 %shard_map.179 = (bf16[128,2048]{1,0:T(8,128)(2,1)}, bf16[128,2048]{1,0:T(8,128)(2,1)}, bf16[128,2048]{1,0:T(8,128)(2,1)}, bf16[64,2048]{1,0:T(8,128)(2,1)S(1)}, bf16[64,2048]{1,0:T(8,128)(2,1)S(1)}) custom-call(s32[4]{0:T(128)S(1)} %pad_add_fusion.place, bf16[512,256]{1,0:T(8,128)(2,1)} %get-tuple-element.24.q, bf16[512,256]{1,0:T(8,128)(2,1)} %get-tuple-element.25.k, ...), custom_call_target="tpu_custom_call" | custom-call | tf_op jit(solution)/shard_map/pallas_call | solution.py:352
  136.0 2.4 %collective-permute-start.2 = (bf16[64,2048]{1,0:T(8,128)(2,1)S(1)}, bf16[64,2048]{1,0:T(8,128)(2,1)S(1)}, u32[]{:S(2)}, u32[]{:S(2)}) collective-permute-start(bf16[64,2048]{1,0:T(8,128)(2,1)S(1)} %get-tuple-element.37), channel_id=1, source_target_pairs={{0,3},{1,2},{2,1},{3,0},{4,7},{5,6},{6,5},{7,4},{8,11},{9,10},{10,... | collective-permute-start | bytes 786440 | tf_op jit(solution)/shard_map/ppermute | solution.py:458
  138.4 5.1 %collective-permute-done.1.from_near = bf16[64,2048]{1,0:T(8,128)(2,1)S(1)} collective-permute-done((bf16[64,2048]{1,0:T(8,128)(2,1)S(1)}, bf16[64,2048]{1,0:T(8,128)(2,1)S(1)}, u32[]{:S(2)}, u32[]{:S(2)}) %collective-permute-start.1) | collective-permute-done | bytes 262176 | tf_op jit(solution)/shard_map/ppermute | solution.py:457
  143.5 0.9 collective-permute-done.2.from_far
  144.5 1.4 shard_map.180
  146.8 1.8 %collective-permute-start.4 = (bf16[128,2048]{1,0:T(8,128)(2,1)S(1)}, bf16[128,2048]{1,0:T(8,128)(2,1)S(1)}, u32[]{:S(2)}, u32[]{:S(2)}) collective-permute-start(bf16[128,2048]{1,0:T(8,128)(2,1)S(1)} %get-tuple-element.39), channel_id=1, source_target_pairs={{0,3},{1,2},{2,1},{3,0},{4,7},{5,6},{6,5},{7,4},{8,11},{9,10},{10,... | collective-permute-start | bytes 1572872 | tf_op jit(solution)/shard_map/ppermute | solution.py:463
  148.6 1.9 %all-to-all-done.3 = bf16[32,16,1024]{2,1,0:T(8,128)(2,1)S(1)} async-done(((bf16[32,16,1024]{2,1,0:T(8,128)(2,1)}), bf16[32,16,1024]{2,1,0:T(8,128)(2,1)S(1)}, u32[]{:S(2)}, u32[]{:S(2)}) %all-to-all-start.3) | async-done | bytes 1048608 | tf_op jit(solution)/shard_map/all_to_all | solution.py:365
  150.5 1.8 %shard_map.186 = (f32[256,512]{1,0:T(8,128)S(1)}, bf16[256,512]{1,0:T(8,128)(2,1)S(1)}) custom-call(f32[256,128]{1,0:T(8,128)} %get-tuple-element.40.notes, bf16[512,1024]{1,0:T(8,128)(2,1)S(1)} %bitcast.21), custom_call_target="tpu_custom_call" | custom-call | tf_op jit(solution)/shard_map/pallas_call | solution.py:352
  153.0 7.8 %collective-permute-start.14 = (bf16[256,512]{1,0:T(8,128)(2,1)S(1)}, bf16[256,512]{1,0:T(8,128)(2,1)S(1)}, u32[]{:S(2)}, u32[]{:S(2)}) collective-permute-start(bf16[256,512]{1,0:T(8,128)(2,1)S(1)} %get-tuple-element.45), channel_id=1, source_target_pairs={{0,3},{1,2},{2,5},{3,4},{4,7},{5,6},{6,1},{7,0},{8,11},{9,10},{10,... | collective-permute-start | bytes 786440 | tf_op jit(solution)/shard_map/ppermute | solution.py:495
  160.8 2.0 %shard_map.181 = bf16[128,2048]{1,0:T(8,128)(2,1)} custom-call(bf16[128,2048]{1,0:T(8,128)(2,1)} %get-tuple-element.33.own, bf16[128,2048]{1,0:T(8,128)(2,1)S(1)} %collective-permute-done.3.near, bf16[128,2048]{1,0:T(8,128)(2,1)S(1)} %collective-permute-done.4.far), custom_call_target="tpu_custom_call" | custom-call | tf_op jit(solution)/shard_map/pallas_call | solution.py:352
  162.9 4.6 %collective-permute-done.14.second = bf16[256,512]{1,0:T(8,128)(2,1)S(1)} collective-permute-done((bf16[256,512]{1,0:T(8,128)(2,1)S(1)}, bf16[256,512]{1,0:T(8,128)(2,1)S(1)}, u32[]{:S(2)}, u32[]{:S(2)}) %collective-permute-start.14) | collective-permute-done | bytes 262176 | tf_op jit(solution)/shard_map/ppermute | solution.py:495
  (28 shorter events, 5.1 us)
Async XLA Ops:
  0.6 46.8 %copy-start.1 = (f32[2,512]{1,0:T(2,128)S(1)}, f32[2,512]{1,0:T(2,128)}, u32[]{:S(2)}) copy-start(f32[2,512]{1,0:T(2,128)} %param.23) | copy-start | bytes 12292
  0.6 47.4 %copy-start.2 = (f32[2,512]{1,0:T(2,128)S(1)}, f32[2,512]{1,0:T(2,128)}, u32[]{:S(2)}) copy-start(f32[2,512]{1,0:T(2,128)} %param.22) | copy-start | bytes 12292
  0.7 3.4 %collective-permute-start.5 = (bf16[256,2048]{1,0:T(8,128)(2,1)}, bf16[256,2048]{1,0:T(8,128)(2,1)S(1)}, u32[]{:S(2)}, u32[]{:S(2)}) collective-permute-start(bf16[256,2048]{1,0:T(8,128)(2,1)} %param.26), channel_id=1, source_target_pairs={{0,0},{1,1},{2,6},{3,7},{4,4},{5,5},{6,2},{7,3},{8,8},{9,9},{10,14... | collective-permute-start | bytes 3145736 | tf_op jit(solution)/shard_map/ppermute | solution.py:393
  2.7 1.4 collective-permute-start.6
  8.0 38.2 %all-to-all-start.2 = ((bf16[32,16,1024]{2,1,0:T(8,128)(2,1)}), bf16[32,16,1024]{2,1,0:T(8,128)(2,1)S(1)}, u32[]{:S(2)}, u32[]{:S(2)}) async-start(bf16[32,16,1024]{2,1,0:T(8,128)(2,1)} %bitcast.27), calls=%async_computation.2 | async-start | bytes 2097152 | tf_op jit(solution)/shard_map/all_to_all | solution.py:365
  20.0 42.8 %collective-permute-start.11 = (bf16[256,2048]{1,0:T(8,128)(2,1)}, bf16[256,2048]{1,0:T(8,128)(2,1)S(1)}, u32[]{:S(2)}, u32[]{:S(2)}) collective-permute-start(bf16[256,2048]{1,0:T(8,128)(2,1)} %bitcast.18.weights), channel_id=1, source_target_pairs={{0,3},{1,2},{2,1},{3,0},{4,7},{5,6},{6,5},{7,4},{8,11},{9,10},{10,... | collective-permute-start | bytes 3145736 | tf_op jit(solution)/shard_map/ppermute | solution.py:395
  25.1 52.5 %collective-permute-start.8 = (bf16[2048,256]{1,0:T(8,128)(2,1)}, bf16[2048,256]{1,0:T(8,128)(2,1)}, u32[]{:S(2)}, u32[]{:S(2)}) collective-permute-start(bf16[2048,256]{1,0:T(8,128)(2,1)} %bitcast.16.gate_in), channel_id=1, source_target_pairs={{0,3},{1,2},{2,1},{3,0},{4,7},{5,6},{6,5},{7,4},{8,11},{9,10},{10,... | collective-permute-start | bytes 3145736 | tf_op jit(solution)/shard_map/ppermute | solution.py:396
  25.2 68.2 %collective-permute-start.9 = (bf16[2048,256]{1,0:T(8,128)(2,1)}, bf16[2048,256]{1,0:T(8,128)(2,1)}, u32[]{:S(2)}, u32[]{:S(2)}) collective-permute-start(bf16[2048,256]{1,0:T(8,128)(2,1)} %bitcast.17.up_in), channel_id=1, source_target_pairs={{0,3},{1,2},{2,1},{3,0},{4,7},{5,6},{6,5},{7,4},{8,11},{9,10},{10,... | collective-permute-start | bytes 3145736 | tf_op jit(solution)/shard_map/ppermute | solution.py:397
  46.2 8.9 %copy-start = (bf16[32,16,1024]{2,1,0:T(8,128)(2,1)}, bf16[32,16,1024]{2,1,0:T(8,128)(2,1)S(1)}, u32[]{:S(2)}) copy-start(bf16[32,16,1024]{2,1,0:T(8,128)(2,1)S(1)} %all-to-all-done.2) | copy-start | bytes 3145732
  46.2 47.3 %collective-permute-start.7 = (bf16[512,1024]{1,0:T(8,128)(2,1)S(1)}, bf16[512,1024]{1,0:T(8,128)(2,1)}, u32[]{:S(2)}, u32[]{:S(2)}) collective-permute-start(bf16[512,1024]{1,0:T(8,128)(2,1)S(1)} %bitcast.25), channel_id=1, source_target_pairs={{0,1},{1,0},{2,3},{3,2},{4,5},{5,4},{6,7},{7,6},{8,9},{9,8},{10,11... | collective-permute-start | bytes 3145736 | tf_op jit(solution)/shard_map/ppermute | solution.py:466
  55.2 17.4 %all-to-all-start = ((f32[8,136,128]{2,1,0:T(8,128)}), f32[8,136,128]{2,1,0:T(8,128)S(1)}, u32[]{:S(2)}, u32[]{:S(2)}) async-start(f32[8,136,128]{2,1,0:T(8,128)} %bitcast.29), calls=%async_computation | async-start | bytes 1114112 | tf_op jit(solution)/shard_map/all_to_all | solution.py:365
  65.5 35.5 %collective-permute-start.12 = (bf16[512,1024]{1,0:T(8,128)(2,1)}, bf16[512,1024]{1,0:T(8,128)(2,1)}, u32[]{:S(2)}, u32[]{:S(2)}) collective-permute-start(bf16[512,1024]{1,0:T(8,128)(2,1)} %get-tuple-element.43), channel_id=1, source_target_pairs={{0,1},{1,0},{2,3},{3,2},{4,5},{5,4},{6,7},{7,6},{8,9},{9,8},{10,11... | collective-permute-start | bytes 3145736 | tf_op jit(solution)/shard_map/ppermute | solution.py:423
  74.1 43.2 %all-to-all-start.1 = ((f32[8,136,128]{2,1,0:T(8,128)}), f32[8,136,128]{2,1,0:T(8,128)S(1)}, u32[]{:S(2)}, u32[]{:S(2)}) async-start(f32[8,136,128]{2,1,0:T(8,128)} %bitcast.28), calls=%async_computation.1 | async-start | bytes 1114112 | tf_op jit(solution)/shard_map/all_to_all | solution.py:365
  100.9 12.5 %collective-permute-start.10 = (bf16[512,512]{1,0:T(8,128)(2,1)S(1)}, bf16[512,512]{1,0:T(8,128)(2,1)S(1)}, u32[]{:S(2)}, u32[]{:S(2)}) collective-permute-start(bf16[512,512]{1,0:T(8,128)(2,1)S(1)} %shard_map.183.own), channel_id=1, source_target_pairs={{0,1},{1,0},{2,3},{3,2},{4,5},{5,4},{6,7},{7,6},{8,9},{9,8},{10,11... | collective-permute-start | bytes 1572872 | tf_op jit(solution)/shard_map/ppermute | solution.py:478
  117.3 33.3 %all-to-all-start.3 = ((bf16[32,16,1024]{2,1,0:T(8,128)(2,1)}), bf16[32,16,1024]{2,1,0:T(8,128)(2,1)S(1)}, u32[]{:S(2)}, u32[]{:S(2)}) async-start(bf16[32,16,1024]{2,1,0:T(8,128)(2,1)} %bitcast.24), calls=%async_computation.3 | async-start | bytes 2097152 | tf_op jit(solution)/shard_map/all_to_all | solution.py:365
  127.0 3.4 %collective-permute-start = (f32[136,128]{1,0:T(8,128)S(1)}, f32[136,128]{1,0:T(8,128)S(1)}, u32[]{:S(2)}, u32[]{:S(2)}) collective-permute-start(f32[136,128]{1,0:T(8,128)S(1)} %get-tuple-element.32), channel_id=1, source_target_pairs={{0,4},{4,0},{1,5},{5,1},{2,6},{6,2},{3,7},{7,3},{8,12},{12,8},{9,1... | collective-permute-start | bytes 208904 | tf_op jit(solution)/shard_map/ppermute | solution.py:445
  136.0 7.5 %collective-permute-start.1 = (bf16[64,2048]{1,0:T(8,128)(2,1)S(1)}, bf16[64,2048]{1,0:T(8,128)(2,1)S(1)}, u32[]{:S(2)}, u32[]{:S(2)}) collective-permute-start(bf16[64,2048]{1,0:T(8,128)(2,1)S(1)} %get-tuple-element.36), channel_id=1, source_target_pairs={{0,1},{1,0},{2,3},{3,2},{4,5},{5,4},{6,7},{7,6},{8,9},{9,8},{10,11... | collective-permute-start | bytes 786440 | tf_op jit(solution)/shard_map/ppermute | solution.py:457
  136.0 8.4 %collective-permute-start.2 = (bf16[64,2048]{1,0:T(8,128)(2,1)S(1)}, bf16[64,2048]{1,0:T(8,128)(2,1)S(1)}, u32[]{:S(2)}, u32[]{:S(2)}) collective-permute-start(bf16[64,2048]{1,0:T(8,128)(2,1)S(1)} %get-tuple-element.37), channel_id=1, source_target_pairs={{0,3},{1,2},{2,1},{3,0},{4,7},{5,6},{6,5},{7,4},{8,11},{9,10},{10,... | collective-permute-start | bytes 786440 | tf_op jit(solution)/shard_map/ppermute | solution.py:458
  145.9 15.0 %collective-permute-start.3 = (bf16[128,2048]{1,0:T(8,128)(2,1)S(1)}, bf16[128,2048]{1,0:T(8,128)(2,1)S(1)}, u32[]{:S(2)}, u32[]{:S(2)}) collective-permute-start(bf16[128,2048]{1,0:T(8,128)(2,1)S(1)} %get-tuple-element.38), channel_id=1, source_target_pairs={{0,1},{1,0},{2,3},{3,2},{4,5},{5,4},{6,7},{7,6},{8,9},{9,8},{10,11... | collective-permute-start | bytes 1572872 | tf_op jit(solution)/shard_map/ppermute | solution.py:462
  146.8 14.0 %collective-permute-start.4 = (bf16[128,2048]{1,0:T(8,128)(2,1)S(1)}, bf16[128,2048]{1,0:T(8,128)(2,1)S(1)}, u32[]{:S(2)}, u32[]{:S(2)}) collective-permute-start(bf16[128,2048]{1,0:T(8,128)(2,1)S(1)} %get-tuple-element.39), channel_id=1, source_target_pairs={{0,3},{1,2},{2,1},{3,0},{4,7},{5,6},{6,5},{7,4},{8,11},{9,10},{10,... | collective-permute-start | bytes 1572872 | tf_op jit(solution)/shard_map/ppermute | solution.py:463
  152.3 15.2 %collective-permute-start.13 = (f32[256,512]{1,0:T(8,128)S(1)}, f32[256,512]{1,0:T(8,128)S(1)}, u32[]{:S(2)}, u32[]{:S(2)}) collective-permute-start(f32[256,512]{1,0:T(8,128)S(1)} %get-tuple-element.44), channel_id=1, source_target_pairs={{0,0},{1,1},{2,6},{3,7},{4,4},{5,5},{6,2},{7,3},{8,8},{9,9},{10,14... | collective-permute-start | bytes 1572872 | tf_op jit(solution)/shard_map/ppermute | solution.py:494
  153.0 14.5 %collective-permute-start.14 = (bf16[256,512]{1,0:T(8,128)(2,1)S(1)}, bf16[256,512]{1,0:T(8,128)(2,1)S(1)}, u32[]{:S(2)}, u32[]{:S(2)}) collective-permute-start(bf16[256,512]{1,0:T(8,128)(2,1)S(1)} %get-tuple-element.45), channel_id=1, source_target_pairs={{0,3},{1,2},{2,5},{3,4},{4,7},{5,6},{6,1},{7,0},{8,11},{9,10},{10,... | collective-permute-start | bytes 786440 | tf_op jit(solution)/shard_map/ppermute | solution.py:495
